TPU v7x, 256 devices: a whole 4x4x8 slice. The times are simulated.
256 devices in a mesh: sp: 32 (over z, y), tp: 8 (over x, core).
Axes of the slice: x: 4, y: 4, z: 8, core: 2. Of those that a mesh axis runs over, the one named last changes fastest.
Arguments:
- block_input: bfloat16 [32768, 2048], P('sp'), may hold values from -6 to 6
- value_proj: bfloat16 [2048, 1024], P(None, 'tp'), may hold values from -0.125 to 0.125
- gate_proj: bfloat16 [2048, 1024], P(None, 'tp'), may hold values from -0.125 to 0.125
- conv_taps: float32 [31, 1024], P(None, 'tp'), may hold values from -3 to 3
- norm_gain: float32 [1024], P('tp'), may hold values from 0.1 to 1.9
- out_proj: bfloat16 [2048, 1024], P(None, 'tp'), may hold values from -0.125 to 0.125
- grad_output: bfloat16 [32768, 2048], P('sp'), may hold values from -6 to 6
Outputs:
- input_grad: bfloat16 [32768, 2048], P('sp', 'tp')
- value_grad: float32 [2048, 1024], P('sp', 'tp')
- gate_grad: float32 [2048, 1024], P('sp', 'tp')
- out_grad: float32 [2048, 1024], P('sp', 'tp')
- taps_grad: float32 [31, 1024], P(None, 'tp')
- gain_grad: float32 [1024], P('tp')
All inputs are finite; a program needn't handle non-finite values.
Results may differ from a plain program's by a relative error of at most 0.015.
Values may be sent and summed in bfloat16 or wider, within the bound.
No kernel may reach another device: no remote copies, remote signals or barrier semaphores. Data moves between devices by JAX's collectives and lax.ppermute only.
A program may use at most 64 MiB of HBM per device.

v0:
```python
import jax
import jax.numpy as jnp
from jax import lax
from jax.experimental import pallas as pl
from jax.experimental.pallas import tpu as pltpu
from jax.sharding import Mesh
from jax.sharding import PartitionSpec as P


SP = ("z", "y")
TP = ("x", "c")
NZ, NY, NX, NC = 8, 4, 4, 2
C = 1024
D = 2048
K = 31
ROWS = 1024
W = 128
PAD = 32
EXT = ROWS + PAD
TAIL = 16
BLOCK = D // 8
PART = D // NY
CUT = D // (NY * NZ)
FLOOR = 0.1
F32 = jnp.float32
BF16 = jnp.bfloat16


def params(mib, **more):
    return pltpu.CompilerParams(vmem_limit_bytes=mib * 1024 * 1024, **more)


def cost(flops, size):
    return pl.CostEstimate(flops=flops, bytes_accessed=size, transcendentals=0)


def dot(a, b):
    return jnp.dot(a, b, preferred_element_type=F32)


def shape_of(shape, dtype=F32):
    return jax.ShapeDtypeStruct(shape, dtype)


def edge_kernel(
    rows, grads, value_proj, gate_proj, out_proj, to_next, to_prior, both, out_side, ends, grad_head, sems
):
    pairs = [
        (rows.at[:PAD], ends.at[:PAD]),
        (rows.at[ROWS - PAD :], ends.at[PAD:]),
        (value_proj, both.at[:, :W]),
        (gate_proj, both.at[:, W:]),
        (grads.at[:PAD], grad_head),
        (out_proj, out_side),
    ]
    copies = [pltpu.make_async_copy(a, b, sems.at[i]) for i, (a, b) in enumerate(pairs)]
    for copy in copies:
        copy.start()
    for copy in copies[:4]:
        copy.wait()
    both_parts = dot(ends[...], both[...])
    mixed = (both_parts[:, :W] * jax.nn.sigmoid(both_parts[:, W:])).astype(BF16).astype(F32)
    to_prior[:PAD] = mixed[:PAD]
    to_next[...] = mixed[PAD:]
    for copy in copies[4:]:
        copy.wait()
    to_prior[PAD:] = dot(grad_head[...], out_side[...])


def in_hbm(value):
    return pltpu.with_memory_space_constraint(value, pltpu.HBM)


def edges(block_input, grad_output, value_proj, gate_proj, out_proj):
    hbm = pl.BlockSpec(memory_space=pltpu.HBM)
    vmem = pl.BlockSpec(memory_space=pltpu.VMEM)
    args = [in_hbm(v) for v in (block_input, grad_output, value_proj, gate_proj, out_proj)]
    return pl.pallas_call(
        edge_kernel,
        in_specs=[hbm] * 5,
        out_specs=[vmem] * 4,
        out_shape=[shape_of((PAD, W)), shape_of((2 * PAD, W)), shape_of((D, 2 * W), BF16), shape_of((D, W), BF16)],
        scratch_shapes=[
            pltpu.VMEM((2 * PAD, D), BF16),
            pltpu.VMEM((PAD, D), BF16),
            pltpu.SemaphoreType.DMA((6,)),
        ],
        compiler_params=params(8),
        cost_estimate=cost(2 * 96 * D * 256, 2 * 1024 * 1024),
    )(*args)


def glu_kernel(rows, both, mixed, sgate, factor):
    step = 256
    for r in range(0, ROWS, step):
        parts = dot(rows[r : r + step, :], both[...])
        value = parts[:, :W]
        gate = jax.nn.sigmoid(parts[:, W:])
        mixed[r : r + step, :] = (value * gate).astype(BF16).astype(F32)
        sgate[r : r + step, :] = gate
        factor[r : r + step, :] = value * gate * (1.0 - gate)


def glu(block_input, both):
    return pl.pallas_call(
        glu_kernel,
        out_shape=[shape_of((ROWS, W))] * 3,
        compiler_params=params(12),
        cost_estimate=cost(2 * ROWS * D * 256, 7 * 1024 * 1024),
    )(block_input, both)


def slope_kernel(rows, out_side, both, slope, lend, sems):
    core = lax.axis_index("c")
    copies = []
    for x in range(NX):
        at = pl.multiple_of((x * NC + 1 - core) * BLOCK, BLOCK)
        copies.append(
            pltpu.make_async_copy(
                both.at[pl.ds(at, BLOCK), :], lend.at[x * BLOCK : (x + 1) * BLOCK, :], sems.at[x]
            )
        )
        copies[-1].start()
    slope[...] = dot(rows[...], out_side[...])
    for copy in copies:
        copy.wait()


def slopes_of(grad_output, out_side, both):
    vmem = pl.BlockSpec(memory_space=pltpu.VMEM)
    return pl.pallas_call(
        slope_kernel,
        in_specs=[vmem] * 3,
        out_specs=[vmem] * 2,
        out_shape=[shape_of((ROWS, W)), shape_of((NX * BLOCK, 2 * W), BF16)],
        scratch_shapes=[pltpu.SemaphoreType.DMA((NX,))],
        compiler_params=params(8),
        cost_estimate=cost(2 * ROWS * D * 256, 5 * 1024 * 1024),
    )(grad_output, out_side, both)


def store_sums(out, value, other):
    out[0, :] = jnp.sum(value, axis=1)
    out[1, :] = jnp.sum(other, axis=1)


def spread_sums(parts, outs):
    total = (parts[0][...] + parts[1][...]) + (parts[2][...] + parts[3][...])
    step = 96
    for row, out in enumerate(outs):
        mean = total[row : row + 1, :] * (1.0 / C)
        for r in range(0, EXT, step):
            out[r : r + step, :] = jnp.broadcast_to(mean[:, r : r + step], (W, step)).T


def swept(source, taps, base, step, shifts):
    total = jnp.zeros((step, W), F32)
    for residue in range(8):
        ks = [k for k in range(K) if shifts(k) % 8 == residue]
        low = min(shifts(k) for k in ks)
        high = max(shifts(k) for k in ks)
        block = source[pl.ds(base + low, step + high - low), :]
        for k in ks:
            at = shifts(k) - low
            total = total + taps[k : k + 1, :] * block[at : at + step]
    return total


def conv_kernel(mixed, prior, after, taps, history, conv, sums):
    history[:PAD] = prior[...]
    history[PAD : PAD + ROWS] = mixed[...]
    history[PAD + ROWS :] = after[:PAD]
    step = 96

    def body(i, carry):
        base = pl.multiple_of(i * step, step)
        conv[pl.ds(base, step), :] = swept(history, taps, base, step, lambda k: PAD - k)
        return carry

    lax.fori_loop(0, EXT // step, body, 0)
    value = conv[...]
    store_sums(sums, value, value * value)


def conv_of(mixed, prior, after, taps):
    return pl.pallas_call(
        conv_kernel,
        out_shape=[shape_of((EXT + PAD, W)), shape_of((EXT, W)), shape_of((2, EXT))],
        compiler_params=params(12),
        cost_estimate=cost(2 * ROWS * D * 128, 2 * 1024 * 1024),
    )(mixed, prior, after, taps)


def norm_kernel(
    conv, slope, after, gain, s0, s1, s2, s3, normed, norm_slope, inverse, activated, back, gain_part, centers, squares
):
    spread_sums((s0, s1, s2, s3), (centers, squares))
    center = centers[...]
    inv = lax.rsqrt(squares[...] - center * center + FLOOR)
    norm = (conv[...] - center) * inv
    inverse[...] = inv
    normed[...] = norm
    scale = gain[...]
    scaled = norm * scale
    squash = jax.nn.sigmoid(scaled)
    activated[...] = (scaled * squash)[:ROWS].astype(BF16)
    bend = squash * (1.0 + scaled * (1.0 - squash))
    own = slope[...] * bend[:ROWS]
    gain_part[...] = jnp.sum(own * norm[:ROWS], axis=0, keepdims=True)
    own = own * scale
    past = after[PAD:] * bend[ROWS:] * scale
    norm_slope[:ROWS] = own
    norm_slope[ROWS:] = past
    value = norm_slope[...]
    store_sums(back, value, value * norm)


def norm_of(conv, slope, after, gain, sums):
    ext = shape_of((EXT, W))
    return pl.pallas_call(
        norm_kernel,
        out_shape=[ext, ext, ext, shape_of((ROWS, W), BF16), shape_of((2, EXT)), shape_of((1, W))],
        scratch_shapes=[pltpu.VMEM((EXT, W), F32)] * 2,
        compiler_params=params(16),
        cost_estimate=cost(2 * ROWS * D * 128, 2 * 1024 * 1024),
    )(conv, slope, after, gain, *sums)


def adjoint_kernel(
    normed, norm_slope, inverse, s0, s1, s2, s3, history, taps, sgate, factor, gain_part,
    slopes, taps_part, curve, means, crosses,
):
    spread_sums((s0, s1, s2, s3), (means, crosses))
    curve[...] = inverse[...] * (norm_slope[...] - means[...] - normed[...] * crosses[...])

    @pl.when((lax.axis_index("z") == NZ - 1) & (lax.axis_index("y") == NY - 1))
    def _():
        curve[ROWS:] = jnp.zeros((PAD, W), F32)

    step = 128

    def spread(i, carry):
        base = pl.multiple_of(i * step, step)
        total = swept(curve, taps, base, step, lambda k: k)
        slopes[pl.ds(base, step), :W] = (total * sgate[pl.ds(base, step), :]).astype(BF16)
        slopes[pl.ds(base, step), W:] = (total * factor[pl.ds(base, step), :]).astype(BF16)
        return carry

    lax.fori_loop(0, ROWS // step, spread, 0)

    inner = 64

    def gather(i, sums):
        base = pl.multiple_of(i * inner, inner)
        now = curve[pl.ds(base, inner), :]
        sums = list(sums)
        for residue in range(8):
            ks = [k for k in range(K) if (PAD - k) % 8 == residue]
            low, high = PAD - max(ks), PAD - min(ks)
            block = history[pl.ds(base + low, inner + high - low), :]
            for k in ks:
                at = PAD - k - low
                sums[k] = sums[k] + jnp.sum((now * block[at : at + inner]).reshape(inner // 8, 8, W), axis=0)
        return tuple(sums)

    sums = lax.fori_loop(0, ROWS // inner, gather, tuple(jnp.zeros((8, W), F32) for _ in range(K)))
    for k in range(K):
        taps_part[k : k + 1, :] = jnp.sum(sums[k], axis=0, keepdims=True)
    taps_part[K:, :] = gain_part[...]


def adjoint_of(normed, norm_slope, inverse, back, history, taps, sgate, factor, gain_part):
    return pl.pallas_call(
        adjoint_kernel,
        out_shape=[shape_of((ROWS, 2 * W), BF16), shape_of((K + 1, W))],
        scratch_shapes=[pltpu.VMEM((EXT, W), F32)] * 3,
        compiler_params=params(16),
        cost_estimate=cost(2 * ROWS * D * 256, 2 * 1024 * 1024),
    )(normed, norm_slope, inverse, *back, history, taps, sgate, factor, gain_part)


def across(rows, side, parts):
    step = D // NZ
    for z in range(NZ):
        part = lax.dot_general(
            rows[:, z * step : (z + 1) * step], side, (((0,), (0,)), ((), ())), preferred_element_type=F32
        )
        parts[:, z * CUT : (z + 1) * CUT, :] = part.astype(BF16).reshape(NY, CUT, side.shape[1])


def out_grad_kernel(rows, activated, *rest):
    outs, parts = rest[:NY], rest[NY]
    across(rows, activated[...], parts)
    for by, out in enumerate(outs):
        out[...] = parts[lax.rem(lax.axis_index("y") + by, NY)]


def out_grad_of(grad_output, activated):
    return pl.pallas_call(
        out_grad_kernel,
        out_shape=[shape_of((PART, W), BF16)] * NY,
        scratch_shapes=[pltpu.VMEM((NY, PART, W), BF16)],
        compiler_params=params(8),
        cost_estimate=cost(2 * ROWS * D * 256, 5 * 1024 * 1024),
    )(grad_output, activated)


def weight_grad_kernel(rows, slopes, taps_part, *rest):
    outs, parts = rest[:NY], rest[NY]
    across(rows, slopes[...], parts)
    small = taps_part[...].astype(BF16)
    small = jnp.concatenate([small[:TAIL], small[TAIL:]], axis=1)
    for by, out in enumerate(outs):
        out[:PART] = parts[lax.rem(lax.axis_index("y") + by, NY)]
        out[PART:] = small


def weight_grad_of(block_input, slopes, taps_part):
    return pl.pallas_call(
        weight_grad_kernel,
        out_shape=[shape_of((PART + TAIL, 2 * W), BF16)] * NY,
        scratch_shapes=[pltpu.VMEM((NY, PART, 2 * W), BF16)],
        compiler_params=params(12),
        cost_estimate=cost(2 * ROWS * D * 256, 7 * 1024 * 1024),
    )(block_input, slopes, taps_part)


def summed(parts):
    total = parts[0][...].astype(F32)
    for part in parts[1:]:
        total = total + part[...].astype(F32)
    return total


def middle_kernel(*refs):
    both, outs, out = refs[:NY], refs[NY : 2 * NY], refs[2 * NY]
    total = summed(both).astype(BF16)
    out[:, :CUT, : 2 * W] = total[:PART].reshape(NZ, CUT, 2 * W)
    out[:, :CUT, 2 * W :] = summed(outs).astype(BF16).reshape(NZ, CUT, W)
    tail = jnp.concatenate([total[PART:], jnp.zeros((TAIL, W), BF16)], axis=1)
    for z in range(NZ):
        out[z, CUT:, :] = tail


def middle_of(both, outs):
    return pl.pallas_call(
        middle_kernel,
        out_shape=shape_of((NZ, CUT + TAIL, 3 * W), BF16),
        compiler_params=params(12),
        cost_estimate=cost(2 * ROWS * D, 2 * 1024 * 1024),
    )(*both, *outs)


def final_kernel(arrived, value_grad, gate_grad, out_grad, taps_grad, gain_grad):
    total = arrived[0].astype(F32)
    for z in range(1, NZ):
        total = total + arrived[z].astype(F32)
    value_grad[...] = total[: CUT, :W]
    gate_grad[...] = total[: CUT, W : 2 * W]
    out_grad[...] = total[: CUT, 2 * W :]
    taps_grad[:16] = total[CUT :, :W]
    taps_grad[16:] = total[CUT : CUT + 15, W : 2 * W]
    gain_grad[...] = total[CUT + 15 :, W : 2 * W]


def final_of(arrived):
    part = shape_of((CUT, W))
    return pl.pallas_call(
        final_kernel,
        out_shape=[part, part, part, shape_of((K, W)), shape_of((1, W))],
        compiler_params=params(12),
        cost_estimate=cost(2 * ROWS * D, 1024 * 1024),
    )(arrived)


def share(by, slopes, others, both, lent):
    here = lax.axis_index("x")
    core = lax.axis_index("c")
    chip = lax.rem(here + by * (1 - 2 * core) + NX, NX)
    mine = both[pl.ds(pl.multiple_of((chip * NC + core) * BLOCK, BLOCK), BLOCK), :]
    theirs = lent[pl.ds(pl.multiple_of(chip * BLOCK, BLOCK), BLOCK), :]
    contract = (((1,), (1,)), ((), ()))
    total = lax.dot_general(slopes[...], mine, contract, preferred_element_type=F32)
    return total + lax.dot_general(others[...], theirs, contract, preferred_element_type=F32)


def far_kernel(slopes, others, both, lent, far, back):
    far[...] = share(2, slopes, others, both, lent).astype(BF16)
    back[...] = share(-1, slopes, others, both, lent).astype(BF16)


def near_kernel(slopes, others, both, lent, arrived, near):
    near[...] = (share(1, slopes, others, both, lent) + arrived[...].astype(F32)).astype(BF16)


def own_kernel(slopes, others, both, lent, first, second, out):
    total = share(0, slopes, others, both, lent)
    out[...] = (total + first[...].astype(F32) + second[...].astype(F32)).astype(BF16)


def share_call(kernel, count, shares, *args):
    piece = shape_of((ROWS, BLOCK), BF16)
    return pl.pallas_call(
        kernel,
        out_shape=[piece] * count,
        compiler_params=params(12),
        cost_estimate=cost(2 * ROWS * D * 256 * shares, shares * 2 * 1024 * 1024),
    )(*args)


def from_behind(value, by):
    count = lax.axis_size(SP)
    return lax.ppermute(value, SP, [(i, i + by) for i in range(count) if 0 <= i + by < count])


def to_slot(value, slot):
    pairs = [(t, (t // NC + slot // 2) % NX * NC + (t + slot) % NC) for t in range(NX * NC)]
    return lax.ppermute(value, TP, pairs)


def chip_sums(own):
    pair = own + to_slot(own, 1)
    return [pair, to_slot(pair, 2), to_slot(pair, 6), to_slot(pair, 4)]


def along(value, by):
    pairs = [(t, (t // NC + (by if t % NC == 0 else -by)) % NX * NC + t % NC) for t in range(NX * NC)]
    return lax.ppermute(value, TP, pairs)


def spread_y(parts):
    return [parts[0]] + [
        lax.ppermute(parts[by], "y", [(y, (y + by) % NY) for y in range(NY)]) for by in (1, 3, 2)
    ]


def shards(block_input, value_proj, gate_proj, conv_taps, norm_gain, out_proj, grad_output):
    to_next, to_prior, both, out_side = edges(block_input, grad_output, value_proj, gate_proj, out_proj)
    prior = from_behind(to_next, 1)
    after = from_behind(to_prior, -1)
    mixed, sgate, factor = glu(block_input, both)
    history, conv, sums = conv_of(mixed, prior, after, conv_taps)
    sums = chip_sums(sums)
    slope, lend = slopes_of(grad_output, out_side, both)
    normed, norm_slope, inverse, activated, back, gain_part = norm_of(
        conv, slope, after, norm_gain.reshape(1, W), sums
    )
    back = chip_sums(back)
    out_parts = out_grad_of(grad_output, activated)
    out_parts = spread_y(out_parts)
    slopes, taps_part = adjoint_of(
        normed, norm_slope, inverse, back, history, conv_taps, sgate, factor, gain_part
    )
    others = to_slot(slopes, 1)
    both_parts = weight_grad_of(block_input, slopes, taps_part)
    both_parts = spread_y(both_parts)
    lent = to_slot(lend, 1)
    sides = (slopes, others, both, lent)
    far, single = share_call(far_kernel, 2, 2, *sides)
    arrived = along(far, 1)
    (near,) = share_call(near_kernel, 1, 1, *sides, arrived)
    near = along(near, 1)
    single = along(single, -1)
    partial = middle_of(both_parts, out_parts)
    partial = lax.all_to_all(partial, "z", 0, 0, tiled=True)
    (input_grad,) = share_call(own_kernel, 1, 1, *sides, near, single)
    value_grad, gate_grad, out_grad, taps_grad, gain_grad = final_of(partial)
    return (input_grad, value_grad, gate_grad, out_grad, taps_grad, gain_grad.reshape(W))


def solution(mesh):
    finer = Mesh(mesh.devices.reshape(NZ, NY, NX, NC), ("z", "y", "x", "c"))
    placed = (P(SP, None), P(None, TP), P(None, TP), P(None, TP), P(TP), P(None, TP), P(SP, None))
    split = P(SP, TP)
    return jax.shard_map(
        shards,
        mesh=finer,
        in_specs=placed,
        out_specs=(split, split, split, split, P(None, TP), P(TP)),
        check_vma=False,
    )
```

profile of v0, /device:TPU:2, one launch (start us, length us, event | category | flops | bytes accessed | tf_op | source)
XLA Modules:
  0.0 99.5 jit_solution(3232952269346665018)
XLA Ops:
  0.6 2.2 %shard_map.118 = (f32[32,128]{1,0:T(8,128)S(1)}, f32[64,128]{1,0:T(8,128)S(1)}, bf16[2048,256]{1,0:T(8,128)(2,1)S(1)}, bf16[2048,128]{1,0:T(8,128)(2,1)S(1)}) custom-call(bf16[1024,2048]{1,0:T(8,128)(2,1)} %rows.8, bf16[1024,2048]{1,0:T(8,128)(2,1)} %rows.9, bf16[2048,128]{1,0:T(8,128)(2,1)} %value_proj.1, bf16[2048,128]{1,0:T(8,128)(2,1)} %gate_proj.1, ...), custom_call_target="tpu_custom_call" | custom-call | flops 100663296 | bytes 2097152 | tf_op jit(solution)/shard_map/pallas_call | solution.py:78
  2.8 3.7 %collective-permute-start = (f32[32,128]{1,0:T(8,128)S(1)}, f32[32,128]{1,0:T(8,128)S(1)}, u32[]{:S(2)}, u32[]{:S(2)}) collective-permute-start(f32[32,128]{1,0:T(8,128)S(1)} %get-tuple-element.43), channel_id=1, source_target_pairs={{0,8},{8,16},{16,24},{24,32},{32,40},{40,48},{48,56},{56,64},{64,7... | collective-permute-start | bytes 49160 | tf_op jit(solution)/shard_map/ppermute | solution.py:413
  6.6 1.3 %collective-permute-start.1 = (f32[64,128]{1,0:T(8,128)S(1)}, f32[64,128]{1,0:T(8,128)S(1)}, u32[]{:S(2)}, u32[]{:S(2)}) collective-permute-start(f32[64,128]{1,0:T(8,128)S(1)} %get-tuple-element.44), channel_id=1, source_target_pairs={{8,0},{16,8},{24,16},{32,24},{40,32},{48,40},{56,48},{64,56},{72,6... | collective-permute-start | bytes 98312 | tf_op jit(solution)/shard_map/ppermute | solution.py:413
  7.9 1.3 %shard_map.119 = (f32[1024,128]{1,0:T(8,128)S(1)}, f32[1024,128]{1,0:T(8,128)S(1)}, f32[1024,128]{1,0:T(8,128)S(1)}) custom-call(bf16[1024,2048]{1,0:T(8,128)(2,1)S(1)} %copy-done, bf16[2048,256]{1,0:T(8,128)(2,1)S(1)} %get-tuple-element.41.both), custom_call_target="tpu_custom_call" | custom-call | flops 1073741824 | bytes 7340032 | tf_op jit(solution)/shard_map/pallas_call | solution.py:105
  9.2 3.2 %collective-permute-done.1.after = f32[64,128]{1,0:T(8,128)S(1)} collective-permute-done((f32[64,128]{1,0:T(8,128)S(1)}, f32[64,128]{1,0:T(8,128)S(1)}, u32[]{:S(2)}, u32[]{:S(2)}) %collective-permute-start.1) | collective-permute-done | bytes 32800 | tf_op jit(solution)/shard_map/ppermute | solution.py:413
  12.4 1.8 %shard_map.120 = (f32[1088,128]{1,0:T(8,128)S(1)}, f32[1056,128]{1,0:T(8,128)S(1)}, f32[2,1056]{1,0:T(2,128)S(1)}) custom-call(f32[1024,128]{1,0:T(8,128)S(1)} %get-tuple-element.42.mixed, f32[32,128]{1,0:T(8,128)S(1)} %collective-permute-done.prior, f32[64,128]{1,0:T(8,128)S(1)} %collective-permute-done.1.after, f32[31,128]{1,0:T(8,128)S(1)} %copy-done.3), custom_call_target="tpu_custom_call" | custom-call | flops 536870912 | bytes 2097152 | tf_op jit(solution)/shard_map/pallas_call | solution.py:186
  14.4 1.2 %collective-permute-done.2 = f32[2,1056]{1,0:T(2,128)S(1)} collective-permute-done((f32[2,1056]{1,0:T(2,128)S(1)}, f32[2,1056]{1,0:T(2,128)S(1)}, u32[]{:S(2)}, u32[]{:S(2)}) %collective-permute-start.2) | collective-permute-done | bytes 8480 | tf_op jit(solution)/shard_map/ppermute | solution.py:418
  15.5 2.1 %collective-permute-start.5 = (f32[2,1056]{1,0:T(2,128)S(1)}, f32[2,1056]{1,0:T(2,128)S(1)}, u32[]{:S(2)}, u32[]{:S(2)}) collective-permute-start(f32[2,1056]{1,0:T(2,128)S(1)} %add.6.s0), channel_id=1, source_target_pairs={{0,4},{1,5},{2,6},{3,7},{4,0},{5,1},{6,2},{7,3},{8,12},{9,13},{10,... | collective-permute-start | bytes 25352 | tf_op jit(solution)/shard_map/ppermute | solution.py:418
  17.6 1.4 %collective-permute-start.4 = (f32[2,1056]{1,0:T(2,128)S(1)}, f32[2,1056]{1,0:T(2,128)S(1)}, u32[]{:S(2)}, u32[]{:S(2)}) collective-permute-start(f32[2,1056]{1,0:T(2,128)S(1)} %add.6.s0), channel_id=1, source_target_pairs={{0,6},{1,7},{2,0},{3,1},{4,2},{5,3},{6,4},{7,5},{8,14},{9,15},{10,... | collective-permute-start | bytes 25352 | tf_op jit(solution)/shard_map/ppermute | solution.py:418
  19.7 1.9 %shard_map.121 = (f32[1024,128]{1,0:T(8,128)S(1)}, bf16[1024,256]{1,0:T(8,128)(2,1)S(1)}) custom-call(bf16[1024,2048]{1,0:T(8,128)(2,1)S(1)} %copy-done.1, bf16[2048,128]{1,0:T(8,128)(2,1)S(1)} %get-tuple-element.46.out_side, bf16[2048,256]{1,0:T(8,128)(2,1)S(1)} %get-tuple-element.41.both), custom_call_target="tpu_custom_call" | custom-call | flops 1073741824 | bytes 5242880 | tf_op jit(solution)/shard_map/pallas_call | solution.py:131
  23.8 1.2 %collective-permute-done.6 = f32[2,1056]{1,0:T(2,128)S(1)} collective-permute-done((f32[2,1056]{1,0:T(2,128)S(1)}, f32[2,1056]{1,0:T(2,128)S(1)}, u32[]{:S(2)}, u32[]{:S(2)}) %collective-permute-start.6) | collective-permute-done | bytes 8480 | tf_op jit(solution)/shard_map/ppermute | solution.py:418
  24.9 1.5 %collective-permute-start.9 = (f32[2,1056]{1,0:T(2,128)S(1)}, f32[2,1056]{1,0:T(2,128)S(1)}, u32[]{:S(2)}, u32[]{:S(2)}) collective-permute-start(f32[2,1056]{1,0:T(2,128)S(1)} %add.7.s0), channel_id=1, source_target_pairs={{0,4},{1,5},{2,6},{3,7},{4,0},{5,1},{6,2},{7,3},{8,12},{9,13},{10,... | collective-permute-start | bytes 25352 | tf_op jit(solution)/shard_map/ppermute | solution.py:418
  26.5 1.1 %collective-permute-start.8 = (f32[2,1056]{1,0:T(2,128)S(1)}, f32[2,1056]{1,0:T(2,128)S(1)}, u32[]{:S(2)}, u32[]{:S(2)}) collective-permute-start(f32[2,1056]{1,0:T(2,128)S(1)} %add.7.s0), channel_id=1, source_target_pairs={{0,6},{1,7},{2,0},{3,1},{4,2},{5,3},{6,4},{7,5},{8,14},{9,15},{10,... | collective-permute-start | bytes 25352 | tf_op jit(solution)/shard_map/ppermute | solution.py:418
  27.6 1.2 %collective-permute-start.7 = (f32[2,1056]{1,0:T(2,128)S(1)}, f32[2,1056]{1,0:T(2,128)S(1)}, u32[]{:S(2)}, u32[]{:S(2)}) collective-permute-start(f32[2,1056]{1,0:T(2,128)S(1)} %add.7.s0), channel_id=1, source_target_pairs={{0,2},{1,3},{2,4},{3,5},{4,6},{5,7},{6,0},{7,1},{8,10},{9,11},{10,... | collective-permute-start | bytes 25352 | tf_op jit(solution)/shard_map/ppermute | solution.py:418
  28.8 1.3 %collective-permute-done.9.s3 = f32[2,1056]{1,0:T(2,128)S(1)} collective-permute-done((f32[2,1056]{1,0:T(2,128)S(1)}, f32[2,1056]{1,0:T(2,128)S(1)}, u32[]{:S(2)}, u32[]{:S(2)}) %collective-permute-start.9) | collective-permute-done | bytes 8480 | tf_op jit(solution)/shard_map/ppermute | solution.py:418
  31.3 3.3 %shard_map.123 = (bf16[1024,256]{1,0:T(8,128)(2,1)S(1)}, f32[32,128]{1,0:T(8,128)S(1)}) custom-call(f32[1056,128]{1,0:T(8,128)S(1)} %get-tuple-element.49.normed, f32[1056,128]{1,0:T(8,128)S(1)} %get-tuple-element.50.norm_slope, f32[1056,128]{1,0:T(8,128)S(1)} %get-tuple-element.51.inverse, f32[2,1056]{1,0:T(2,128)S(1)} %add.7.s0, ...), custom_call_target="tpu_custom_call" | custom-call | flops 1073741824 | bytes 2097152 | tf_op jit(solution)/shard_map/pallas_call | solution.py:273
  34.7 1.5 %shard_map.128 = (bf16[512,128]{1,0:T(8,128)(2,1)S(1)}, bf16[512,128]{1,0:T(8,128)(2,1)S(1)}, bf16[512,128]{1,0:T(8,128)(2,1)S(1)}, bf16[512,128]{1,0:T(8,128)(2,1)S(1)}) custom-call(bf16[1024,2048]{1,0:T(8,128)(2,1)S(1)} %copy-done.1, bf16[1024,128]{1,0:T(8,128)(2,1)S(1)} %get-tuple-element.66.activated), custom_call_target="tpu_custom_call" | custom-call | flops 1073741824 | bytes 5242880 | tf_op jit(solution)/shard_map/pallas_call | solution.py:299
  36.1 1.8 %collective-permute-start.18 = (bf16[512,128]{1,0:T(8,128)(2,1)S(1)}, bf16[512,128]{1,0:T(8,128)(2,1)S(1)}, u32[]{:S(2)}, u32[]{:S(2)}) collective-permute-start(bf16[512,128]{1,0:T(8,128)(2,1)S(1)} %get-tuple-element.68), channel_id=1, source_target_pairs={{0,8},{8,16},{16,24},{24,0},{1,9},{9,17},{17,25},{25,1},{2,10},{10... | collective-permute-start | bytes 393224 | tf_op jit(solution)/shard_map/ppermute | solution.py:433
  38.0 1.5 %shard_map.124 = (bf16[1024,256]{1,0:T(8,128)(2,1)}, bf16[1024,256]{1,0:T(8,128)(2,1)S(1)}) custom-call(bf16[1024,256]{1,0:T(8,128)(2,1)S(1)} %get-tuple-element.57.slopes, bf16[1024,256]{1,0:T(8,128)(2,1)S(1)} %collective-permute-done.10.others, bf16[2048,256]{1,0:T(8,128)(2,1)S(1)} %get-tuple-element.41.both, ...), custom_call_target="tpu_custom_call" | custom-call | flops 2147483648 | bytes 4194304 | tf_op jit(solution)/shard_map/pallas_call | solution.py:403
  39.5 1.1 %collective-permute-start.12 = (bf16[1024,256]{1,0:T(8,128)(2,1)}, bf16[1024,256]{1,0:T(8,128)(2,1)}, u32[]{:S(2)}, u32[]{:S(2)}) collective-permute-start(bf16[1024,256]{1,0:T(8,128)(2,1)} %get-tuple-element.59), channel_id=1, source_target_pairs={{0,2},{1,7},{2,4},{3,1},{4,6},{5,3},{6,0},{7,5},{8,10},{9,15},{10,... | collective-permute-start | bytes 1572872 | tf_op jit(solution)/shard_map/ppermute | solution.py:428
  40.7 1.6 %shard_map.127 = (bf16[528,256]{1,0:T(8,128)(2,1)S(1)}, bf16[528,256]{1,0:T(8,128)(2,1)S(1)}, bf16[528,256]{1,0:T(8,128)(2,1)S(1)}, bf16[528,256]{1,0:T(8,128)(2,1)S(1)}) custom-call(bf16[1024,2048]{1,0:T(8,128)(2,1)S(1)} %copy-done, bf16[1024,256]{1,0:T(8,128)(2,1)S(1)} %get-tuple-element.57.slopes, f32[32,128]{1,0:T(8,128)S(1)} %get-tuple-element.61.taps_part), custom_call_target="tpu_custom_call" | custom-call | flops 1073741824 | bytes 7340032 | tf_op jit(solution)/shard_map/pallas_call | solution.py:319
  42.3 1.4 %collective-permute-start.15 = (bf16[528,256]{1,0:T(8,128)(2,1)S(1)}, bf16[528,256]{1,0:T(8,128)(2,1)S(1)}, u32[]{:S(2)}, u32[]{:S(2)}) collective-permute-start(bf16[528,256]{1,0:T(8,128)(2,1)S(1)} %get-tuple-element.63), channel_id=1, source_target_pairs={{0,8},{8,16},{16,24},{24,0},{1,9},{9,17},{17,25},{25,1},{2,10},{10... | collective-permute-start | bytes 811016 | tf_op jit(solution)/shard_map/ppermute | solution.py:433
  43.6 2.5 %collective-permute-start.16 = (bf16[528,256]{1,0:T(8,128)(2,1)S(1)}, bf16[528,256]{1,0:T(8,128)(2,1)S(1)}, u32[]{:S(2)}, u32[]{:S(2)}) collective-permute-start(bf16[528,256]{1,0:T(8,128)(2,1)S(1)} %get-tuple-element.64), channel_id=1, source_target_pairs={{0,24},{8,0},{16,8},{24,16},{1,25},{9,1},{17,9},{25,17},{2,26},{10... | collective-permute-start | bytes 811016 | tf_op jit(solution)/shard_map/ppermute | solution.py:433
  46.2 3.2 %collective-permute-start.17 = (bf16[528,256]{1,0:T(8,128)(2,1)S(1)}, bf16[528,256]{1,0:T(8,128)(2,1)S(1)}, u32[]{:S(2)}, u32[]{:S(2)}) collective-permute-start(bf16[528,256]{1,0:T(8,128)(2,1)S(1)} %get-tuple-element.65), channel_id=1, source_target_pairs={{0,16},{8,24},{16,0},{24,8},{1,17},{9,25},{17,1},{25,9},{2,18},{10... | collective-permute-start | bytes 811016 | tf_op jit(solution)/shard_map/ppermute | solution.py:433
  50.0 12.2 %collective-permute-done.19.refs_6_ = bf16[512,128]{1,0:T(8,128)(2,1)S(1)} collective-permute-done((bf16[512,128]{1,0:T(8,128)(2,1)S(1)}, bf16[512,128]{1,0:T(8,128)(2,1)S(1)}, u32[]{:S(2)}, u32[]{:S(2)}) %collective-permute-start.19) | collective-permute-done | bytes 131104 | tf_op jit(solution)/shard_map/ppermute | solution.py:433
  62.2 2.3 %collective-permute-start.20 = (bf16[512,128]{1,0:T(8,128)(2,1)S(1)}, bf16[512,128]{1,0:T(8,128)(2,1)S(1)}, u32[]{:S(2)}, u32[]{:S(2)}) collective-permute-start(bf16[512,128]{1,0:T(8,128)(2,1)S(1)} %get-tuple-element.70), channel_id=1, source_target_pairs={{0,16},{8,24},{16,0},{24,8},{1,17},{9,25},{17,1},{25,9},{2,18},{10... | collective-permute-start | bytes 393224 | tf_op jit(solution)/shard_map/ppermute | solution.py:433
  64.5 5.5 %collective-permute-done.20.refs_7_ = bf16[512,128]{1,0:T(8,128)(2,1)S(1)} collective-permute-done((bf16[512,128]{1,0:T(8,128)(2,1)S(1)}, bf16[512,128]{1,0:T(8,128)(2,1)S(1)}, u32[]{:S(2)}, u32[]{:S(2)}) %collective-permute-start.20) | collective-permute-done | bytes 131104 | tf_op jit(solution)/shard_map/ppermute | solution.py:433
  71.0 8.3 %all-to-all-start = ((bf16[8,80,384]{2,1,0:T(8,128)(2,1)}), bf16[8,80,384]{2,1,0:T(8,128)(2,1)S(1)}, u32[]{:S(2)}, u32[]{:S(2)}) async-start(bf16[8,80,384]{2,1,0:T(8,128)(2,1)} %shard_map.129), calls=%async_computation | async-start | bytes 983040 | tf_op jit(solution)/shard_map/all_to_all | solution.py:465
  79.4 1.4 %collective-permute-start.14 = (bf16[1024,256]{1,0:T(8,128)(2,1)}, bf16[1024,256]{1,0:T(8,128)(2,1)}, u32[]{:S(2)}, u32[]{:S(2)}) collective-permute-start(bf16[1024,256]{1,0:T(8,128)(2,1)} %copy-done.2), channel_id=1, source_target_pairs={{0,6},{1,3},{2,0},{3,5},{4,2},{5,7},{6,4},{7,1},{8,14},{9,11},{10,... | collective-permute-start | bytes 1572872 | tf_op jit(solution)/shard_map/ppermute | solution.py:428
  80.7 2.3 %shard_map.125 = bf16[1024,256]{1,0:T(8,128)(2,1)} custom-call(bf16[1024,256]{1,0:T(8,128)(2,1)S(1)} %get-tuple-element.57.slopes, bf16[1024,256]{1,0:T(8,128)(2,1)S(1)} %collective-permute-done.10.others, bf16[2048,256]{1,0:T(8,128)(2,1)S(1)} %get-tuple-element.41.both, bf16[1024,256]{1,0:T(8,128)(2,1)S(1)} %collective-permute-done.11.lent, ...), custom_call_target="tpu_custom_call" | custom-call | flops 1073741824 | bytes 2097152 | tf_op jit(solution)/shard_map/pallas_call | solution.py:403
  83.7 12.6 %all-to-all-done.arrived = bf16[8,80,384]{2,1,0:T(8,128)(2,1)S(1)} async-done(((bf16[8,80,384]{2,1,0:T(8,128)(2,1)}), bf16[8,80,384]{2,1,0:T(8,128)(2,1)S(1)}, u32[]{:S(2)}, u32[]{:S(2)}) %all-to-all-start) | async-done | bytes 491552 | tf_op jit(solution)/shard_map/all_to_all | solution.py:465
  97.0 2.5 %shard_map.126 = bf16[1024,256]{1,0:T(8,128)(2,1)} custom-call(bf16[1024,256]{1,0:T(8,128)(2,1)S(1)} %get-tuple-element.57.slopes, bf16[1024,256]{1,0:T(8,128)(2,1)S(1)} %collective-permute-done.10.others, bf16[2048,256]{1,0:T(8,128)(2,1)S(1)} %get-tuple-element.41.both, bf16[1024,256]{1,0:T(8,128)(2,1)S(1)} %collective-permute-done.11.lent, ...), custom_call_target="tpu_custom_call" | custom-call | flops 1073741824 | bytes 2097152 | tf_op jit(solution)/shard_map/pallas_call | solution.py:403
  (37 shorter events, 7.1 us)
Async XLA Ops:
  0.6 7.3 %copy-start = (bf16[1024,2048]{1,0:T(8,128)(2,1)S(1)}, bf16[1024,2048]{1,0:T(8,128)(2,1)}, u32[]{:S(2)}) copy-start(bf16[1024,2048]{1,0:T(8,128)(2,1)} %rows.8) | copy-start | bytes 12582916
  2.8 9.6 %copy-start.3 = (f32[31,128]{1,0:T(8,128)S(1)}, f32[31,128]{1,0:T(8,128)}, u32[]{:S(2)}) copy-start(f32[31,128]{1,0:T(8,128)} %taps.3) | copy-start | bytes 47620
  2.8 16.9 %copy-start.1 = (bf16[1024,2048]{1,0:T(8,128)(2,1)S(1)}, bf16[1024,2048]{1,0:T(8,128)(2,1)}, u32[]{:S(2)}) copy-start(bf16[1024,2048]{1,0:T(8,128)(2,1)} %rows.9) | copy-start | bytes 12582916
  2.8 6.4 %collective-permute-start = (f32[32,128]{1,0:T(8,128)S(1)}, f32[32,128]{1,0:T(8,128)S(1)}, u32[]{:S(2)}, u32[]{:S(2)}) collective-permute-start(f32[32,128]{1,0:T(8,128)S(1)} %get-tuple-element.43), channel_id=1, source_target_pairs={{0,8},{8,16},{16,24},{24,32},{32,40},{40,48},{48,56},{56,64},{64,7... | collective-permute-start | bytes 49160 | tf_op jit(solution)/shard_map/ppermute | solution.py:413
  6.6 5.8 %collective-permute-start.1 = (f32[64,128]{1,0:T(8,128)S(1)}, f32[64,128]{1,0:T(8,128)S(1)}, u32[]{:S(2)}, u32[]{:S(2)}) collective-permute-start(f32[64,128]{1,0:T(8,128)S(1)} %get-tuple-element.44), channel_id=1, source_target_pairs={{8,0},{16,8},{24,16},{32,24},{40,32},{48,40},{56,48},{64,56},{72,6... | collective-permute-start | bytes 98312 | tf_op jit(solution)/shard_map/ppermute | solution.py:413
  9.2 13.6 %copy-start.4 = (f32[128]{0:T(128)S(1)}, f32[128]{0:T(128)}, u32[]{:S(2)}) copy-start(f32[128]{0:T(128)} %param.11) | copy-start | bytes 1540
  14.2 1.3 %collective-permute-start.2 = (f32[2,1056]{1,0:T(2,128)S(1)}, f32[2,1056]{1,0:T(2,128)S(1)}, u32[]{:S(2)}, u32[]{:S(2)}) collective-permute-start(f32[2,1056]{1,0:T(2,128)S(1)} %get-tuple-element.48), channel_id=1, source_target_pairs={{0,1},{1,0},{2,3},{3,2},{4,5},{5,4},{6,7},{7,6},{8,9},{9,8},{10,11... | collective-permute-start | bytes 25352 | tf_op jit(solution)/shard_map/ppermute | solution.py:418
  15.5 6.1 %collective-permute-start.5 = (f32[2,1056]{1,0:T(2,128)S(1)}, f32[2,1056]{1,0:T(2,128)S(1)}, u32[]{:S(2)}, u32[]{:S(2)}) collective-permute-start(f32[2,1056]{1,0:T(2,128)S(1)} %add.6.s0), channel_id=1, source_target_pairs={{0,4},{1,5},{2,6},{3,7},{4,0},{5,1},{6,2},{7,3},{8,12},{9,13},{10,... | collective-permute-start | bytes 25352 | tf_op jit(solution)/shard_map/ppermute | solution.py:418
  17.6 4.0 %collective-permute-start.4 = (f32[2,1056]{1,0:T(2,128)S(1)}, f32[2,1056]{1,0:T(2,128)S(1)}, u32[]{:S(2)}, u32[]{:S(2)}) collective-permute-start(f32[2,1056]{1,0:T(2,128)S(1)} %add.6.s0), channel_id=1, source_target_pairs={{0,6},{1,7},{2,0},{3,1},{4,2},{5,3},{6,4},{7,5},{8,14},{9,15},{10,... | collective-permute-start | bytes 25352 | tf_op jit(solution)/shard_map/ppermute | solution.py:418
  19.1 3.7 %collective-permute-start.3 = (f32[2,1056]{1,0:T(2,128)S(1)}, f32[2,1056]{1,0:T(2,128)S(1)}, u32[]{:S(2)}, u32[]{:S(2)}) collective-permute-start(f32[2,1056]{1,0:T(2,128)S(1)} %add.6.s0), channel_id=1, source_target_pairs={{0,2},{1,3},{2,4},{3,5},{4,6},{5,7},{6,0},{7,1},{8,10},{9,11},{10,... | collective-permute-start | bytes 25352 | tf_op jit(solution)/shard_map/ppermute | solution.py:418
  23.7 1.3 %collective-permute-start.6 = (f32[2,1056]{1,0:T(2,128)S(1)}, f32[2,1056]{1,0:T(2,128)S(1)}, u32[]{:S(2)}, u32[]{:S(2)}) collective-permute-start(f32[2,1056]{1,0:T(2,128)S(1)} %get-tuple-element.52), channel_id=1, source_target_pairs={{0,1},{1,0},{2,3},{3,2},{4,5},{5,4},{6,7},{7,6},{8,9},{9,8},{10,11... | collective-permute-start | bytes 25352 | tf_op jit(solution)/shard_map/ppermute | solution.py:418
  24.9 5.2 %collective-permute-start.9 = (f32[2,1056]{1,0:T(2,128)S(1)}, f32[2,1056]{1,0:T(2,128)S(1)}, u32[]{:S(2)}, u32[]{:S(2)}) collective-permute-start(f32[2,1056]{1,0:T(2,128)S(1)} %add.7.s0), channel_id=1, source_target_pairs={{0,4},{1,5},{2,6},{3,7},{4,0},{5,1},{6,2},{7,3},{8,12},{9,13},{10,... | collective-permute-start | bytes 25352 | tf_op jit(solution)/shard_map/ppermute | solution.py:418
  26.5 3.9 %collective-permute-start.8 = (f32[2,1056]{1,0:T(2,128)S(1)}, f32[2,1056]{1,0:T(2,128)S(1)}, u32[]{:S(2)}, u32[]{:S(2)}) collective-permute-start(f32[2,1056]{1,0:T(2,128)S(1)} %add.7.s0), channel_id=1, source_target_pairs={{0,6},{1,7},{2,0},{3,1},{4,2},{5,3},{6,4},{7,5},{8,14},{9,15},{10,... | collective-permute-start | bytes 25352 | tf_op jit(solution)/shard_map/ppermute | solution.py:418
  27.6 3.7 %collective-permute-start.7 = (f32[2,1056]{1,0:T(2,128)S(1)}, f32[2,1056]{1,0:T(2,128)S(1)}, u32[]{:S(2)}, u32[]{:S(2)}) collective-permute-start(f32[2,1056]{1,0:T(2,128)S(1)} %add.7.s0), channel_id=1, source_target_pairs={{0,2},{1,3},{2,4},{3,5},{4,6},{5,7},{6,0},{7,1},{8,10},{9,11},{10,... | collective-permute-start | bytes 25352 | tf_op jit(solution)/shard_map/ppermute | solution.py:418
  28.8 9.2 %collective-permute-start.11 = (bf16[1024,256]{1,0:T(8,128)(2,1)S(1)}, bf16[1024,256]{1,0:T(8,128)(2,1)S(1)}, u32[]{:S(2)}, u32[]{:S(2)}) collective-permute-start(bf16[1024,256]{1,0:T(8,128)(2,1)S(1)} %get-tuple-element.58), channel_id=1, source_target_pairs={{0,1},{1,0},{2,3},{3,2},{4,5},{5,4},{6,7},{7,6},{8,9},{9,8},{10,11... | collective-permute-start | bytes 1572872 | tf_op jit(solution)/shard_map/ppermute | solution.py:418
  34.6 3.4 %collective-permute-start.10 = (bf16[1024,256]{1,0:T(8,128)(2,1)S(1)}, bf16[1024,256]{1,0:T(8,128)(2,1)S(1)}, u32[]{:S(2)}, u32[]{:S(2)}) collective-permute-start(bf16[1024,256]{1,0:T(8,128)(2,1)S(1)} %get-tuple-element.57.slopes), channel_id=1, source_target_pairs={{0,1},{1,0},{2,3},{3,2},{4,5},{5,4},{6,7},{7,6},{8,9},{9,8},{10,11... | collective-permute-start | bytes 1572872 | tf_op jit(solution)/shard_map/ppermute | solution.py:418
  36.1 13.3 %collective-permute-start.18 = (bf16[512,128]{1,0:T(8,128)(2,1)S(1)}, bf16[512,128]{1,0:T(8,128)(2,1)S(1)}, u32[]{:S(2)}, u32[]{:S(2)}) collective-permute-start(bf16[512,128]{1,0:T(8,128)(2,1)S(1)} %get-tuple-element.68), channel_id=1, source_target_pairs={{0,8},{8,16},{16,24},{24,0},{1,9},{9,17},{17,25},{25,1},{2,10},{10... | collective-permute-start | bytes 393224 | tf_op jit(solution)/shard_map/ppermute | solution.py:433
  39.5 4.1 %copy-start.2 = (bf16[1024,256]{1,0:T(8,128)(2,1)}, bf16[1024,256]{1,0:T(8,128)(2,1)S(1)}, u32[]{:S(2)}) copy-start(bf16[1024,256]{1,0:T(8,128)(2,1)S(1)} %get-tuple-element.60) | copy-start | bytes 1572868
  39.5 41.2 %collective-permute-start.12 = (bf16[1024,256]{1,0:T(8,128)(2,1)}, bf16[1024,256]{1,0:T(8,128)(2,1)}, u32[]{:S(2)}, u32[]{:S(2)}) collective-permute-start(bf16[1024,256]{1,0:T(8,128)(2,1)} %get-tuple-element.59), channel_id=1, source_target_pairs={{0,2},{1,7},{2,4},{3,1},{4,6},{5,3},{6,0},{7,5},{8,10},{9,15},{10,... | collective-permute-start | bytes 1572872 | tf_op jit(solution)/shard_map/ppermute | solution.py:428
  42.3 27.8 %collective-permute-start.15 = (bf16[528,256]{1,0:T(8,128)(2,1)S(1)}, bf16[528,256]{1,0:T(8,128)(2,1)S(1)}, u32[]{:S(2)}, u32[]{:S(2)}) collective-permute-start(bf16[528,256]{1,0:T(8,128)(2,1)S(1)} %get-tuple-element.63), channel_id=1, source_target_pairs={{0,8},{8,16},{16,24},{24,0},{1,9},{9,17},{17,25},{25,1},{2,10},{10... | collective-permute-start | bytes 811016 | tf_op jit(solution)/shard_map/ppermute | solution.py:433
  43.6 26.4 %collective-permute-start.16 = (bf16[528,256]{1,0:T(8,128)(2,1)S(1)}, bf16[528,256]{1,0:T(8,128)(2,1)S(1)}, u32[]{:S(2)}, u32[]{:S(2)}) collective-permute-start(bf16[528,256]{1,0:T(8,128)(2,1)S(1)} %get-tuple-element.64), channel_id=1, source_target_pairs={{0,24},{8,0},{16,8},{24,16},{1,25},{9,1},{17,9},{25,17},{2,26},{10... | collective-permute-start | bytes 811016 | tf_op jit(solution)/shard_map/ppermute | solution.py:433
  46.2 23.9 %collective-permute-start.17 = (bf16[528,256]{1,0:T(8,128)(2,1)S(1)}, bf16[528,256]{1,0:T(8,128)(2,1)S(1)}, u32[]{:S(2)}, u32[]{:S(2)}) collective-permute-start(bf16[528,256]{1,0:T(8,128)(2,1)S(1)} %get-tuple-element.65), channel_id=1, source_target_pairs={{0,16},{8,24},{16,0},{24,8},{1,17},{9,25},{17,1},{25,9},{2,18},{10... | collective-permute-start | bytes 811016 | tf_op jit(solution)/shard_map/ppermute | solution.py:433
  49.4 12.8 %collective-permute-start.19 = (bf16[512,128]{1,0:T(8,128)(2,1)S(1)}, bf16[512,128]{1,0:T(8,128)(2,1)S(1)}, u32[]{:S(2)}, u32[]{:S(2)}) collective-permute-start(bf16[512,128]{1,0:T(8,128)(2,1)S(1)} %get-tuple-element.69), channel_id=1, source_target_pairs={{0,24},{8,0},{16,8},{24,16},{1,25},{9,1},{17,9},{25,17},{2,26},{10... | collective-permute-start | bytes 393224 | tf_op jit(solution)/shard_map/ppermute | solution.py:433
  62.2 7.8 %collective-permute-start.20 = (bf16[512,128]{1,0:T(8,128)(2,1)S(1)}, bf16[512,128]{1,0:T(8,128)(2,1)S(1)}, u32[]{:S(2)}, u32[]{:S(2)}) collective-permute-start(bf16[512,128]{1,0:T(8,128)(2,1)S(1)} %get-tuple-element.70), channel_id=1, source_target_pairs={{0,16},{8,24},{16,0},{24,8},{1,17},{9,25},{17,1},{25,9},{2,18},{10... | collective-permute-start | bytes 393224 | tf_op jit(solution)/shard_map/ppermute | solution.py:433
  71.0 25.3 %all-to-all-start = ((bf16[8,80,384]{2,1,0:T(8,128)(2,1)}), bf16[8,80,384]{2,1,0:T(8,128)(2,1)S(1)}, u32[]{:S(2)}, u32[]{:S(2)}) async-start(bf16[8,80,384]{2,1,0:T(8,128)(2,1)} %shard_map.129), calls=%async_computation | async-start | bytes 983040 | tf_op jit(solution)/shard_map/all_to_all | solution.py:465
  79.4 17.7 %collective-permute-start.14 = (bf16[1024,256]{1,0:T(8,128)(2,1)}, bf16[1024,256]{1,0:T(8,128)(2,1)}, u32[]{:S(2)}, u32[]{:S(2)}) collective-permute-start(bf16[1024,256]{1,0:T(8,128)(2,1)} %copy-done.2), channel_id=1, source_target_pairs={{0,6},{1,3},{2,0},{3,5},{4,2},{5,7},{6,4},{7,1},{8,14},{9,11},{10,... | collective-permute-start | bytes 1572872 | tf_op jit(solution)/shard_map/ppermute | solution.py:428
  83.1 14.0 %collective-permute-start.13 = (bf16[1024,256]{1,0:T(8,128)(2,1)}, bf16[1024,256]{1,0:T(8,128)(2,1)}, u32[]{:S(2)}, u32[]{:S(2)}) collective-permute-start(bf16[1024,256]{1,0:T(8,128)(2,1)} %shard_map.125), channel_id=1, source_target_pairs={{0,2},{1,7},{2,4},{3,1},{4,6},{5,3},{6,0},{7,5},{8,10},{9,15},{10,... | collective-permute-start | bytes 1572872 | tf_op jit(solution)/shard_map/ppermute | solution.py:428
where the time goes:
time: 100 us; the launch traced here: 99.5 us
  waiting for transfers between devices  39.5 us (40%)
  starting transfers between devices  36.6 us (37%)
  Pallas kernels  22.5 us (22%)
    ppermute x6, waiting for transfers between devices, spread_y(): lax.ppermute(parts[by], 'y', [(y, (y + by) % NY) for y in range(NY)])  17.8 us
    all_to_all x1, waiting for transfers between devices, shards(): partial = lax.all_to_all(partial, 'z', 0, 0, tiled=True)  12.6 us
    ppermute x6, starting transfers between devices, spread_y(): lax.ppermute(parts[by], 'y', [(y, (y + by) % NY) for y in range(NY)])  11.9 us
    all_to_all x1, starting transfers between devices, shards(): partial = lax.all_to_all(partial, 'z', 0, 0, tiled=True)  8.32 us
    ppermute x10, starting transfers between devices, to_slot(): return lax.ppermute(value, TP, pairs)  8.25 us
    pallas_call x3, Pallas kernels, share_call(): pl.pallas_call(kernel, out_shape=[piece] * count, compiler_params=params(...  6.31 us
    ppermute x10, waiting for transfers between devices, to_slot(): return lax.ppermute(value, TP, pairs)  5.94 us
    ppermute x2, starting transfers between devices, from_behind(): lax.ppermute(value, SP, [(i, i + by) for i in range(count) if 0 <= i + by...  5.04 us
  transfers between devices with their start and end apart: 22, of which 10 were waited for; matrix products, arithmetic and copies ran while one was open for 0% of the time, Pallas kernels for 15%

commit v1 on v0

--- a/solution.py
+++ b/solution.py
@@ -333,44 +333,45 @@
 
 
 def middle_kernel(*refs):
-    both, outs, out = refs[:NY], refs[NY : 2 * NY], refs[2 * NY]
+    both, side, outs, parts = refs[:NY], refs[NY : 2 * NY], refs[2 * NY : 2 * NY + NZ], refs[2 * NY + NZ]
     total = summed(both).astype(BF16)
-    out[:, :CUT, : 2 * W] = total[:PART].reshape(NZ, CUT, 2 * W)
-    out[:, :CUT, 2 * W :] = summed(outs).astype(BF16).reshape(NZ, CUT, W)
-    tail = jnp.concatenate([total[PART:], jnp.zeros((TAIL, W), BF16)], axis=1)
-    for z in range(NZ):
-        out[z, CUT:, :] = tail
-
-
-def middle_of(both, outs):
+    parts[:, :CUT, :] = total[:PART, :W].reshape(NZ, CUT, W)
+    parts[:, CUT : 2 * CUT, :] = total[:PART, W:].reshape(NZ, CUT, W)
+    parts[:, 2 * CUT :, :] = summed(side).astype(BF16).reshape(NZ, CUT, W)
+    for by, out in enumerate(outs):
+        out[: 3 * CUT] = parts[lax.rem(lax.axis_index("z") + by, NZ)]
+        out[3 * CUT : 3 * CUT + TAIL] = total[PART:, :W]
+        out[3 * CUT + TAIL :] = total[PART:, W:]
+
+
+def middle_of(both, side):
     return pl.pallas_call(
         middle_kernel,
-        out_shape=shape_of((NZ, CUT + TAIL, 3 * W), BF16),
+        out_shape=[shape_of((3 * CUT + 2 * TAIL, W), BF16)] * NZ,
+        scratch_shapes=[pltpu.VMEM((NZ, 3 * CUT, W), BF16)],
         compiler_params=params(12),
         cost_estimate=cost(2 * ROWS * D, 2 * 1024 * 1024),
-    )(*both, *outs)
-
-
-def final_kernel(arrived, value_grad, gate_grad, out_grad, taps_grad, gain_grad):
-    total = arrived[0].astype(F32)
-    for z in range(1, NZ):
-        total = total + arrived[z].astype(F32)
-    value_grad[...] = total[: CUT, :W]
-    gate_grad[...] = total[: CUT, W : 2 * W]
-    out_grad[...] = total[: CUT, 2 * W :]
-    taps_grad[:16] = total[CUT :, :W]
-    taps_grad[16:] = total[CUT : CUT + 15, W : 2 * W]
-    gain_grad[...] = total[CUT + 15 :, W : 2 * W]
-
-
-def final_of(arrived):
+    )(*both, *side)
+
+
+def final_kernel(*refs):
+    parts, (value_grad, gate_grad, out_grad, taps_grad, gain_grad) = refs[:NZ], refs[NZ:]
+    total = summed(parts)
+    value_grad[...] = total[:CUT]
+    gate_grad[...] = total[CUT : 2 * CUT]
+    out_grad[...] = total[2 * CUT : 3 * CUT]
+    taps_grad[...] = total[3 * CUT : 3 * CUT + K]
+    gain_grad[...] = total[3 * CUT + K :]
+
+
+def final_of(parts):
     part = shape_of((CUT, W))
     return pl.pallas_call(
         final_kernel,
         out_shape=[part, part, part, shape_of((K, W)), shape_of((1, W))],
         compiler_params=params(12),
         cost_estimate=cost(2 * ROWS * D, 1024 * 1024),
-    )(arrived)
+    )(*parts)
 
 
 def share(by, slopes, others, both, lent):
@@ -428,10 +429,13 @@
     return lax.ppermute(value, TP, pairs)
 
 
-def spread_y(parts):
-    return [parts[0]] + [
-        lax.ppermute(parts[by], "y", [(y, (y + by) % NY) for y in range(NY)]) for by in (1, 3, 2)
-    ]
+def further(value, axis, by):
+    count = lax.axis_size(axis)
+    return lax.ppermute(value, axis, [(i, (i + by) % count) for i in range(count)])
+
+
+def spread(parts, axis, order):
+    return [parts[0]] + [further(parts[by], axis, by) for by in order]
 
 
 def shards(block_input, value_proj, gate_proj, conv_taps, norm_gain, out_proj, grad_output):
@@ -447,13 +451,11 @@
     )
     back = chip_sums(back)
     out_parts = out_grad_of(grad_output, activated)
-    out_parts = spread_y(out_parts)
-    slopes, taps_part = adjoint_of(
-        normed, norm_slope, inverse, back, history, conv_taps, sgate, factor, gain_part
-    )
+    out_parts = spread(out_parts, "y", Y_ORDER)
+    slopes, taps_part = adjoint_of(normed, norm_slope, inverse, back, history, conv_taps, sgate, factor, gain_part)
     others = to_slot(slopes, 1)
     both_parts = weight_grad_of(block_input, slopes, taps_part)
-    both_parts = spread_y(both_parts)
+    both_parts = spread(both_parts, "y", Y_ORDER)
     lent = to_slot(lend, 1)
     sides = (slopes, others, both, lent)
     far, single = share_call(far_kernel, 2, 2, *sides)
@@ -461,11 +463,15 @@
     (near,) = share_call(near_kernel, 1, 1, *sides, arrived)
     near = along(near, 1)
     single = along(single, -1)
-    partial = middle_of(both_parts, out_parts)
-    partial = lax.all_to_all(partial, "z", 0, 0, tiled=True)
+    parts = middle_of(both_parts, out_parts)
+    parts = spread(parts, "z", Z_ORDER)
     (input_grad,) = share_call(own_kernel, 1, 1, *sides, near, single)
-    value_grad, gate_grad, out_grad, taps_grad, gain_grad = final_of(partial)
+    value_grad, gate_grad, out_grad, taps_grad, gain_grad = final_of(parts)
     return (input_grad, value_grad, gate_grad, out_grad, taps_grad, gain_grad.reshape(W))
+
+
+Y_ORDER = (2, 1, 3)
+Z_ORDER = (4, 3, 5, 2, 6, 1, 7)
 
 
 def solution(mesh):

time: 100 us -> 96.4 us (0.964)
  starting transfers between devices: 36.6 us -> 49.1 us
  waiting for transfers between devices: 39.5 us -> 28.6 us
  Pallas kernels: 22.5 us -> 17.7 us
    ppermute x6 -> x13, starting transfers between devices: 11.9 us -> 32.2 us  [further(): lax.ppermute(value, axis, [(i, (i + by) % count) for i in range(count)])]
    all_to_all x1 -> x0, waiting for transfers between devices: 12.6 us -> none  [shards(): partial = lax.all_to_all(partial, 'z', 0, 0, tiled=True)]
    all_to_all x1 -> x0, starting transfers between devices: 8.32 us -> none  [shards(): partial = lax.all_to_all(partial, 'z', 0, 0, tiled=True)]
    pallas_call x3, Pallas kernels: 6.31 us -> 2.51 us  [share_call(): pl.pallas_call(kernel, out_shape=[piece] * count, compiler_params=params(...]
    ppermute x10, waiting for transfers between devices: 5.94 us -> 7.83 us  [to_slot(): return lax.ppermute(value, TP, pairs)]
    ppermute x6 -> x13, waiting for transfers between devices: 17.8 us -> 17.5 us  [further(): lax.ppermute(value, axis, [(i, (i + by) % count) for i in range(count)])]
  transfers between devices with their start and end apart: 22 -> 28, of which waited for: 10 -> 15; matrix products, arithmetic and copies ran while one was open for 0% -> 0% of each run, Pallas kernels for 15% -> 11%
where the time goes in v1:
time: 96.4 us; the launch traced here: 96.3 us
  starting transfers between devices  49.1 us (51%)
  waiting for transfers between devices  28.6 us (30%)
  Pallas kernels  17.7 us (18%)
    ppermute x13, starting transfers between devices, further(): lax.ppermute(value, axis, [(i, (i + by) % count) for i in range(count)])  32.2 us
    ppermute x13, waiting for transfers between devices, further(): lax.ppermute(value, axis, [(i, (i + by) % count) for i in range(count)])  17.5 us
    ppermute x10, starting transfers between devices, to_slot(): return lax.ppermute(value, TP, pairs)  8.25 us
    ppermute x10, waiting for transfers between devices, to_slot(): return lax.ppermute(value, TP, pairs)  7.83 us
    ppermute x2, starting transfers between devices, from_behind(): lax.ppermute(value, SP, [(i, i + by) for i in range(count) if 0 <= i + by...  5.04 us
    ppermute x3, starting transfers between devices, along(): return lax.ppermute(value, TP, pairs)  3.58 us
    ppermute x2, waiting for transfers between devices, from_behind(): lax.ppermute(value, SP, [(i, i + by) for i in range(count) if 0 <= i + by...  3.21 us
    pallas_call x1, Pallas kernels, adjoint_of(): pl.pallas_call(adjoint_kernel, out_shape=[shape_of((ROWS, 2 * W), BF16),...  3.09 us
  transfers between devices with their start and end apart: 28, of which 15 were waited for; matrix products, arithmetic and copies ran while one was open for 0% of the time, Pallas kernels for 11%

profile of v1, /device:TPU:2, one launch (start us, length us, event | category | flops | bytes accessed | tf_op | source)
XLA Modules:
  0.0 96.3 jit_solution(2828657168521639286)
XLA Ops:
  0.6 2.2 %shard_map.118 = (f32[32,128]{1,0:T(8,128)S(1)}, f32[64,128]{1,0:T(8,128)S(1)}, bf16[2048,256]{1,0:T(8,128)(2,1)S(1)}, bf16[2048,128]{1,0:T(8,128)(2,1)S(1)}) custom-call(bf16[1024,2048]{1,0:T(8,128)(2,1)} %rows.8, bf16[1024,2048]{1,0:T(8,128)(2,1)} %rows.9, bf16[2048,128]{1,0:T(8,128)(2,1)} %value_proj.1, bf16[2048,128]{1,0:T(8,128)(2,1)} %gate_proj.1, ...), custom_call_target="tpu_custom_call" | custom-call | flops 100663296 | bytes 2097152 | tf_op jit(solution)/shard_map/pallas_call | solution.py:78
  2.8 3.7 %collective-permute-start = (f32[32,128]{1,0:T(8,128)S(1)}, f32[32,128]{1,0:T(8,128)S(1)}, u32[]{:S(2)}, u32[]{:S(2)}) collective-permute-start(f32[32,128]{1,0:T(8,128)S(1)} %get-tuple-element.51), channel_id=1, source_target_pairs={{0,8},{8,16},{16,24},{24,32},{32,40},{40,48},{48,56},{56,64},{64,7... | collective-permute-start | bytes 49160 | tf_op jit(solution)/shard_map/ppermute | solution.py:414
  6.6 1.3 %collective-permute-start.1 = (f32[64,128]{1,0:T(8,128)S(1)}, f32[64,128]{1,0:T(8,128)S(1)}, u32[]{:S(2)}, u32[]{:S(2)}) collective-permute-start(f32[64,128]{1,0:T(8,128)S(1)} %get-tuple-element.52), channel_id=1, source_target_pairs={{8,0},{16,8},{24,16},{32,24},{40,32},{48,40},{56,48},{64,56},{72,6... | collective-permute-start | bytes 98312 | tf_op jit(solution)/shard_map/ppermute | solution.py:414
  7.9 1.3 %shard_map.119 = (f32[1024,128]{1,0:T(8,128)S(1)}, f32[1024,128]{1,0:T(8,128)S(1)}, f32[1024,128]{1,0:T(8,128)S(1)}) custom-call(bf16[1024,2048]{1,0:T(8,128)(2,1)S(1)} %copy-done, bf16[2048,256]{1,0:T(8,128)(2,1)S(1)} %get-tuple-element.49.both), custom_call_target="tpu_custom_call" | custom-call | flops 1073741824 | bytes 7340032 | tf_op jit(solution)/shard_map/pallas_call | solution.py:105
  9.2 3.2 %collective-permute-done.1.after = f32[64,128]{1,0:T(8,128)S(1)} collective-permute-done((f32[64,128]{1,0:T(8,128)S(1)}, f32[64,128]{1,0:T(8,128)S(1)}, u32[]{:S(2)}, u32[]{:S(2)}) %collective-permute-start.1) | collective-permute-done | bytes 32800 | tf_op jit(solution)/shard_map/ppermute | solution.py:414
  12.4 1.7 %shard_map.120 = (f32[1088,128]{1,0:T(8,128)S(1)}, f32[1056,128]{1,0:T(8,128)S(1)}, f32[2,1056]{1,0:T(2,128)S(1)}) custom-call(f32[1024,128]{1,0:T(8,128)S(1)} %get-tuple-element.50.mixed, f32[32,128]{1,0:T(8,128)S(1)} %collective-permute-done.prior, f32[64,128]{1,0:T(8,128)S(1)} %collective-permute-done.1.after, f32[31,128]{1,0:T(8,128)S(1)} %copy-done.2), custom_call_target="tpu_custom_call" | custom-call | flops 536870912 | bytes 2097152 | tf_op jit(solution)/shard_map/pallas_call | solution.py:186
  15.4 2.1 %collective-permute-start.5 = (f32[2,1056]{1,0:T(2,128)S(1)}, f32[2,1056]{1,0:T(2,128)S(1)}, u32[]{:S(2)}, u32[]{:S(2)}) collective-permute-start(f32[2,1056]{1,0:T(2,128)S(1)} %add.6.s0), channel_id=1, source_target_pairs={{0,4},{1,5},{2,6},{3,7},{4,0},{5,1},{6,2},{7,3},{8,12},{9,13},{10,... | collective-permute-start | bytes 25352 | tf_op jit(solution)/shard_map/ppermute | solution.py:419
  17.5 1.4 %collective-permute-start.4 = (f32[2,1056]{1,0:T(2,128)S(1)}, f32[2,1056]{1,0:T(2,128)S(1)}, u32[]{:S(2)}, u32[]{:S(2)}) collective-permute-start(f32[2,1056]{1,0:T(2,128)S(1)} %add.6.s0), channel_id=1, source_target_pairs={{0,6},{1,7},{2,0},{3,1},{4,2},{5,3},{6,4},{7,5},{8,14},{9,15},{10,... | collective-permute-start | bytes 25352 | tf_op jit(solution)/shard_map/ppermute | solution.py:419
  19.6 1.9 %shard_map.121 = (f32[1024,128]{1,0:T(8,128)S(1)}, bf16[1024,256]{1,0:T(8,128)(2,1)S(1)}) custom-call(bf16[1024,2048]{1,0:T(8,128)(2,1)S(1)} %copy-done.1, bf16[2048,128]{1,0:T(8,128)(2,1)S(1)} %get-tuple-element.54.out_side, bf16[2048,256]{1,0:T(8,128)(2,1)S(1)} %get-tuple-element.49.both), custom_call_target="tpu_custom_call" | custom-call | flops 1073741824 | bytes 5242880 | tf_op jit(solution)/shard_map/pallas_call | solution.py:131
  24.8 1.5 %collective-permute-start.9 = (f32[2,1056]{1,0:T(2,128)S(1)}, f32[2,1056]{1,0:T(2,128)S(1)}, u32[]{:S(2)}, u32[]{:S(2)}) collective-permute-start(f32[2,1056]{1,0:T(2,128)S(1)} %add.7.s0), channel_id=1, source_target_pairs={{0,4},{1,5},{2,6},{3,7},{4,0},{5,1},{6,2},{7,3},{8,12},{9,13},{10,... | collective-permute-start | bytes 25352 | tf_op jit(solution)/shard_map/ppermute | solution.py:419
  28.7 1.3 %collective-permute-done.9.s3 = f32[2,1056]{1,0:T(2,128)S(1)} collective-permute-done((f32[2,1056]{1,0:T(2,128)S(1)}, f32[2,1056]{1,0:T(2,128)S(1)}, u32[]{:S(2)}, u32[]{:S(2)}) %collective-permute-start.9) | collective-permute-done | bytes 8480 | tf_op jit(solution)/shard_map/ppermute | solution.py:419
  31.2 3.1 %shard_map.123 = (bf16[1024,256]{1,0:T(8,128)(2,1)S(1)}, f32[32,128]{1,0:T(8,128)S(1)}) custom-call(f32[1056,128]{1,0:T(8,128)S(1)} %get-tuple-element.57.normed, f32[1056,128]{1,0:T(8,128)S(1)} %get-tuple-element.58.norm_slope, f32[1056,128]{1,0:T(8,128)S(1)} %get-tuple-element.59.inverse, f32[2,1056]{1,0:T(2,128)S(1)} %add.7.s0, ...), custom_call_target="tpu_custom_call" | custom-call | flops 1073741824 | bytes 2097152 | tf_op jit(solution)/shard_map/pallas_call | solution.py:273
  34.4 1.9 %collective-permute-done.10.others = bf16[1024,256]{1,0:T(8,128)(2,1)S(1)} collective-permute-done((bf16[1024,256]{1,0:T(8,128)(2,1)S(1)}, bf16[1024,256]{1,0:T(8,128)(2,1)S(1)}, u32[]{:S(2)}, u32[]{:S(2)}) %collective-permute-start.10) | collective-permute-done | bytes 524320 | tf_op jit(solution)/shard_map/ppermute | solution.py:419
  37.0 1.4 %collective-permute-start.12 = (bf16[1024,256]{1,0:T(8,128)(2,1)S(1)}, bf16[1024,256]{1,0:T(8,128)(2,1)S(1)}, u32[]{:S(2)}, u32[]{:S(2)}) collective-permute-start(bf16[1024,256]{1,0:T(8,128)(2,1)S(1)} %get-tuple-element.67), channel_id=1, source_target_pairs={{0,2},{1,7},{2,4},{3,1},{4,6},{5,3},{6,0},{7,5},{8,10},{9,15},{10,... | collective-permute-start | bytes 1572872 | tf_op jit(solution)/shard_map/ppermute | solution.py:429
  38.4 1.5 %shard_map.128 = (bf16[512,128]{1,0:T(8,128)(2,1)S(1)}, bf16[512,128]{1,0:T(8,128)(2,1)S(1)}, bf16[512,128]{1,0:T(8,128)(2,1)S(1)}, bf16[512,128]{1,0:T(8,128)(2,1)S(1)}) custom-call(bf16[1024,2048]{1,0:T(8,128)(2,1)S(1)} %copy-done.1, bf16[1024,128]{1,0:T(8,128)(2,1)S(1)} %get-tuple-element.74.activated), custom_call_target="tpu_custom_call" | custom-call | flops 1073741824 | bytes 5242880 | tf_op jit(solution)/shard_map/pallas_call | solution.py:299
  39.9 3.0 %collective-permute-start.18 = (bf16[512,128]{1,0:T(8,128)(2,1)S(1)}, bf16[512,128]{1,0:T(8,128)(2,1)S(1)}, u32[]{:S(2)}, u32[]{:S(2)}) collective-permute-start(bf16[512,128]{1,0:T(8,128)(2,1)S(1)} %get-tuple-element.76), channel_id=1, source_target_pairs={{0,16},{8,24},{16,0},{24,8},{1,17},{9,25},{17,1},{25,9},{2,18},{10... | collective-permute-start | bytes 393224 | tf_op jit(solution)/shard_map/ppermute | solution.py:434
  42.9 3.1 %collective-permute-start.19 = (bf16[512,128]{1,0:T(8,128)(2,1)S(1)}, bf16[512,128]{1,0:T(8,128)(2,1)S(1)}, u32[]{:S(2)}, u32[]{:S(2)}) collective-permute-start(bf16[512,128]{1,0:T(8,128)(2,1)S(1)} %get-tuple-element.77), channel_id=1, source_target_pairs={{0,8},{8,16},{16,24},{24,0},{1,9},{9,17},{17,25},{25,1},{2,10},{10... | collective-permute-start | bytes 393224 | tf_op jit(solution)/shard_map/ppermute | solution.py:434
  46.1 2.1 %collective-permute-start.14 = (bf16[1024,256]{1,0:T(8,128)(2,1)S(1)}, bf16[1024,256]{1,0:T(8,128)(2,1)S(1)}, u32[]{:S(2)}, u32[]{:S(2)}) collective-permute-start(bf16[1024,256]{1,0:T(8,128)(2,1)S(1)} %get-tuple-element.68), channel_id=1, source_target_pairs={{0,6},{1,3},{2,0},{3,5},{4,2},{5,7},{6,4},{7,1},{8,14},{9,11},{10,... | collective-permute-start | bytes 1572872 | tf_op jit(solution)/shard_map/ppermute | solution.py:429
  48.8 1.6 %shard_map.127 = (bf16[528,256]{1,0:T(8,128)(2,1)S(1)}, bf16[528,256]{1,0:T(8,128)(2,1)S(1)}, bf16[528,256]{1,0:T(8,128)(2,1)S(1)}, bf16[528,256]{1,0:T(8,128)(2,1)S(1)}) custom-call(bf16[1024,2048]{1,0:T(8,128)(2,1)S(1)} %copy-done, bf16[1024,256]{1,0:T(8,128)(2,1)S(1)} %get-tuple-element.65.slopes, f32[32,128]{1,0:T(8,128)S(1)} %get-tuple-element.69.taps_part), custom_call_target="tpu_custom_call" | custom-call | flops 1073741824 | bytes 7340032 | tf_op jit(solution)/shard_map/pallas_call | solution.py:319
  50.4 2.4 %collective-permute-start.15 = (bf16[528,256]{1,0:T(8,128)(2,1)S(1)}, bf16[528,256]{1,0:T(8,128)(2,1)S(1)}, u32[]{:S(2)}, u32[]{:S(2)}) collective-permute-start(bf16[528,256]{1,0:T(8,128)(2,1)S(1)} %get-tuple-element.71), channel_id=1, source_target_pairs={{0,16},{8,24},{16,0},{24,8},{1,17},{9,25},{17,1},{25,9},{2,18},{10... | collective-permute-start | bytes 811016 | tf_op jit(solution)/shard_map/ppermute | solution.py:434
  52.8 5.8 %collective-permute-start.16 = (bf16[528,256]{1,0:T(8,128)(2,1)S(1)}, bf16[528,256]{1,0:T(8,128)(2,1)S(1)}, u32[]{:S(2)}, u32[]{:S(2)}) collective-permute-start(bf16[528,256]{1,0:T(8,128)(2,1)S(1)} %get-tuple-element.72), channel_id=1, source_target_pairs={{0,8},{8,16},{16,24},{24,0},{1,9},{9,17},{17,25},{25,1},{2,10},{10... | collective-permute-start | bytes 811016 | tf_op jit(solution)/shard_map/ppermute | solution.py:434
  58.7 2.7 %collective-permute-done.15.refs_1_ = bf16[528,256]{1,0:T(8,128)(2,1)S(1)} collective-permute-done((bf16[528,256]{1,0:T(8,128)(2,1)S(1)}, bf16[528,256]{1,0:T(8,128)(2,1)S(1)}, u32[]{:S(2)}, u32[]{:S(2)}) %collective-permute-start.15) | collective-permute-done | bytes 270368 | tf_op jit(solution)/shard_map/ppermute | solution.py:434
  61.4 5.4 %collective-permute-done.16.refs_2_ = bf16[528,256]{1,0:T(8,128)(2,1)S(1)} collective-permute-done((bf16[528,256]{1,0:T(8,128)(2,1)S(1)}, bf16[528,256]{1,0:T(8,128)(2,1)S(1)}, u32[]{:S(2)}, u32[]{:S(2)}) %collective-permute-start.16) | collective-permute-done | bytes 270368 | tf_op jit(solution)/shard_map/ppermute | solution.py:434
  66.8 3.4 %collective-permute-done.17.refs_3_ = bf16[528,256]{1,0:T(8,128)(2,1)S(1)} collective-permute-done((bf16[528,256]{1,0:T(8,128)(2,1)S(1)}, bf16[528,256]{1,0:T(8,128)(2,1)S(1)}, u32[]{:S(2)}, u32[]{:S(2)}) %collective-permute-start.17) | collective-permute-done | bytes 270368 | tf_op jit(solution)/shard_map/ppermute | solution.py:434
  70.5 6.4 %collective-permute-start.21 = (bf16[224,128]{1,0:T(8,128)(2,1)S(1)}, bf16[224,128]{1,0:T(8,128)(2,1)S(1)}, u32[]{:S(2)}, u32[]{:S(2)}) collective-permute-start(bf16[224,128]{1,0:T(8,128)(2,1)S(1)} %get-tuple-element.80), channel_id=1, source_target_pairs={{0,128},{32,160},{64,192},{96,224},{128,0},{160,32},{192,64},{224,... | collective-permute-start | bytes 172040 | tf_op jit(solution)/shard_map/ppermute | solution.py:434
  77.8 4.2 %collective-permute-start.23 = (bf16[224,128]{1,0:T(8,128)(2,1)S(1)}, bf16[224,128]{1,0:T(8,128)(2,1)S(1)}, u32[]{:S(2)}, u32[]{:S(2)}) collective-permute-start(bf16[224,128]{1,0:T(8,128)(2,1)S(1)} %get-tuple-element.82), channel_id=1, source_target_pairs={{0,160},{32,192},{64,224},{96,0},{128,32},{160,64},{192,96},{224,1... | collective-permute-start | bytes 172040 | tf_op jit(solution)/shard_map/ppermute | solution.py:434
  82.0 1.5 %collective-permute-start.24 = (bf16[224,128]{1,0:T(8,128)(2,1)S(1)}, bf16[224,128]{1,0:T(8,128)(2,1)S(1)}, u32[]{:S(2)}, u32[]{:S(2)}) collective-permute-start(bf16[224,128]{1,0:T(8,128)(2,1)S(1)} %get-tuple-element.83), channel_id=1, source_target_pairs={{0,64},{32,96},{64,128},{96,160},{128,192},{160,224},{192,0},{224,... | collective-permute-start | bytes 172040 | tf_op jit(solution)/shard_map/ppermute | solution.py:434
  83.4 2.6 %collective-permute-done.22.refs_2_ = bf16[224,128]{1,0:T(8,128)(2,1)S(1)} collective-permute-done((bf16[224,128]{1,0:T(8,128)(2,1)S(1)}, bf16[224,128]{1,0:T(8,128)(2,1)S(1)}, u32[]{:S(2)}, u32[]{:S(2)}) %collective-permute-start.22) | collective-permute-done | bytes 57376 | tf_op jit(solution)/shard_map/ppermute | solution.py:434
  86.1 1.6 %collective-permute-start.25 = (bf16[224,128]{1,0:T(8,128)(2,1)S(1)}, bf16[224,128]{1,0:T(8,128)(2,1)S(1)}, u32[]{:S(2)}, u32[]{:S(2)}) collective-permute-start(bf16[224,128]{1,0:T(8,128)(2,1)S(1)} %get-tuple-element.84), channel_id=1, source_target_pairs={{0,192},{32,224},{64,0},{96,32},{128,64},{160,96},{192,128},{224,1... | collective-permute-start | bytes 172040 | tf_op jit(solution)/shard_map/ppermute | solution.py:434
  87.7 2.4 %collective-permute-start.26 = (bf16[224,128]{1,0:T(8,128)(2,1)S(1)}, bf16[224,128]{1,0:T(8,128)(2,1)S(1)}, u32[]{:S(2)}, u32[]{:S(2)}) collective-permute-start(bf16[224,128]{1,0:T(8,128)(2,1)S(1)} %get-tuple-element.85), channel_id=1, source_target_pairs={{0,32},{32,64},{64,96},{96,128},{128,160},{160,192},{192,224},{224... | collective-permute-start | bytes 172040 | tf_op jit(solution)/shard_map/ppermute | solution.py:434
  91.8 1.3 %collective-permute-done.26.refs_6_ = bf16[224,128]{1,0:T(8,128)(2,1)S(1)} collective-permute-done((bf16[224,128]{1,0:T(8,128)(2,1)S(1)}, bf16[224,128]{1,0:T(8,128)(2,1)S(1)}, u32[]{:S(2)}, u32[]{:S(2)}) %collective-permute-start.26) | collective-permute-done | bytes 57376 | tf_op jit(solution)/shard_map/ppermute | solution.py:434
  95.0 1.3 %shard_map.126 = bf16[1024,256]{1,0:T(8,128)(2,1)} custom-call(bf16[1024,256]{1,0:T(8,128)(2,1)S(1)} %get-tuple-element.65.slopes, bf16[1024,256]{1,0:T(8,128)(2,1)S(1)} %collective-permute-done.10.others, bf16[2048,256]{1,0:T(8,128)(2,1)S(1)} %get-tuple-element.49.both, bf16[1024,256]{1,0:T(8,128)(2,1)S(1)} %collective-permute-done.11.lent, ...), custom_call_target="tpu_custom_call" | custom-call | flops 1073741824 | bytes 2097152 | tf_op jit(solution)/shard_map/pallas_call | solution.py:404
  (47 shorter events, 14.9 us)
Async XLA Ops:
  0.6 7.3 %copy-start = (bf16[1024,2048]{1,0:T(8,128)(2,1)S(1)}, bf16[1024,2048]{1,0:T(8,128)(2,1)}, u32[]{:S(2)}) copy-start(bf16[1024,2048]{1,0:T(8,128)(2,1)} %rows.8) | copy-start | bytes 12582916
  2.8 9.6 %copy-start.2 = (f32[31,128]{1,0:T(8,128)S(1)}, f32[31,128]{1,0:T(8,128)}, u32[]{:S(2)}) copy-start(f32[31,128]{1,0:T(8,128)} %taps.3) | copy-start | bytes 47620
  2.8 16.7 %copy-start.1 = (bf16[1024,2048]{1,0:T(8,128)(2,1)S(1)}, bf16[1024,2048]{1,0:T(8,128)(2,1)}, u32[]{:S(2)}) copy-start(bf16[1024,2048]{1,0:T(8,128)(2,1)} %rows.9) | copy-start | bytes 12582916
  2.8 6.3 %collective-permute-start = (f32[32,128]{1,0:T(8,128)S(1)}, f32[32,128]{1,0:T(8,128)S(1)}, u32[]{:S(2)}, u32[]{:S(2)}) collective-permute-start(f32[32,128]{1,0:T(8,128)S(1)} %get-tuple-element.51), channel_id=1, source_target_pairs={{0,8},{8,16},{16,24},{24,32},{32,40},{40,48},{48,56},{56,64},{64,7... | collective-permute-start | bytes 49160 | tf_op jit(solution)/shard_map/ppermute | solution.py:414
  6.6 5.8 %collective-permute-start.1 = (f32[64,128]{1,0:T(8,128)S(1)}, f32[64,128]{1,0:T(8,128)S(1)}, u32[]{:S(2)}, u32[]{:S(2)}) collective-permute-start(f32[64,128]{1,0:T(8,128)S(1)} %get-tuple-element.52), channel_id=1, source_target_pairs={{8,0},{16,8},{24,16},{32,24},{40,32},{48,40},{56,48},{64,56},{72,6... | collective-permute-start | bytes 98312 | tf_op jit(solution)/shard_map/ppermute | solution.py:414
  9.2 13.5 %copy-start.3 = (f32[128]{0:T(128)S(1)}, f32[128]{0:T(128)}, u32[]{:S(2)}) copy-start(f32[128]{0:T(128)} %param.11) | copy-start | bytes 1540
  14.1 1.3 %collective-permute-start.2 = (f32[2,1056]{1,0:T(2,128)S(1)}, f32[2,1056]{1,0:T(2,128)S(1)}, u32[]{:S(2)}, u32[]{:S(2)}) collective-permute-start(f32[2,1056]{1,0:T(2,128)S(1)} %get-tuple-element.56), channel_id=1, source_target_pairs={{0,1},{1,0},{2,3},{3,2},{4,5},{5,4},{6,7},{7,6},{8,9},{9,8},{10,11... | collective-permute-start | bytes 25352 | tf_op jit(solution)/shard_map/ppermute | solution.py:419
  15.4 6.1 %collective-permute-start.5 = (f32[2,1056]{1,0:T(2,128)S(1)}, f32[2,1056]{1,0:T(2,128)S(1)}, u32[]{:S(2)}, u32[]{:S(2)}) collective-permute-start(f32[2,1056]{1,0:T(2,128)S(1)} %add.6.s0), channel_id=1, source_target_pairs={{0,4},{1,5},{2,6},{3,7},{4,0},{5,1},{6,2},{7,3},{8,12},{9,13},{10,... | collective-permute-start | bytes 25352 | tf_op jit(solution)/shard_map/ppermute | solution.py:419
  17.5 4.0 %collective-permute-start.4 = (f32[2,1056]{1,0:T(2,128)S(1)}, f32[2,1056]{1,0:T(2,128)S(1)}, u32[]{:S(2)}, u32[]{:S(2)}) collective-permute-start(f32[2,1056]{1,0:T(2,128)S(1)} %add.6.s0), channel_id=1, source_target_pairs={{0,6},{1,7},{2,0},{3,1},{4,2},{5,3},{6,4},{7,5},{8,14},{9,15},{10,... | collective-permute-start | bytes 25352 | tf_op jit(solution)/shard_map/ppermute | solution.py:419
  19.0 3.7 %collective-permute-start.3 = (f32[2,1056]{1,0:T(2,128)S(1)}, f32[2,1056]{1,0:T(2,128)S(1)}, u32[]{:S(2)}, u32[]{:S(2)}) collective-permute-start(f32[2,1056]{1,0:T(2,128)S(1)} %add.6.s0), channel_id=1, source_target_pairs={{0,2},{1,3},{2,4},{3,5},{4,6},{5,7},{6,0},{7,1},{8,10},{9,11},{10,... | collective-permute-start | bytes 25352 | tf_op jit(solution)/shard_map/ppermute | solution.py:419
  23.6 1.3 %collective-permute-start.6 = (f32[2,1056]{1,0:T(2,128)S(1)}, f32[2,1056]{1,0:T(2,128)S(1)}, u32[]{:S(2)}, u32[]{:S(2)}) collective-permute-start(f32[2,1056]{1,0:T(2,128)S(1)} %get-tuple-element.60), channel_id=1, source_target_pairs={{0,1},{1,0},{2,3},{3,2},{4,5},{5,4},{6,7},{7,6},{8,9},{9,8},{10,11... | collective-permute-start | bytes 25352 | tf_op jit(solution)/shard_map/ppermute | solution.py:419
  24.8 5.2 %collective-permute-start.9 = (f32[2,1056]{1,0:T(2,128)S(1)}, f32[2,1056]{1,0:T(2,128)S(1)}, u32[]{:S(2)}, u32[]{:S(2)}) collective-permute-start(f32[2,1056]{1,0:T(2,128)S(1)} %add.7.s0), channel_id=1, source_target_pairs={{0,4},{1,5},{2,6},{3,7},{4,0},{5,1},{6,2},{7,3},{8,12},{9,13},{10,... | collective-permute-start | bytes 25352 | tf_op jit(solution)/shard_map/ppermute | solution.py:419
  26.4 3.9 %collective-permute-start.8 = (f32[2,1056]{1,0:T(2,128)S(1)}, f32[2,1056]{1,0:T(2,128)S(1)}, u32[]{:S(2)}, u32[]{:S(2)}) collective-permute-start(f32[2,1056]{1,0:T(2,128)S(1)} %add.7.s0), channel_id=1, source_target_pairs={{0,6},{1,7},{2,0},{3,1},{4,2},{5,3},{6,4},{7,5},{8,14},{9,15},{10,... | collective-permute-start | bytes 25352 | tf_op jit(solution)/shard_map/ppermute | solution.py:419
  27.5 3.7 %collective-permute-start.7 = (f32[2,1056]{1,0:T(2,128)S(1)}, f32[2,1056]{1,0:T(2,128)S(1)}, u32[]{:S(2)}, u32[]{:S(2)}) collective-permute-start(f32[2,1056]{1,0:T(2,128)S(1)} %add.7.s0), channel_id=1, source_target_pairs={{0,2},{1,3},{2,4},{3,5},{4,6},{5,7},{6,0},{7,1},{8,10},{9,11},{10,... | collective-permute-start | bytes 25352 | tf_op jit(solution)/shard_map/ppermute | solution.py:419
  28.6 5.7 %collective-permute-start.11 = (bf16[1024,256]{1,0:T(8,128)(2,1)S(1)}, bf16[1024,256]{1,0:T(8,128)(2,1)S(1)}, u32[]{:S(2)}, u32[]{:S(2)}) collective-permute-start(bf16[1024,256]{1,0:T(8,128)(2,1)S(1)} %get-tuple-element.66), channel_id=1, source_target_pairs={{0,1},{1,0},{2,3},{3,2},{4,5},{5,4},{6,7},{7,6},{8,9},{9,8},{10,11... | collective-permute-start | bytes 1572872 | tf_op jit(solution)/shard_map/ppermute | solution.py:419
  34.3 2.0 %collective-permute-start.10 = (bf16[1024,256]{1,0:T(8,128)(2,1)S(1)}, bf16[1024,256]{1,0:T(8,128)(2,1)S(1)}, u32[]{:S(2)}, u32[]{:S(2)}) collective-permute-start(bf16[1024,256]{1,0:T(8,128)(2,1)S(1)} %get-tuple-element.65.slopes), channel_id=1, source_target_pairs={{0,1},{1,0},{2,3},{3,2},{4,5},{5,4},{6,7},{7,6},{8,9},{9,8},{10,11... | collective-permute-start | bytes 1572872 | tf_op jit(solution)/shard_map/ppermute | solution.py:419
  37.0 11.2 %collective-permute-start.12 = (bf16[1024,256]{1,0:T(8,128)(2,1)S(1)}, bf16[1024,256]{1,0:T(8,128)(2,1)S(1)}, u32[]{:S(2)}, u32[]{:S(2)}) collective-permute-start(bf16[1024,256]{1,0:T(8,128)(2,1)S(1)} %get-tuple-element.67), channel_id=1, source_target_pairs={{0,2},{1,7},{2,4},{3,1},{4,6},{5,3},{6,0},{7,5},{8,10},{9,15},{10,... | collective-permute-start | bytes 1572872 | tf_op jit(solution)/shard_map/ppermute | solution.py:429
  39.9 10.5 %collective-permute-start.18 = (bf16[512,128]{1,0:T(8,128)(2,1)S(1)}, bf16[512,128]{1,0:T(8,128)(2,1)S(1)}, u32[]{:S(2)}, u32[]{:S(2)}) collective-permute-start(bf16[512,128]{1,0:T(8,128)(2,1)S(1)} %get-tuple-element.76), channel_id=1, source_target_pairs={{0,16},{8,24},{16,0},{24,8},{1,17},{9,25},{17,1},{25,9},{2,18},{10... | collective-permute-start | bytes 393224 | tf_op jit(solution)/shard_map/ppermute | solution.py:434
  42.9 9.9 %collective-permute-start.19 = (bf16[512,128]{1,0:T(8,128)(2,1)S(1)}, bf16[512,128]{1,0:T(8,128)(2,1)S(1)}, u32[]{:S(2)}, u32[]{:S(2)}) collective-permute-start(bf16[512,128]{1,0:T(8,128)(2,1)S(1)} %get-tuple-element.77), channel_id=1, source_target_pairs={{0,8},{8,16},{16,24},{24,0},{1,9},{9,17},{17,25},{25,1},{2,10},{10... | collective-permute-start | bytes 393224 | tf_op jit(solution)/shard_map/ppermute | solution.py:434
  46.0 12.7 %collective-permute-start.20 = (bf16[512,128]{1,0:T(8,128)(2,1)S(1)}, bf16[512,128]{1,0:T(8,128)(2,1)S(1)}, u32[]{:S(2)}, u32[]{:S(2)}) collective-permute-start(bf16[512,128]{1,0:T(8,128)(2,1)S(1)} %get-tuple-element.78), channel_id=1, source_target_pairs={{0,24},{8,0},{16,8},{24,16},{1,25},{9,1},{17,9},{25,17},{2,26},{10... | collective-permute-start | bytes 393224 | tf_op jit(solution)/shard_map/ppermute | solution.py:434
  46.1 48.8 %collective-permute-start.14 = (bf16[1024,256]{1,0:T(8,128)(2,1)S(1)}, bf16[1024,256]{1,0:T(8,128)(2,1)S(1)}, u32[]{:S(2)}, u32[]{:S(2)}) collective-permute-start(bf16[1024,256]{1,0:T(8,128)(2,1)S(1)} %get-tuple-element.68), channel_id=1, source_target_pairs={{0,6},{1,3},{2,0},{3,5},{4,2},{5,7},{6,4},{7,1},{8,14},{9,11},{10,... | collective-permute-start | bytes 1572872 | tf_op jit(solution)/shard_map/ppermute | solution.py:429
  48.7 46.3 %collective-permute-start.13 = (bf16[1024,256]{1,0:T(8,128)(2,1)S(1)}, bf16[1024,256]{1,0:T(8,128)(2,1)S(1)}, u32[]{:S(2)}, u32[]{:S(2)}) collective-permute-start(bf16[1024,256]{1,0:T(8,128)(2,1)S(1)} %shard_map.125), channel_id=1, source_target_pairs={{0,2},{1,7},{2,4},{3,1},{4,6},{5,3},{6,0},{7,5},{8,10},{9,15},{10,... | collective-permute-start | bytes 1572872 | tf_op jit(solution)/shard_map/ppermute | solution.py:429
  50.4 11.0 %collective-permute-start.15 = (bf16[528,256]{1,0:T(8,128)(2,1)S(1)}, bf16[528,256]{1,0:T(8,128)(2,1)S(1)}, u32[]{:S(2)}, u32[]{:S(2)}) collective-permute-start(bf16[528,256]{1,0:T(8,128)(2,1)S(1)} %get-tuple-element.71), channel_id=1, source_target_pairs={{0,16},{8,24},{16,0},{24,8},{1,17},{9,25},{17,1},{25,9},{2,18},{10... | collective-permute-start | bytes 811016 | tf_op jit(solution)/shard_map/ppermute | solution.py:434
  52.8 13.9 %collective-permute-start.16 = (bf16[528,256]{1,0:T(8,128)(2,1)S(1)}, bf16[528,256]{1,0:T(8,128)(2,1)S(1)}, u32[]{:S(2)}, u32[]{:S(2)}) collective-permute-start(bf16[528,256]{1,0:T(8,128)(2,1)S(1)} %get-tuple-element.72), channel_id=1, source_target_pairs={{0,8},{8,16},{16,24},{24,0},{1,9},{9,17},{17,25},{25,1},{2,10},{10... | collective-permute-start | bytes 811016 | tf_op jit(solution)/shard_map/ppermute | solution.py:434
  58.7 11.5 %collective-permute-start.17 = (bf16[528,256]{1,0:T(8,128)(2,1)S(1)}, bf16[528,256]{1,0:T(8,128)(2,1)S(1)}, u32[]{:S(2)}, u32[]{:S(2)}) collective-permute-start(bf16[528,256]{1,0:T(8,128)(2,1)S(1)} %get-tuple-element.73), channel_id=1, source_target_pairs={{0,24},{8,0},{16,8},{24,16},{1,25},{9,1},{17,9},{25,17},{2,26},{10... | collective-permute-start | bytes 811016 | tf_op jit(solution)/shard_map/ppermute | solution.py:434
  70.5 11.4 %collective-permute-start.21 = (bf16[224,128]{1,0:T(8,128)(2,1)S(1)}, bf16[224,128]{1,0:T(8,128)(2,1)S(1)}, u32[]{:S(2)}, u32[]{:S(2)}) collective-permute-start(bf16[224,128]{1,0:T(8,128)(2,1)S(1)} %get-tuple-element.80), channel_id=1, source_target_pairs={{0,128},{32,160},{64,192},{96,224},{128,0},{160,32},{192,64},{224,... | collective-permute-start | bytes 172040 | tf_op jit(solution)/shard_map/ppermute | solution.py:434
  76.9 9.2 %collective-permute-start.22 = (bf16[224,128]{1,0:T(8,128)(2,1)S(1)}, bf16[224,128]{1,0:T(8,128)(2,1)S(1)}, u32[]{:S(2)}, u32[]{:S(2)}) collective-permute-start(bf16[224,128]{1,0:T(8,128)(2,1)S(1)} %get-tuple-element.81), channel_id=1, source_target_pairs={{0,96},{32,128},{64,160},{96,192},{128,224},{160,0},{192,32},{224,... | collective-permute-start | bytes 172040 | tf_op jit(solution)/shard_map/ppermute | solution.py:434
  77.8 9.9 %collective-permute-start.23 = (bf16[224,128]{1,0:T(8,128)(2,1)S(1)}, bf16[224,128]{1,0:T(8,128)(2,1)S(1)}, u32[]{:S(2)}, u32[]{:S(2)}) collective-permute-start(bf16[224,128]{1,0:T(8,128)(2,1)S(1)} %get-tuple-element.82), channel_id=1, source_target_pairs={{0,160},{32,192},{64,224},{96,0},{128,32},{160,64},{192,96},{224,1... | collective-permute-start | bytes 172040 | tf_op jit(solution)/shard_map/ppermute | solution.py:434
  82.0 8.2 %collective-permute-start.24 = (bf16[224,128]{1,0:T(8,128)(2,1)S(1)}, bf16[224,128]{1,0:T(8,128)(2,1)S(1)}, u32[]{:S(2)}, u32[]{:S(2)}) collective-permute-start(bf16[224,128]{1,0:T(8,128)(2,1)S(1)} %get-tuple-element.83), channel_id=1, source_target_pairs={{0,64},{32,96},{64,128},{96,160},{128,192},{160,224},{192,0},{224,... | collective-permute-start | bytes 172040 | tf_op jit(solution)/shard_map/ppermute | solution.py:434
  86.1 5.7 %collective-permute-start.25 = (bf16[224,128]{1,0:T(8,128)(2,1)S(1)}, bf16[224,128]{1,0:T(8,128)(2,1)S(1)}, u32[]{:S(2)}, u32[]{:S(2)}) collective-permute-start(bf16[224,128]{1,0:T(8,128)(2,1)S(1)} %get-tuple-element.84), channel_id=1, source_target_pairs={{0,192},{32,224},{64,0},{96,32},{128,64},{160,96},{192,128},{224,1... | collective-permute-start | bytes 172040 | tf_op jit(solution)/shard_map/ppermute | solution.py:434
  87.7 5.4 %collective-permute-start.26 = (bf16[224,128]{1,0:T(8,128)(2,1)S(1)}, bf16[224,128]{1,0:T(8,128)(2,1)S(1)}, u32[]{:S(2)}, u32[]{:S(2)}) collective-permute-start(bf16[224,128]{1,0:T(8,128)(2,1)S(1)} %get-tuple-element.85), channel_id=1, source_target_pairs={{0,32},{32,64},{64,96},{96,128},{128,160},{160,192},{192,224},{224... | collective-permute-start | bytes 172040 | tf_op jit(solution)/shard_map/ppermute | solution.py:434
  90.1 4.2 %collective-permute-start.27 = (bf16[224,128]{1,0:T(8,128)(2,1)S(1)}, bf16[224,128]{1,0:T(8,128)(2,1)S(1)}, u32[]{:S(2)}, u32[]{:S(2)}) collective-permute-start(bf16[224,128]{1,0:T(8,128)(2,1)S(1)} %get-tuple-element.86), channel_id=1, source_target_pairs={{0,224},{32,0},{64,32},{96,64},{128,96},{160,128},{192,160},{224,1... | collective-permute-start | bytes 172040 | tf_op jit(solution)/shard_map/ppermute | solution.py:434

commit v2 on v1

--- a/solution.py
+++ b/solution.py
@@ -19,8 +19,10 @@
 EXT = ROWS + PAD
 TAIL = 16
 BLOCK = D // 8
-PART = D // NY
+SLOTS = NZ // NC
+PART = D // (NY * NC)
 CUT = D // (NY * NZ)
+PIECE = 3 * CUT + 2 * TAIL
 FLOOR = 0.1
 F32 = jnp.float32
 BF16 = jnp.bfloat16
@@ -166,38 +168,67 @@
     return total
 
 
-def conv_kernel(mixed, prior, after, taps, history, conv, sums):
-    history[:PAD] = prior[...]
-    history[PAD : PAD + ROWS] = mixed[...]
-    history[PAD + ROWS :] = after[:PAD]
-    step = 96
+def conv_kernel(mixed, taps, conv, sums, history):
+    history[:PAD] = jnp.zeros((PAD, W), F32)
+    history[PAD:] = mixed[...]
+    step = 128
 
     def body(i, carry):
         base = pl.multiple_of(i * step, step)
         conv[pl.ds(base, step), :] = swept(history, taps, base, step, lambda k: PAD - k)
         return carry
 
-    lax.fori_loop(0, EXT // step, body, 0)
+    lax.fori_loop(0, ROWS // step, body, 0)
     value = conv[...]
     store_sums(sums, value, value * value)
 
 
-def conv_of(mixed, prior, after, taps):
+def conv_of(mixed, taps):
     return pl.pallas_call(
         conv_kernel,
-        out_shape=[shape_of((EXT + PAD, W)), shape_of((EXT, W)), shape_of((2, EXT))],
+        out_shape=[shape_of((ROWS, W)), shape_of((2, ROWS))],
+        scratch_shapes=[pltpu.VMEM((PAD + ROWS, W), F32)],
         compiler_params=params(12),
         cost_estimate=cost(2 * ROWS * D * 128, 2 * 1024 * 1024),
-    )(mixed, prior, after, taps)
+    )(mixed, taps)
+
+
+def edge_conv_kernel(mixed, prior, after, taps, main_sums, edge, sums, low, high):
+    low[:PAD] = prior[...]
+    low[PAD:] = mixed[:PAD]
+    high[:PAD] = mixed[ROWS - PAD :]
+    high[PAD:] = after[:PAD]
+    edge[:PAD] = swept(low, taps, 0, PAD, lambda k: PAD - k)
+    edge[PAD:] = swept(high, taps, 0, PAD, lambda k: PAD - k)
+    value = edge[...]
+    sums[:, PAD:ROWS] = main_sums[:, PAD:]
+    for row, term in enumerate((value, value * value)):
+        ends = jnp.sum(term, axis=1)[None]
+        sums[row : row + 1, :PAD] = ends[:, :PAD]
+        sums[row : row + 1, ROWS:] = ends[:, PAD:]
+
+
+def edge_conv_of(mixed, prior, after, taps, main_sums):
+    return pl.pallas_call(
+        edge_conv_kernel,
+        out_shape=[shape_of((2 * PAD, W)), shape_of((2, EXT))],
+        scratch_shapes=[pltpu.VMEM((2 * PAD, W), F32)] * 2,
+        compiler_params=params(8),
+        cost_estimate=cost(2 * ROWS * D * 16, 1024 * 1024),
+    )(mixed, prior, after, taps, main_sums)
 
 
 def norm_kernel(
-    conv, slope, after, gain, s0, s1, s2, s3, normed, norm_slope, inverse, activated, back, gain_part, centers, squares
+    main, edge, slope, after, gain, s0, s1, s2, s3, normed, norm_slope, inverse, activated, back, gain_part,
+    centers, squares,
 ):
+    normed[:PAD] = edge[:PAD]
+    normed[PAD:ROWS] = main[PAD:]
+    normed[ROWS:] = edge[PAD:]
     spread_sums((s0, s1, s2, s3), (centers, squares))
     center = centers[...]
     inv = lax.rsqrt(squares[...] - center * center + FLOOR)
-    norm = (conv[...] - center) * inv
+    norm = (normed[...] - center) * inv
     inverse[...] = inv
     normed[...] = norm
     scale = gain[...]
@@ -215,7 +246,7 @@
     store_sums(back, value, value * norm)
 
 
-def norm_of(conv, slope, after, gain, sums):
+def norm_of(main, edge, slope, after, gain, sums):
     ext = shape_of((EXT, W))
     return pl.pallas_call(
         norm_kernel,
@@ -223,13 +254,15 @@
         scratch_shapes=[pltpu.VMEM((EXT, W), F32)] * 2,
         compiler_params=params(16),
         cost_estimate=cost(2 * ROWS * D * 128, 2 * 1024 * 1024),
-    )(conv, slope, after, gain, *sums)
+    )(main, edge, slope, after, gain, *sums)
 
 
 def adjoint_kernel(
-    normed, norm_slope, inverse, s0, s1, s2, s3, history, taps, sgate, factor, gain_part,
-    slopes, taps_part, curve, means, crosses,
+    normed, norm_slope, inverse, s0, s1, s2, s3, mixed, prior, taps, sgate, factor, gain_part,
+    slopes, curve, means, crosses, history, taps_part,
 ):
+    history[:PAD] = prior[...]
+    history[PAD:] = mixed[...]
     spread_sums((s0, s1, s2, s3), (means, crosses))
     curve[...] = inverse[...] * (norm_slope[...] - means[...] - normed[...] * crosses[...])
 
@@ -267,62 +300,90 @@
     for k in range(K):
         taps_part[k : k + 1, :] = jnp.sum(sums[k], axis=0, keepdims=True)
     taps_part[K:, :] = gain_part[...]
-
-
-def adjoint_of(normed, norm_slope, inverse, back, history, taps, sgate, factor, gain_part):
+    small = taps_part[...].astype(BF16)
+    slopes[ROWS:, :W] = small[:TAIL]
+    slopes[ROWS:, W:] = small[TAIL:]
+
+
+def adjoint_of(normed, norm_slope, inverse, back, mixed, prior, taps, sgate, factor, gain_part):
     return pl.pallas_call(
         adjoint_kernel,
-        out_shape=[shape_of((ROWS, 2 * W), BF16), shape_of((K + 1, W))],
-        scratch_shapes=[pltpu.VMEM((EXT, W), F32)] * 3,
+        out_shape=shape_of((ROWS + TAIL, 2 * W), BF16),
+        scratch_shapes=[pltpu.VMEM((EXT, W), F32)] * 4 + [pltpu.VMEM((K + 1, W), F32)],
         compiler_params=params(16),
         cost_estimate=cost(2 * ROWS * D * 256, 2 * 1024 * 1024),
-    )(normed, norm_slope, inverse, *back, history, taps, sgate, factor, gain_part)
-
-
-def across(rows, side, parts):
+    )(normed, norm_slope, inverse, *back, mixed, prior, taps, sgate, factor, gain_part)
+
+
+def kept_by(slot):
+    core = lax.axis_index("c")
+    by = 4 * (1 - core) if slot == 0 else slot * (1 - 2 * core) + NZ
+    return lax.rem(lax.axis_index("z") + by, NZ)
+
+
+def across(rows, side, parts, lanes):
     step = D // NZ
-    for z in range(NZ):
+    for slot in range(SLOTS):
+        at = pl.multiple_of(kept_by(slot) * step, step)
         part = lax.dot_general(
-            rows[:, z * step : (z + 1) * step], side, (((0,), (0,)), ((), ())), preferred_element_type=F32
+            rows[:, pl.ds(at, step)], side, (((0,), (0,)), ((), ())), preferred_element_type=F32
         )
-        parts[:, z * CUT : (z + 1) * CUT, :] = part.astype(BF16).reshape(NY, CUT, side.shape[1])
-
-
-def out_grad_kernel(rows, activated, *rest):
+        parts[:, slot * CUT : (slot + 1) * CUT, lanes] = part.astype(BF16).reshape(NY, CUT, side.shape[1])
+
+
+def along_y(by):
+    return lax.rem(lax.axis_index("y") + by, NY)
+
+
+def out_grad_kernel(rows, activated, other, *rest):
     outs, parts = rest[:NY], rest[NY]
-    across(rows, activated[...], parts)
+    across(rows, activated[...], parts, slice(0, W))
+    across(rows, other[...], parts, slice(W, 2 * W))
     for by, out in enumerate(outs):
-        out[...] = parts[lax.rem(lax.axis_index("y") + by, NY)]
-
-
-def out_grad_of(grad_output, activated):
+        out[...] = parts[along_y(by)]
+
+
+def out_grad_of(grad_output, activated, other):
     return pl.pallas_call(
         out_grad_kernel,
-        out_shape=[shape_of((PART, W), BF16)] * NY,
-        scratch_shapes=[pltpu.VMEM((NY, PART, W), BF16)],
+        out_shape=[shape_of((PART, 2 * W), BF16)] * NY,
+        scratch_shapes=[pltpu.VMEM((NY, PART, 2 * W), BF16)],
         compiler_params=params(8),
         cost_estimate=cost(2 * ROWS * D * 256, 5 * 1024 * 1024),
-    )(grad_output, activated)
-
-
-def weight_grad_kernel(rows, slopes, taps_part, *rest):
+    )(grad_output, activated, other)
+
+
+def own_weight_grad_kernel(rows, slopes, parts):
+    across(rows, slopes[:ROWS], parts, slice(0, 2 * W))
+
+
+def own_weight_grad_of(block_input, slopes):
+    return pl.pallas_call(
+        own_weight_grad_kernel,
+        out_shape=shape_of((NY, PART, 2 * W), BF16),
+        compiler_params=params(8),
+        cost_estimate=cost(2 * ROWS * D * 128, 3 * 1024 * 1024),
+    )(block_input, slopes)
+
+
+def weight_grad_kernel(rows, slopes, others, own, *rest):
     outs, parts = rest[:NY], rest[NY]
-    across(rows, slopes[...], parts)
-    small = taps_part[...].astype(BF16)
-    small = jnp.concatenate([small[:TAIL], small[TAIL:]], axis=1)
+    across(rows, others[:ROWS], parts, slice(0, 2 * W))
     for by, out in enumerate(outs):
-        out[:PART] = parts[lax.rem(lax.axis_index("y") + by, NY)]
-        out[PART:] = small
-
-
-def weight_grad_of(block_input, slopes, taps_part):
+        out[:PART, : 2 * W] = own[along_y(by)]
+        out[:PART, 2 * W :] = parts[along_y(by)]
+        out[PART:, : 2 * W] = slopes[ROWS:]
+        out[PART:, 2 * W :] = others[ROWS:]
+
+
+def weight_grad_of(block_input, slopes, others, own):
     return pl.pallas_call(
         weight_grad_kernel,
-        out_shape=[shape_of((PART + TAIL, 2 * W), BF16)] * NY,
+        out_shape=[shape_of((PART + TAIL, 4 * W), BF16)] * NY,
         scratch_shapes=[pltpu.VMEM((NY, PART, 2 * W), BF16)],
         compiler_params=params(12),
-        cost_estimate=cost(2 * ROWS * D * 256, 7 * 1024 * 1024),
-    )(block_input, slopes, taps_part)
+        cost_estimate=cost(2 * ROWS * D * 128, 5 * 1024 * 1024),
+    )(block_input, slopes, others, own)
 
 
 def summed(parts):
@@ -333,30 +394,47 @@
 
 
 def middle_kernel(*refs):
-    both, side, outs, parts = refs[:NY], refs[NY : 2 * NY], refs[2 * NY : 2 * NY + NZ], refs[2 * NY + NZ]
+    both, side, outs = refs[:NY], refs[NY : 2 * NY], refs[2 * NY :]
     total = summed(both).astype(BF16)
-    parts[:, :CUT, :] = total[:PART, :W].reshape(NZ, CUT, W)
-    parts[:, CUT : 2 * CUT, :] = total[:PART, W:].reshape(NZ, CUT, W)
-    parts[:, 2 * CUT :, :] = summed(side).astype(BF16).reshape(NZ, CUT, W)
-    for by, out in enumerate(outs):
-        out[: 3 * CUT] = parts[lax.rem(lax.axis_index("z") + by, NZ)]
-        out[3 * CUT : 3 * CUT + TAIL] = total[PART:, :W]
-        out[3 * CUT + TAIL :] = total[PART:, W:]
+    outer = summed(side).astype(BF16)
+    for slot, out in enumerate(outs):
+        rows = slice(slot * CUT, (slot + 1) * CUT)
+        for core in range(NC):
+            at, lane = core * PIECE, core * 2 * W
+            out[at : at + CUT] = total[rows, lane : lane + W]
+            out[at + CUT : at + 2 * CUT] = total[rows, lane + W : lane + 2 * W]
+            out[at + 2 * CUT : at + 3 * CUT] = outer[rows, core * W : (core + 1) * W]
+            out[at + 3 * CUT : at + 3 * CUT + TAIL] = total[PART:, lane : lane + W]
+            out[at + 3 * CUT + TAIL : at + PIECE] = total[PART:, lane + W : lane + 2 * W]
 
 
 def middle_of(both, side):
     return pl.pallas_call(
         middle_kernel,
-        out_shape=[shape_of((3 * CUT + 2 * TAIL, W), BF16)] * NZ,
-        scratch_shapes=[pltpu.VMEM((NZ, 3 * CUT, W), BF16)],
+        out_shape=[shape_of((NC * PIECE, W), BF16)] * SLOTS,
         compiler_params=params(12),
         cost_estimate=cost(2 * ROWS * D, 2 * 1024 * 1024),
     )(*both, *side)
 
 
-def final_kernel(*refs):
-    parts, (value_grad, gate_grad, out_grad, taps_grad, gain_grad) = refs[:NZ], refs[NZ:]
-    total = summed(parts)
+def chip_kernel(mine, opposite, one, two, three, own, other):
+    first = jnp.where(lax.axis_index("c") == 0, opposite[...].astype(F32), mine[...].astype(F32))
+    total = first + summed((one, two, three))
+    own[...] = total[:PIECE]
+    other[...] = total[PIECE:]
+
+
+def chip_of(mine, parts):
+    return pl.pallas_call(
+        chip_kernel,
+        out_shape=[shape_of((PIECE, W))] * 2,
+        compiler_params=params(8),
+        cost_estimate=cost(2 * ROWS * D, 1024 * 1024),
+    )(mine, *parts)
+
+
+def final_kernel(own, other, value_grad, gate_grad, out_grad, taps_grad, gain_grad):
+    total = own[...] + other[...]
     value_grad[...] = total[:CUT]
     gate_grad[...] = total[CUT : 2 * CUT]
     out_grad[...] = total[2 * CUT : 3 * CUT]
@@ -364,14 +442,14 @@
     gain_grad[...] = total[3 * CUT + K :]
 
 
-def final_of(parts):
+def final_of(own, other):
     part = shape_of((CUT, W))
     return pl.pallas_call(
         final_kernel,
         out_shape=[part, part, part, shape_of((K, W)), shape_of((1, W))],
-        compiler_params=params(12),
+        compiler_params=params(8),
         cost_estimate=cost(2 * ROWS * D, 1024 * 1024),
-    )(*parts)
+    )(own, other)
 
 
 def share(by, slopes, others, both, lent):
@@ -381,8 +459,8 @@
     mine = both[pl.ds(pl.multiple_of((chip * NC + core) * BLOCK, BLOCK), BLOCK), :]
     theirs = lent[pl.ds(pl.multiple_of(chip * BLOCK, BLOCK), BLOCK), :]
     contract = (((1,), (1,)), ((), ()))
-    total = lax.dot_general(slopes[...], mine, contract, preferred_element_type=F32)
-    return total + lax.dot_general(others[...], theirs, contract, preferred_element_type=F32)
+    total = lax.dot_general(slopes[:ROWS], mine, contract, preferred_element_type=F32)
+    return total + lax.dot_general(others[:ROWS], theirs, contract, preferred_element_type=F32)
 
 
 def far_kernel(slopes, others, both, lent, far, back):
@@ -421,7 +499,7 @@
 
 def chip_sums(own):
     pair = own + to_slot(own, 1)
-    return [pair, to_slot(pair, 2), to_slot(pair, 6), to_slot(pair, 4)]
+    return [pair] + [to_slot(pair, slot) for slot in (2, 6, 4)]
 
 
 def along(value, by):
@@ -436,6 +514,16 @@
 
 def spread(parts, axis, order):
     return [parts[0]] + [further(parts[by], axis, by) for by in order]
+
+
+def to_keeper(value, slot):
+    if slot == 0:
+        pairs = [(z * NC, (z + 4) % NZ * NC) for z in range(NZ)]
+    else:
+        pairs = [
+            (z * NC + c, (z + (slot if c == 0 else -slot)) % NZ * NC + c) for z in range(NZ) for c in range(NC)
+        ]
+    return lax.ppermute(value, ("z", "c"), pairs)
 
 
 def shards(block_input, value_proj, gate_proj, conv_taps, norm_gain, out_proj, grad_output):
@@ -443,18 +531,23 @@
     prior = from_behind(to_next, 1)
     after = from_behind(to_prior, -1)
     mixed, sgate, factor = glu(block_input, both)
-    history, conv, sums = conv_of(mixed, prior, after, conv_taps)
+    conv, sums = conv_of(mixed, conv_taps)
+    edge, sums = edge_conv_of(mixed, prior, after, conv_taps, sums)
     sums = chip_sums(sums)
     slope, lend = slopes_of(grad_output, out_side, both)
     normed, norm_slope, inverse, activated, back, gain_part = norm_of(
-        conv, slope, after, norm_gain.reshape(1, W), sums
+        conv, edge, slope, after, norm_gain.reshape(1, W), sums
     )
     back = chip_sums(back)
-    out_parts = out_grad_of(grad_output, activated)
+    other_activated = to_slot(activated, 1)
+    out_parts = out_grad_of(grad_output, activated, other_activated)
     out_parts = spread(out_parts, "y", Y_ORDER)
-    slopes, taps_part = adjoint_of(normed, norm_slope, inverse, back, history, conv_taps, sgate, factor, gain_part)
+    slopes = adjoint_of(
+        normed, norm_slope, inverse, back, mixed, prior, conv_taps, sgate, factor, gain_part
+    )
     others = to_slot(slopes, 1)
-    both_parts = weight_grad_of(block_input, slopes, taps_part)
+    own_parts = own_weight_grad_of(block_input, slopes)
+    both_parts = weight_grad_of(block_input, slopes, others, own_parts)
     both_parts = spread(both_parts, "y", Y_ORDER)
     lent = to_slot(lend, 1)
     sides = (slopes, others, both, lent)
@@ -464,14 +557,16 @@
     near = along(near, 1)
     single = along(single, -1)
     parts = middle_of(both_parts, out_parts)
-    parts = spread(parts, "z", Z_ORDER)
+    sent = {slot: to_keeper(parts[slot], slot) for slot in Z_ORDER}
+    own, other = chip_of(parts[0], [sent[slot] for slot in range(SLOTS)])
+    other = to_slot(other, 1)
     (input_grad,) = share_call(own_kernel, 1, 1, *sides, near, single)
-    value_grad, gate_grad, out_grad, taps_grad, gain_grad = final_of(parts)
+    value_grad, gate_grad, out_grad, taps_grad, gain_grad = final_of(own, other)
     return (input_grad, value_grad, gate_grad, out_grad, taps_grad, gain_grad.reshape(W))
 
 
 Y_ORDER = (2, 1, 3)
-Z_ORDER = (4, 3, 5, 2, 6, 1, 7)
+Z_ORDER = (0, 3, 2, 1)
 
 
 def solution(mesh):

time: 96.4 us -> 91.6 us (0.950); the launches traced: 96.3 us -> 89.8 us
  waiting for transfers between devices: 28.6 us -> 24.4 us
  starting transfers between devices: 49.1 us -> 46.3 us
    ppermute x13 -> x6, starting transfers between devices: 32.2 us -> 11.6 us  [further(): lax.ppermute(value, axis, [(i, (i + by) % count) for i in range(count)])]
    ppermute x0 -> x4, starting transfers between devices: none -> 15.6 us  [to_keeper(): return lax.ppermute(value, ('z', 'c'), pairs)]
    ppermute x13 -> x6, waiting for transfers between devices: 17.5 us -> 8.58 us  [further(): lax.ppermute(value, axis, [(i, (i + by) % count) for i in range(count)])]
    ppermute x0 -> x4, waiting for transfers between devices: none -> 3.76 us  [to_keeper(): return lax.ppermute(value, ('z', 'c'), pairs)]
    ppermute x10 -> x12, waiting for transfers between devices: 7.83 us -> 10.6 us  [to_slot(): return lax.ppermute(value, TP, pairs)]
    ppermute x10 -> x12, starting transfers between devices: 8.25 us -> 10.8 us  [to_slot(): return lax.ppermute(value, TP, pairs)]
    ppermute x2, waiting for transfers between devices: 3.21 us -> 1.51 us  [from_behind(): lax.ppermute(value, SP, [(i, i + by) for i in range(count) if 0 <= i + by...]
    pallas_call x5 -> x8, Pallas kernels: 8.25 us -> 8.65 us  [the longest x1 3.21 us: adjoint_of(): pl.pallas_call(adjoint_kernel, out_shape=shape_of((ROWS + TAIL, 2 * W), B...]
  transfers between devices with their start and end apart: 28 -> 27, of which waited for: 15 -> 14; matrix products, arithmetic and copies ran while one was open for 0% -> 0% of each run, Pallas kernels for 11% -> 11%
where the time goes in v2:
time: 91.6 us; the launch traced here: 89.8 us
  starting transfers between devices  46.3 us (51%)
  waiting for transfers between devices  24.4 us (27%)
  Pallas kernels  18.1 us (20%)
    ppermute x4, starting transfers between devices, to_keeper(): return lax.ppermute(value, ('z', 'c'), pairs)  15.6 us
    ppermute x6, starting transfers between devices, further(): lax.ppermute(value, axis, [(i, (i + by) % count) for i in range(count)])  11.6 us
    ppermute x12, starting transfers between devices, to_slot(): return lax.ppermute(value, TP, pairs)  10.8 us
    ppermute x12, waiting for transfers between devices, to_slot(): return lax.ppermute(value, TP, pairs)  10.6 us
    ppermute x6, waiting for transfers between devices, further(): lax.ppermute(value, axis, [(i, (i + by) % count) for i in range(count)])  8.58 us
    ppermute x2, starting transfers between devices, from_behind(): lax.ppermute(value, SP, [(i, i + by) for i in range(count) if 0 <= i + by...  5.04 us
    ppermute x4, waiting for transfers between devices, to_keeper(): return lax.ppermute(value, ('z', 'c'), pairs)  3.76 us
    ppermute x3, starting transfers between devices, along(): return lax.ppermute(value, TP, pairs)  3.33 us
  transfers between devices with their start and end apart: 27, of which 14 were waited for; matrix products, arithmetic and copies ran while one was open for 0% of the time, Pallas kernels for 11%

profile of v2, /device:TPU:2, one launch (start us, length us, event | category | flops | bytes accessed | tf_op | source)
XLA Modules:
  0.0 89.8 jit_solution(9186470312869307908)
XLA Ops:
  0.6 2.2 %shard_map.118 = (f32[32,128]{1,0:T(8,128)S(1)}, f32[64,128]{1,0:T(8,128)S(1)}, bf16[2048,256]{1,0:T(8,128)(2,1)S(1)}, bf16[2048,128]{1,0:T(8,128)(2,1)S(1)}) custom-call(bf16[1024,2048]{1,0:T(8,128)(2,1)} %rows.10, bf16[1024,2048]{1,0:T(8,128)(2,1)} %rows.11, bf16[2048,128]{1,0:T(8,128)(2,1)} %value_proj.1, bf16[2048,128]{1,0:T(8,128)(2,1)} %gate_proj.1, ...), custom_call_target="tpu_custom_call" | custom-call | flops 100663296 | bytes 2097152 | tf_op jit(solution)/shard_map/pallas_call | solution.py:80
  2.8 3.7 %collective-permute-start = (f32[32,128]{1,0:T(8,128)S(1)}, f32[32,128]{1,0:T(8,128)S(1)}, u32[]{:S(2)}, u32[]{:S(2)}) collective-permute-start(f32[32,128]{1,0:T(8,128)S(1)} %get-tuple-element.49), channel_id=1, source_target_pairs={{0,8},{8,16},{16,24},{24,32},{32,40},{40,48},{48,56},{56,64},{64,7... | collective-permute-start | bytes 49160 | tf_op jit(solution)/shard_map/ppermute | solution.py:492
  6.6 1.3 %collective-permute-start.1 = (f32[64,128]{1,0:T(8,128)S(1)}, f32[64,128]{1,0:T(8,128)S(1)}, u32[]{:S(2)}, u32[]{:S(2)}) collective-permute-start(f32[64,128]{1,0:T(8,128)S(1)} %get-tuple-element.50), channel_id=1, source_target_pairs={{8,0},{16,8},{24,16},{32,24},{40,32},{48,40},{56,48},{64,56},{72,6... | collective-permute-start | bytes 98312 | tf_op jit(solution)/shard_map/ppermute | solution.py:492
  7.9 1.3 %shard_map.119 = (f32[1024,128]{1,0:T(8,128)S(1)}, f32[1024,128]{1,0:T(8,128)S(1)}, f32[1024,128]{1,0:T(8,128)S(1)}) custom-call(bf16[1024,2048]{1,0:T(8,128)(2,1)S(1)} %copy-done, bf16[2048,256]{1,0:T(8,128)(2,1)S(1)} %get-tuple-element.46.both), custom_call_target="tpu_custom_call" | custom-call | flops 1073741824 | bytes 7340032 | tf_op jit(solution)/shard_map/pallas_call | solution.py:107
  9.2 1.7 %shard_map.120 = (f32[1024,128]{1,0:T(8,128)S(1)}, f32[2,1024]{1,0:T(2,128)S(1)}) custom-call(f32[1024,128]{1,0:T(8,128)S(1)} %get-tuple-element.47.mixed, f32[31,128]{1,0:T(8,128)S(1)} %copy-done.2), custom_call_target="tpu_custom_call" | custom-call | flops 536870912 | bytes 2097152 | tf_op jit(solution)/shard_map/pallas_call | solution.py:187
  10.9 1.5 %collective-permute-done.1.after = f32[64,128]{1,0:T(8,128)S(1)} collective-permute-done((f32[64,128]{1,0:T(8,128)S(1)}, f32[64,128]{1,0:T(8,128)S(1)}, u32[]{:S(2)}, u32[]{:S(2)}) %collective-permute-start.1) | collective-permute-done | bytes 32800 | tf_op jit(solution)/shard_map/ppermute | solution.py:492
  12.7 1.2 %collective-permute-done.2 = f32[2,1056]{1,0:T(2,128)S(1)} collective-permute-done((f32[2,1056]{1,0:T(2,128)S(1)}, f32[2,1056]{1,0:T(2,128)S(1)}, u32[]{:S(2)}, u32[]{:S(2)}) %collective-permute-start.2) | collective-permute-done | bytes 8480 | tf_op jit(solution)/shard_map/ppermute | solution.py:497
  13.9 2.1 %collective-permute-start.5 = (f32[2,1056]{1,0:T(2,128)S(1)}, f32[2,1056]{1,0:T(2,128)S(1)}, u32[]{:S(2)}, u32[]{:S(2)}) collective-permute-start(f32[2,1056]{1,0:T(2,128)S(1)} %add.6.s0), channel_id=1, source_target_pairs={{0,4},{1,5},{2,6},{3,7},{4,0},{5,1},{6,2},{7,3},{8,12},{9,13},{10,... | collective-permute-start | bytes 25352 | tf_op jit(solution)/shard_map/ppermute | solution.py:497
  16.0 1.4 %collective-permute-start.4 = (f32[2,1056]{1,0:T(2,128)S(1)}, f32[2,1056]{1,0:T(2,128)S(1)}, u32[]{:S(2)}, u32[]{:S(2)}) collective-permute-start(f32[2,1056]{1,0:T(2,128)S(1)} %add.6.s0), channel_id=1, source_target_pairs={{0,6},{1,7},{2,0},{3,1},{4,2},{5,3},{6,4},{7,5},{8,14},{9,15},{10,... | collective-permute-start | bytes 25352 | tf_op jit(solution)/shard_map/ppermute | solution.py:497
  18.0 1.9 %shard_map.122 = (f32[1024,128]{1,0:T(8,128)S(1)}, bf16[1024,256]{1,0:T(8,128)(2,1)S(1)}) custom-call(bf16[1024,2048]{1,0:T(8,128)(2,1)S(1)} %copy-done.1, bf16[2048,128]{1,0:T(8,128)(2,1)S(1)} %get-tuple-element.53.out_side, bf16[2048,256]{1,0:T(8,128)(2,1)S(1)} %get-tuple-element.46.both), custom_call_target="tpu_custom_call" | custom-call | flops 1073741824 | bytes 5242880 | tf_op jit(solution)/shard_map/pallas_call | solution.py:133
  22.1 1.2 %collective-permute-done.6 = f32[2,1056]{1,0:T(2,128)S(1)} collective-permute-done((f32[2,1056]{1,0:T(2,128)S(1)}, f32[2,1056]{1,0:T(2,128)S(1)}, u32[]{:S(2)}, u32[]{:S(2)}) %collective-permute-start.6) | collective-permute-done | bytes 8480 | tf_op jit(solution)/shard_map/ppermute | solution.py:497
  23.3 1.5 %collective-permute-start.9 = (f32[2,1056]{1,0:T(2,128)S(1)}, f32[2,1056]{1,0:T(2,128)S(1)}, u32[]{:S(2)}, u32[]{:S(2)}) collective-permute-start(f32[2,1056]{1,0:T(2,128)S(1)} %add.7.s0), channel_id=1, source_target_pairs={{0,4},{1,5},{2,6},{3,7},{4,0},{5,1},{6,2},{7,3},{8,12},{9,13},{10,... | collective-permute-start | bytes 25352 | tf_op jit(solution)/shard_map/ppermute | solution.py:497
  27.1 1.3 %collective-permute-done.9.s3 = f32[2,1056]{1,0:T(2,128)S(1)} collective-permute-done((f32[2,1056]{1,0:T(2,128)S(1)}, f32[2,1056]{1,0:T(2,128)S(1)}, u32[]{:S(2)}, u32[]{:S(2)}) %collective-permute-start.9) | collective-permute-done | bytes 8480 | tf_op jit(solution)/shard_map/ppermute | solution.py:497
  29.6 3.2 %shard_map.124.slopes = bf16[1040,256]{1,0:T(8,128)(2,1)S(1)} custom-call(f32[1056,128]{1,0:T(8,128)S(1)} %get-tuple-element.56.normed, f32[1056,128]{1,0:T(8,128)S(1)} %get-tuple-element.57.norm_slope, f32[1056,128]{1,0:T(8,128)S(1)} %get-tuple-element.58.inverse, f32[2,1056]{1,0:T(2,128)S(1)} %add.7.s0, f32[2,1056]{1,0:T(2,128)S(1)} %collective-permute-done.7.s1, ...), custom_call_target="tpu_custom_call" | custom-call | flops 1073741824 | bytes 2097152 | tf_op jit(solution)/shard_map/pallas_call | solution.py:309
  33.4 2.2 %collective-permute-done.11.lent = bf16[1024,256]{1,0:T(8,128)(2,1)S(1)} collective-permute-done((bf16[1024,256]{1,0:T(8,128)(2,1)S(1)}, bf16[1024,256]{1,0:T(8,128)(2,1)S(1)}, u32[]{:S(2)}, u32[]{:S(2)}) %collective-permute-start.11) | collective-permute-done | bytes 524320 | tf_op jit(solution)/shard_map/ppermute | solution.py:497
  36.3 1.2 %collective-permute-start.12 = (bf16[1024,256]{1,0:T(8,128)(2,1)S(1)}, bf16[1024,256]{1,0:T(8,128)(2,1)S(1)}, u32[]{:S(2)}, u32[]{:S(2)}) collective-permute-start(bf16[1024,256]{1,0:T(8,128)(2,1)S(1)} %get-tuple-element.64), channel_id=1, source_target_pairs={{0,2},{1,7},{2,4},{3,1},{4,6},{5,3},{6,0},{7,5},{8,10},{9,15},{10,... | collective-permute-start | bytes 1572872 | tf_op jit(solution)/shard_map/ppermute | solution.py:507
  37.6 1.9 %collective-permute-start.18 = (bf16[1024,128]{1,0:T(8,128)(2,1)S(1)}, bf16[1024,128]{1,0:T(8,128)(2,1)S(1)}, u32[]{:S(2)}, u32[]{:S(2)}) collective-permute-start(bf16[1024,128]{1,0:T(8,128)(2,1)S(1)} %get-tuple-element.70.activated), channel_id=1, source_target_pairs={{0,1},{1,0},{2,3},{3,2},{4,5},{5,4},{6,7},{7,6},{8,9},{9,8},{10,11... | collective-permute-start | bytes 786440 | tf_op jit(solution)/shard_map/ppermute | solution.py:497
  39.5 1.2 %collective-permute-done.18.other = bf16[1024,128]{1,0:T(8,128)(2,1)S(1)} collective-permute-done((bf16[1024,128]{1,0:T(8,128)(2,1)S(1)}, bf16[1024,128]{1,0:T(8,128)(2,1)S(1)}, u32[]{:S(2)}, u32[]{:S(2)}) %collective-permute-start.18) | collective-permute-done | bytes 262176 | tf_op jit(solution)/shard_map/ppermute | solution.py:497
  40.7 1.5 %shard_map.130 = (bf16[256,256]{1,0:T(8,128)(2,1)S(1)}, bf16[256,256]{1,0:T(8,128)(2,1)S(1)}, bf16[256,256]{1,0:T(8,128)(2,1)S(1)}, bf16[256,256]{1,0:T(8,128)(2,1)S(1)}) custom-call(bf16[1024,2048]{1,0:T(8,128)(2,1)S(1)} %copy-done.1, bf16[1024,128]{1,0:T(8,128)(2,1)S(1)} %get-tuple-element.70.activated, bf16[1024,128]{1,0:T(8,128)(2,1)S(1)} %collective-permute-done.18.other), custom_call_target="tpu_custom_call" | custom-call | flops 1073741824 | bytes 5242880 | tf_op jit(solution)/shard_map/pallas_call | solution.py:347
  42.2 3.0 %collective-permute-start.19 = (bf16[256,256]{1,0:T(8,128)(2,1)S(1)}, bf16[256,256]{1,0:T(8,128)(2,1)S(1)}, u32[]{:S(2)}, u32[]{:S(2)}) collective-permute-start(bf16[256,256]{1,0:T(8,128)(2,1)S(1)} %get-tuple-element.72), channel_id=1, source_target_pairs={{0,16},{8,24},{16,0},{24,8},{1,17},{9,25},{17,1},{25,9},{2,18},{10... | collective-permute-start | bytes 393224 | tf_op jit(solution)/shard_map/ppermute | solution.py:512
  46.0 3.2 %collective-permute-start.20 = (bf16[256,256]{1,0:T(8,128)(2,1)S(1)}, bf16[256,256]{1,0:T(8,128)(2,1)S(1)}, u32[]{:S(2)}, u32[]{:S(2)}) collective-permute-start(bf16[256,256]{1,0:T(8,128)(2,1)S(1)} %get-tuple-element.73), channel_id=1, source_target_pairs={{0,8},{8,16},{16,24},{24,0},{1,9},{9,17},{17,25},{25,1},{2,10},{10... | collective-permute-start | bytes 393224 | tf_op jit(solution)/shard_map/ppermute | solution.py:512
  50.3 2.1 %collective-permute-start.15 = (bf16[272,512]{1,0:T(8,128)(2,1)S(1)}, bf16[272,512]{1,0:T(8,128)(2,1)S(1)}, u32[]{:S(2)}, u32[]{:S(2)}) collective-permute-start(bf16[272,512]{1,0:T(8,128)(2,1)S(1)} %get-tuple-element.67), channel_id=1, source_target_pairs={{0,16},{8,24},{16,0},{24,8},{1,17},{9,25},{17,1},{25,9},{2,18},{10... | collective-permute-start | bytes 835592 | tf_op jit(solution)/shard_map/ppermute | solution.py:512
  52.6 3.0 %collective-permute-start.17 = (bf16[272,512]{1,0:T(8,128)(2,1)S(1)}, bf16[272,512]{1,0:T(8,128)(2,1)S(1)}, u32[]{:S(2)}, u32[]{:S(2)}) collective-permute-start(bf16[272,512]{1,0:T(8,128)(2,1)S(1)} %get-tuple-element.69), channel_id=1, source_target_pairs={{0,24},{8,0},{16,8},{24,16},{1,25},{9,1},{17,9},{25,17},{2,26},{10... | collective-permute-start | bytes 835592 | tf_op jit(solution)/shard_map/ppermute | solution.py:512
  57.0 1.2 %collective-permute-start.13 = (bf16[1024,256]{1,0:T(8,128)(2,1)S(1)}, bf16[1024,256]{1,0:T(8,128)(2,1)S(1)}, u32[]{:S(2)}, u32[]{:S(2)}) collective-permute-start(bf16[1024,256]{1,0:T(8,128)(2,1)S(1)} %shard_map.126), channel_id=1, source_target_pairs={{0,2},{1,7},{2,4},{3,1},{4,6},{5,3},{6,0},{7,5},{8,10},{9,15},{10,... | collective-permute-start | bytes 1572872 | tf_op jit(solution)/shard_map/ppermute | solution.py:507
  58.2 3.2 %collective-permute-done.15.refs_1_ = bf16[272,512]{1,0:T(8,128)(2,1)S(1)} collective-permute-done((bf16[272,512]{1,0:T(8,128)(2,1)S(1)}, bf16[272,512]{1,0:T(8,128)(2,1)S(1)}, u32[]{:S(2)}, u32[]{:S(2)}) %collective-permute-start.15) | collective-permute-done | bytes 278560 | tf_op jit(solution)/shard_map/ppermute | solution.py:512
  61.5 4.6 %collective-permute-done.16.refs_2_ = bf16[272,512]{1,0:T(8,128)(2,1)S(1)} collective-permute-done((bf16[272,512]{1,0:T(8,128)(2,1)S(1)}, bf16[272,512]{1,0:T(8,128)(2,1)S(1)}, u32[]{:S(2)}, u32[]{:S(2)}) %collective-permute-start.16) | collective-permute-done | bytes 278560 | tf_op jit(solution)/shard_map/ppermute | solution.py:512
  67.0 2.0 %collective-permute-start.23 = (bf16[448,128]{1,0:T(8,128)(2,1)S(1)}, bf16[448,128]{1,0:T(8,128)(2,1)S(1)}, u32[]{:S(2)}, u32[]{:S(2)}) collective-permute-start(bf16[448,128]{1,0:T(8,128)(2,1)S(1)} %get-tuple-element.76), channel_id=1, source_target_pairs={{0,32},{1,225},{32,64},{33,1},{64,96},{65,33},{96,128},{97,65},{12... | collective-permute-start | bytes 344072 | tf_op jit(solution)/shard_map/ppermute | solution.py:526
  69.0 5.7 %collective-permute-start.24 = (bf16[448,128]{1,0:T(8,128)(2,1)S(1)}, bf16[448,128]{1,0:T(8,128)(2,1)S(1)}, u32[]{:S(2)}, u32[]{:S(2)}) collective-permute-start(bf16[448,128]{1,0:T(8,128)(2,1)S(1)} %get-tuple-element.77), channel_id=1, source_target_pairs={{0,64},{1,193},{32,96},{33,225},{64,128},{65,1},{96,160},{97,33},{... | collective-permute-start | bytes 344072 | tf_op jit(solution)/shard_map/ppermute | solution.py:526
  75.5 7.1 %collective-permute-start.22 = (bf16[448,128]{1,0:T(8,128)(2,1)S(1)}, bf16[448,128]{1,0:T(8,128)(2,1)S(1)}, u32[]{:S(2)}, u32[]{:S(2)}) collective-permute-start(bf16[448,128]{1,0:T(8,128)(2,1)S(1)} %get-tuple-element.75.mine), channel_id=1, source_target_pairs={{0,128},{32,160},{64,192},{96,224},{128,0},{160,32},{192,64},{224,... | collective-permute-start | bytes 344072 | tf_op jit(solution)/shard_map/ppermute | solution.py:526
  82.6 3.8 %collective-permute-done.22.opposite = bf16[448,128]{1,0:T(8,128)(2,1)S(1)} collective-permute-done((bf16[448,128]{1,0:T(8,128)(2,1)S(1)}, bf16[448,128]{1,0:T(8,128)(2,1)S(1)}, u32[]{:S(2)}, u32[]{:S(2)}) %collective-permute-start.22) | collective-permute-done | bytes 114720 | tf_op jit(solution)/shard_map/ppermute | solution.py:526
  86.6 1.3 %collective-permute-done.26.other = f32[224,128]{1,0:T(8,128)S(1)} collective-permute-done((f32[224,128]{1,0:T(8,128)S(1)}, f32[224,128]{1,0:T(8,128)S(1)}, u32[]{:S(2)}, u32[]{:S(2)}) %collective-permute-start.26) | collective-permute-done | bytes 114720 | tf_op jit(solution)/shard_map/ppermute | solution.py:497
  88.5 1.3 %shard_map.127 = bf16[1024,256]{1,0:T(8,128)(2,1)} custom-call(bf16[1040,256]{1,0:T(8,128)(2,1)S(1)} %shard_map.124.slopes, bf16[1040,256]{1,0:T(8,128)(2,1)S(1)} %collective-permute-done.10.others, bf16[2048,256]{1,0:T(8,128)(2,1)S(1)} %get-tuple-element.46.both, bf16[1024,256]{1,0:T(8,128)(2,1)S(1)} %collective-permute-done.11.lent, ...), custom_call_target="tpu_custom_call" | custom-call | flops 1073741824 | bytes 2097152 | tf_op jit(solution)/shard_map/pallas_call | solution.py:482
  (48 shorter events, 13.9 us)
Async XLA Ops:
  0.6 7.3 %copy-start = (bf16[1024,2048]{1,0:T(8,128)(2,1)S(1)}, bf16[1024,2048]{1,0:T(8,128)(2,1)}, u32[]{:S(2)}) copy-start(bf16[1024,2048]{1,0:T(8,128)(2,1)} %rows.10) | copy-start | bytes 12582916
  2.8 6.4 %copy-start.2 = (f32[31,128]{1,0:T(8,128)S(1)}, f32[31,128]{1,0:T(8,128)}, u32[]{:S(2)}) copy-start(f32[31,128]{1,0:T(8,128)} %taps.5) | copy-start | bytes 47620
  2.8 15.2 %copy-start.1 = (bf16[1024,2048]{1,0:T(8,128)(2,1)S(1)}, bf16[1024,2048]{1,0:T(8,128)(2,1)}, u32[]{:S(2)}) copy-start(bf16[1024,2048]{1,0:T(8,128)(2,1)} %rows.11) | copy-start | bytes 12582916
  2.8 8.0 %collective-permute-start = (f32[32,128]{1,0:T(8,128)S(1)}, f32[32,128]{1,0:T(8,128)S(1)}, u32[]{:S(2)}, u32[]{:S(2)}) collective-permute-start(f32[32,128]{1,0:T(8,128)S(1)} %get-tuple-element.49), channel_id=1, source_target_pairs={{0,8},{8,16},{16,24},{24,32},{32,40},{40,48},{48,56},{56,64},{64,7... | collective-permute-start | bytes 49160 | tf_op jit(solution)/shard_map/ppermute | solution.py:492
  6.6 5.8 %collective-permute-start.1 = (f32[64,128]{1,0:T(8,128)S(1)}, f32[64,128]{1,0:T(8,128)S(1)}, u32[]{:S(2)}, u32[]{:S(2)}) collective-permute-start(f32[64,128]{1,0:T(8,128)S(1)} %get-tuple-element.50), channel_id=1, source_target_pairs={{8,0},{16,8},{24,16},{32,24},{40,32},{48,40},{56,48},{64,56},{72,6... | collective-permute-start | bytes 98312 | tf_op jit(solution)/shard_map/ppermute | solution.py:492
  9.2 11.9 %copy-start.3 = (f32[128]{0:T(128)S(1)}, f32[128]{0:T(128)}, u32[]{:S(2)}) copy-start(f32[128]{0:T(128)} %param.11) | copy-start | bytes 1540
  12.6 1.3 %collective-permute-start.2 = (f32[2,1056]{1,0:T(2,128)S(1)}, f32[2,1056]{1,0:T(2,128)S(1)}, u32[]{:S(2)}, u32[]{:S(2)}) collective-permute-start(f32[2,1056]{1,0:T(2,128)S(1)} %get-tuple-element.55), channel_id=1, source_target_pairs={{0,1},{1,0},{2,3},{3,2},{4,5},{5,4},{6,7},{7,6},{8,9},{9,8},{10,11... | collective-permute-start | bytes 25352 | tf_op jit(solution)/shard_map/ppermute | solution.py:497
  13.9 6.1 %collective-permute-start.5 = (f32[2,1056]{1,0:T(2,128)S(1)}, f32[2,1056]{1,0:T(2,128)S(1)}, u32[]{:S(2)}, u32[]{:S(2)}) collective-permute-start(f32[2,1056]{1,0:T(2,128)S(1)} %add.6.s0), channel_id=1, source_target_pairs={{0,4},{1,5},{2,6},{3,7},{4,0},{5,1},{6,2},{7,3},{8,12},{9,13},{10,... | collective-permute-start | bytes 25352 | tf_op jit(solution)/shard_map/ppermute | solution.py:497
  16.0 4.0 %collective-permute-start.4 = (f32[2,1056]{1,0:T(2,128)S(1)}, f32[2,1056]{1,0:T(2,128)S(1)}, u32[]{:S(2)}, u32[]{:S(2)}) collective-permute-start(f32[2,1056]{1,0:T(2,128)S(1)} %add.6.s0), channel_id=1, source_target_pairs={{0,6},{1,7},{2,0},{3,1},{4,2},{5,3},{6,4},{7,5},{8,14},{9,15},{10,... | collective-permute-start | bytes 25352 | tf_op jit(solution)/shard_map/ppermute | solution.py:497
  17.4 3.7 %collective-permute-start.3 = (f32[2,1056]{1,0:T(2,128)S(1)}, f32[2,1056]{1,0:T(2,128)S(1)}, u32[]{:S(2)}, u32[]{:S(2)}) collective-permute-start(f32[2,1056]{1,0:T(2,128)S(1)} %add.6.s0), channel_id=1, source_target_pairs={{0,2},{1,3},{2,4},{3,5},{4,6},{5,7},{6,0},{7,1},{8,10},{9,11},{10,... | collective-permute-start | bytes 25352 | tf_op jit(solution)/shard_map/ppermute | solution.py:497
  22.0 1.3 %collective-permute-start.6 = (f32[2,1056]{1,0:T(2,128)S(1)}, f32[2,1056]{1,0:T(2,128)S(1)}, u32[]{:S(2)}, u32[]{:S(2)}) collective-permute-start(f32[2,1056]{1,0:T(2,128)S(1)} %get-tuple-element.59), channel_id=1, source_target_pairs={{0,1},{1,0},{2,3},{3,2},{4,5},{5,4},{6,7},{7,6},{8,9},{9,8},{10,11... | collective-permute-start | bytes 25352 | tf_op jit(solution)/shard_map/ppermute | solution.py:497
  23.3 5.2 %collective-permute-start.9 = (f32[2,1056]{1,0:T(2,128)S(1)}, f32[2,1056]{1,0:T(2,128)S(1)}, u32[]{:S(2)}, u32[]{:S(2)}) collective-permute-start(f32[2,1056]{1,0:T(2,128)S(1)} %add.7.s0), channel_id=1, source_target_pairs={{0,4},{1,5},{2,6},{3,7},{4,0},{5,1},{6,2},{7,3},{8,12},{9,13},{10,... | collective-permute-start | bytes 25352 | tf_op jit(solution)/shard_map/ppermute | solution.py:497
  24.8 3.9 %collective-permute-start.8 = (f32[2,1056]{1,0:T(2,128)S(1)}, f32[2,1056]{1,0:T(2,128)S(1)}, u32[]{:S(2)}, u32[]{:S(2)}) collective-permute-start(f32[2,1056]{1,0:T(2,128)S(1)} %add.7.s0), channel_id=1, source_target_pairs={{0,6},{1,7},{2,0},{3,1},{4,2},{5,3},{6,4},{7,5},{8,14},{9,15},{10,... | collective-permute-start | bytes 25352 | tf_op jit(solution)/shard_map/ppermute | solution.py:497
  25.9 3.7 %collective-permute-start.7 = (f32[2,1056]{1,0:T(2,128)S(1)}, f32[2,1056]{1,0:T(2,128)S(1)}, u32[]{:S(2)}, u32[]{:S(2)}) collective-permute-start(f32[2,1056]{1,0:T(2,128)S(1)} %add.7.s0), channel_id=1, source_target_pairs={{0,2},{1,3},{2,4},{3,5},{4,6},{5,7},{6,0},{7,1},{8,10},{9,11},{10,... | collective-permute-start | bytes 25352 | tf_op jit(solution)/shard_map/ppermute | solution.py:497
  32.8 2.8 %collective-permute-start.10 = (bf16[1040,256]{1,0:T(8,128)(2,1)S(1)}, bf16[1040,256]{1,0:T(8,128)(2,1)S(1)}, u32[]{:S(2)}, u32[]{:S(2)}) collective-permute-start(bf16[1040,256]{1,0:T(8,128)(2,1)S(1)} %shard_map.124.slopes), channel_id=1, source_target_pairs={{0,1},{1,0},{2,3},{3,2},{4,5},{5,4},{6,7},{7,6},{8,9},{9,8},{10,11... | collective-permute-start | bytes 1597448 | tf_op jit(solution)/shard_map/ppermute | solution.py:497
  32.9 2.7 %collective-permute-start.11 = (bf16[1024,256]{1,0:T(8,128)(2,1)S(1)}, bf16[1024,256]{1,0:T(8,128)(2,1)S(1)}, u32[]{:S(2)}, u32[]{:S(2)}) collective-permute-start(bf16[1024,256]{1,0:T(8,128)(2,1)S(1)} %get-tuple-element.63), channel_id=1, source_target_pairs={{0,1},{1,0},{2,3},{3,2},{4,5},{5,4},{6,7},{7,6},{8,9},{9,8},{10,11... | collective-permute-start | bytes 1572872 | tf_op jit(solution)/shard_map/ppermute | solution.py:497
  36.3 16.3 %collective-permute-start.12 = (bf16[1024,256]{1,0:T(8,128)(2,1)S(1)}, bf16[1024,256]{1,0:T(8,128)(2,1)S(1)}, u32[]{:S(2)}, u32[]{:S(2)}) collective-permute-start(bf16[1024,256]{1,0:T(8,128)(2,1)S(1)} %get-tuple-element.64), channel_id=1, source_target_pairs={{0,2},{1,7},{2,4},{3,1},{4,6},{5,3},{6,0},{7,5},{8,10},{9,15},{10,... | collective-permute-start | bytes 1572872 | tf_op jit(solution)/shard_map/ppermute | solution.py:507
  37.6 3.1 %collective-permute-start.18 = (bf16[1024,128]{1,0:T(8,128)(2,1)S(1)}, bf16[1024,128]{1,0:T(8,128)(2,1)S(1)}, u32[]{:S(2)}, u32[]{:S(2)}) collective-permute-start(bf16[1024,128]{1,0:T(8,128)(2,1)S(1)} %get-tuple-element.70.activated), channel_id=1, source_target_pairs={{0,1},{1,0},{2,3},{3,2},{4,5},{5,4},{6,7},{7,6},{8,9},{9,8},{10,11... | collective-permute-start | bytes 786440 | tf_op jit(solution)/shard_map/ppermute | solution.py:497
  42.2 10.2 %collective-permute-start.19 = (bf16[256,256]{1,0:T(8,128)(2,1)S(1)}, bf16[256,256]{1,0:T(8,128)(2,1)S(1)}, u32[]{:S(2)}, u32[]{:S(2)}) collective-permute-start(bf16[256,256]{1,0:T(8,128)(2,1)S(1)} %get-tuple-element.72), channel_id=1, source_target_pairs={{0,16},{8,24},{16,0},{24,8},{1,17},{9,25},{17,1},{25,9},{2,18},{10... | collective-permute-start | bytes 393224 | tf_op jit(solution)/shard_map/ppermute | solution.py:512
  46.0 10.1 %collective-permute-start.20 = (bf16[256,256]{1,0:T(8,128)(2,1)S(1)}, bf16[256,256]{1,0:T(8,128)(2,1)S(1)}, u32[]{:S(2)}, u32[]{:S(2)}) collective-permute-start(bf16[256,256]{1,0:T(8,128)(2,1)S(1)} %get-tuple-element.73), channel_id=1, source_target_pairs={{0,8},{8,16},{16,24},{24,0},{1,9},{9,17},{17,25},{25,1},{2,10},{10... | collective-permute-start | bytes 393224 | tf_op jit(solution)/shard_map/ppermute | solution.py:512
  49.2 7.8 %collective-permute-start.21 = (bf16[256,256]{1,0:T(8,128)(2,1)S(1)}, bf16[256,256]{1,0:T(8,128)(2,1)S(1)}, u32[]{:S(2)}, u32[]{:S(2)}) collective-permute-start(bf16[256,256]{1,0:T(8,128)(2,1)S(1)} %get-tuple-element.74), channel_id=1, source_target_pairs={{0,24},{8,0},{16,8},{24,16},{1,25},{9,1},{17,9},{25,17},{2,26},{10... | collective-permute-start | bytes 393224 | tf_op jit(solution)/shard_map/ppermute | solution.py:512
  50.3 11.2 %collective-permute-start.15 = (bf16[272,512]{1,0:T(8,128)(2,1)S(1)}, bf16[272,512]{1,0:T(8,128)(2,1)S(1)}, u32[]{:S(2)}, u32[]{:S(2)}) collective-permute-start(bf16[272,512]{1,0:T(8,128)(2,1)S(1)} %get-tuple-element.67), channel_id=1, source_target_pairs={{0,16},{8,24},{16,0},{24,8},{1,17},{9,25},{17,1},{25,9},{2,18},{10... | collective-permute-start | bytes 835592 | tf_op jit(solution)/shard_map/ppermute | solution.py:512
  52.4 13.7 %collective-permute-start.16 = (bf16[272,512]{1,0:T(8,128)(2,1)S(1)}, bf16[272,512]{1,0:T(8,128)(2,1)S(1)}, u32[]{:S(2)}, u32[]{:S(2)}) collective-permute-start(bf16[272,512]{1,0:T(8,128)(2,1)S(1)} %get-tuple-element.68), channel_id=1, source_target_pairs={{0,8},{8,16},{16,24},{24,0},{1,9},{9,17},{17,25},{25,1},{2,10},{10... | collective-permute-start | bytes 835592 | tf_op jit(solution)/shard_map/ppermute | solution.py:512
  52.6 14.2 %collective-permute-start.17 = (bf16[272,512]{1,0:T(8,128)(2,1)S(1)}, bf16[272,512]{1,0:T(8,128)(2,1)S(1)}, u32[]{:S(2)}, u32[]{:S(2)}) collective-permute-start(bf16[272,512]{1,0:T(8,128)(2,1)S(1)} %get-tuple-element.69), channel_id=1, source_target_pairs={{0,24},{8,0},{16,8},{24,16},{1,25},{9,1},{17,9},{25,17},{2,26},{10... | collective-permute-start | bytes 835592 | tf_op jit(solution)/shard_map/ppermute | solution.py:512
  56.1 32.4 %collective-permute-start.14 = (bf16[1024,256]{1,0:T(8,128)(2,1)S(1)}, bf16[1024,256]{1,0:T(8,128)(2,1)S(1)}, u32[]{:S(2)}, u32[]{:S(2)}) collective-permute-start(bf16[1024,256]{1,0:T(8,128)(2,1)S(1)} %get-tuple-element.65), channel_id=1, source_target_pairs={{0,6},{1,3},{2,0},{3,5},{4,2},{5,7},{6,4},{7,1},{8,14},{9,11},{10,... | collective-permute-start | bytes 1572872 | tf_op jit(solution)/shard_map/ppermute | solution.py:507
  57.0 31.5 %collective-permute-start.13 = (bf16[1024,256]{1,0:T(8,128)(2,1)S(1)}, bf16[1024,256]{1,0:T(8,128)(2,1)S(1)}, u32[]{:S(2)}, u32[]{:S(2)}) collective-permute-start(bf16[1024,256]{1,0:T(8,128)(2,1)S(1)} %shard_map.126), channel_id=1, source_target_pairs={{0,2},{1,7},{2,4},{3,1},{4,6},{5,3},{6,0},{7,5},{8,10},{9,15},{10,... | collective-permute-start | bytes 1572872 | tf_op jit(solution)/shard_map/ppermute | solution.py:507
  67.0 8.5 %collective-permute-start.23 = (bf16[448,128]{1,0:T(8,128)(2,1)S(1)}, bf16[448,128]{1,0:T(8,128)(2,1)S(1)}, u32[]{:S(2)}, u32[]{:S(2)}) collective-permute-start(bf16[448,128]{1,0:T(8,128)(2,1)S(1)} %get-tuple-element.76), channel_id=1, source_target_pairs={{0,32},{1,225},{32,64},{33,1},{64,96},{65,33},{96,128},{97,65},{12... | collective-permute-start | bytes 344072 | tf_op jit(solution)/shard_map/ppermute | solution.py:526
  69.0 13.6 %collective-permute-start.24 = (bf16[448,128]{1,0:T(8,128)(2,1)S(1)}, bf16[448,128]{1,0:T(8,128)(2,1)S(1)}, u32[]{:S(2)}, u32[]{:S(2)}) collective-permute-start(bf16[448,128]{1,0:T(8,128)(2,1)S(1)} %get-tuple-element.77), channel_id=1, source_target_pairs={{0,64},{1,193},{32,96},{33,225},{64,128},{65,1},{96,160},{97,33},{... | collective-permute-start | bytes 344072 | tf_op jit(solution)/shard_map/ppermute | solution.py:526
  74.7 7.9 %collective-permute-start.25 = (bf16[448,128]{1,0:T(8,128)(2,1)S(1)}, bf16[448,128]{1,0:T(8,128)(2,1)S(1)}, u32[]{:S(2)}, u32[]{:S(2)}) collective-permute-start(bf16[448,128]{1,0:T(8,128)(2,1)S(1)} %get-tuple-element.78), channel_id=1, source_target_pairs={{0,96},{1,161},{32,128},{33,193},{64,160},{65,225},{96,192},{97,1}... | collective-permute-start | bytes 344072 | tf_op jit(solution)/shard_map/ppermute | solution.py:526
  75.5 10.9 %collective-permute-start.22 = (bf16[448,128]{1,0:T(8,128)(2,1)S(1)}, bf16[448,128]{1,0:T(8,128)(2,1)S(1)}, u32[]{:S(2)}, u32[]{:S(2)}) collective-permute-start(bf16[448,128]{1,0:T(8,128)(2,1)S(1)} %get-tuple-element.75.mine), channel_id=1, source_target_pairs={{0,128},{32,160},{64,192},{96,224},{128,0},{160,32},{192,64},{224,... | collective-permute-start | bytes 344072 | tf_op jit(solution)/shard_map/ppermute | solution.py:526
  86.5 1.4 %collective-permute-start.26 = (f32[224,128]{1,0:T(8,128)S(1)}, f32[224,128]{1,0:T(8,128)S(1)}, u32[]{:S(2)}, u32[]{:S(2)}) collective-permute-start(f32[224,128]{1,0:T(8,128)S(1)} %get-tuple-element.80), channel_id=1, source_target_pairs={{0,1},{1,0},{2,3},{3,2},{4,5},{5,4},{6,7},{7,6},{8,9},{9,8},{10,11... | collective-permute-start | bytes 344072 | tf_op jit(solution)/shard_map/ppermute | solution.py:497

commit v3 on v2

--- a/solution.py
+++ b/solution.py
@@ -17,12 +17,11 @@
 W = 128
 PAD = 32
 EXT = ROWS + PAD
-TAIL = 16
 BLOCK = D // 8
 SLOTS = NZ // NC
 PART = D // (NY * NC)
 CUT = D // (NY * NZ)
-PIECE = 3 * CUT + 2 * TAIL
+PIECE = 3 * CUT + K + 1
 FLOOR = 0.1
 F32 = jnp.float32
 BF16 = jnp.bfloat16
@@ -258,11 +257,8 @@
 
 
 def adjoint_kernel(
-    normed, norm_slope, inverse, s0, s1, s2, s3, mixed, prior, taps, sgate, factor, gain_part,
-    slopes, curve, means, crosses, history, taps_part,
+    normed, norm_slope, inverse, s0, s1, s2, s3, taps, sgate, factor, slopes, curve, means, crosses
 ):
-    history[:PAD] = prior[...]
-    history[PAD:] = mixed[...]
     spread_sums((s0, s1, s2, s3), (means, crosses))
     curve[...] = inverse[...] * (norm_slope[...] - means[...] - normed[...] * crosses[...])
 
@@ -281,6 +277,20 @@
 
     lax.fori_loop(0, ROWS // step, spread, 0)
 
+
+def adjoint_of(normed, norm_slope, inverse, back, taps, sgate, factor):
+    return pl.pallas_call(
+        adjoint_kernel,
+        out_shape=[shape_of((ROWS, 2 * W), BF16), shape_of((EXT, W))],
+        scratch_shapes=[pltpu.VMEM((EXT, W), F32)] * 2,
+        compiler_params=params(16),
+        cost_estimate=cost(2 * ROWS * D * 256, 2 * 1024 * 1024),
+    )(normed, norm_slope, inverse, *back, taps, sgate, factor)
+
+
+def taps_kernel(curve, mixed, prior, gain_part, taps_part, history):
+    history[:PAD] = prior[...]
+    history[PAD:] = mixed[...]
     inner = 64
 
     def gather(i, sums):
@@ -300,19 +310,16 @@
     for k in range(K):
         taps_part[k : k + 1, :] = jnp.sum(sums[k], axis=0, keepdims=True)
     taps_part[K:, :] = gain_part[...]
-    small = taps_part[...].astype(BF16)
-    slopes[ROWS:, :W] = small[:TAIL]
-    slopes[ROWS:, W:] = small[TAIL:]
-
-
-def adjoint_of(normed, norm_slope, inverse, back, mixed, prior, taps, sgate, factor, gain_part):
-    return pl.pallas_call(
-        adjoint_kernel,
-        out_shape=shape_of((ROWS + TAIL, 2 * W), BF16),
-        scratch_shapes=[pltpu.VMEM((EXT, W), F32)] * 4 + [pltpu.VMEM((K + 1, W), F32)],
-        compiler_params=params(16),
-        cost_estimate=cost(2 * ROWS * D * 256, 2 * 1024 * 1024),
-    )(normed, norm_slope, inverse, *back, mixed, prior, taps, sgate, factor, gain_part)
+
+
+def taps_of(curve, mixed, prior, gain_part):
+    return pl.pallas_call(
+        taps_kernel,
+        out_shape=shape_of((K + 1, W)),
+        scratch_shapes=[pltpu.VMEM((PAD + ROWS, W), F32)],
+        compiler_params=params(8),
+        cost_estimate=cost(2 * ROWS * D * 64, 1024 * 1024),
+    )(curve, mixed, prior, gain_part)
 
 
 def kept_by(slot):
@@ -354,7 +361,7 @@
 
 
 def own_weight_grad_kernel(rows, slopes, parts):
-    across(rows, slopes[:ROWS], parts, slice(0, 2 * W))
+    across(rows, slopes[...], parts, slice(0, 2 * W))
 
 
 def own_weight_grad_of(block_input, slopes):
@@ -366,24 +373,22 @@
     )(block_input, slopes)
 
 
-def weight_grad_kernel(rows, slopes, others, own, *rest):
+def weight_grad_kernel(rows, others, own, *rest):
     outs, parts = rest[:NY], rest[NY]
-    across(rows, others[:ROWS], parts, slice(0, 2 * W))
+    across(rows, others[...], parts, slice(0, 2 * W))
     for by, out in enumerate(outs):
-        out[:PART, : 2 * W] = own[along_y(by)]
-        out[:PART, 2 * W :] = parts[along_y(by)]
-        out[PART:, : 2 * W] = slopes[ROWS:]
-        out[PART:, 2 * W :] = others[ROWS:]
-
-
-def weight_grad_of(block_input, slopes, others, own):
+        out[:, : 2 * W] = own[along_y(by)]
+        out[:, 2 * W :] = parts[along_y(by)]
+
+
+def weight_grad_of(block_input, others, own):
     return pl.pallas_call(
         weight_grad_kernel,
-        out_shape=[shape_of((PART + TAIL, 4 * W), BF16)] * NY,
+        out_shape=[shape_of((PART, 4 * W), BF16)] * NY,
         scratch_shapes=[pltpu.VMEM((NY, PART, 2 * W), BF16)],
         compiler_params=params(12),
         cost_estimate=cost(2 * ROWS * D * 128, 5 * 1024 * 1024),
-    )(block_input, slopes, others, own)
+    )(block_input, others, own)
 
 
 def summed(parts):
@@ -394,9 +399,10 @@
 
 
 def middle_kernel(*refs):
-    both, side, outs = refs[:NY], refs[NY : 2 * NY], refs[2 * NY :]
+    both, side, small, outs = refs[:NY], refs[NY : 2 * NY], refs[2 * NY : 3 * NY], refs[3 * NY :]
     total = summed(both).astype(BF16)
     outer = summed(side).astype(BF16)
+    tail = summed(small).astype(BF16)
     for slot, out in enumerate(outs):
         rows = slice(slot * CUT, (slot + 1) * CUT)
         for core in range(NC):
@@ -404,33 +410,45 @@
             out[at : at + CUT] = total[rows, lane : lane + W]
             out[at + CUT : at + 2 * CUT] = total[rows, lane + W : lane + 2 * W]
             out[at + 2 * CUT : at + 3 * CUT] = outer[rows, core * W : (core + 1) * W]
-            out[at + 3 * CUT : at + 3 * CUT + TAIL] = total[PART:, lane : lane + W]
-            out[at + 3 * CUT + TAIL : at + PIECE] = total[PART:, lane + W : lane + 2 * W]
-
-
-def middle_of(both, side):
+            out[at + 3 * CUT : at + PIECE] = tail[:, core * W : (core + 1) * W]
+
+
+def middle_of(both, side, small):
     return pl.pallas_call(
         middle_kernel,
         out_shape=[shape_of((NC * PIECE, W), BF16)] * SLOTS,
         compiler_params=params(12),
         cost_estimate=cost(2 * ROWS * D, 2 * 1024 * 1024),
-    )(*both, *side)
-
-
-def chip_kernel(mine, opposite, one, two, three, own, other):
-    first = jnp.where(lax.axis_index("c") == 0, opposite[...].astype(F32), mine[...].astype(F32))
-    total = first + summed((one, two, three))
+    )(*both, *side, *small)
+
+
+def add_kernel(mine, arrived, out):
+    out[...] = (mine[...].astype(F32) + arrived[...].astype(F32)).astype(BF16)
+
+
+def added(mine, arrived):
+    return pl.pallas_call(
+        add_kernel,
+        out_shape=shape_of(mine.shape, BF16),
+        compiler_params=params(8),
+        cost_estimate=cost(2 * ROWS * D, 1024 * 1024),
+    )(mine, arrived)
+
+
+def chip_kernel(mine, arrived, own, other):
+    total = arrived[...].astype(F32)
+    total = total + jnp.where(lax.axis_index("c") == 0, jnp.zeros_like(total), mine[...].astype(F32))
     own[...] = total[:PIECE]
     other[...] = total[PIECE:]
 
 
-def chip_of(mine, parts):
+def chip_of(mine, arrived):
     return pl.pallas_call(
         chip_kernel,
         out_shape=[shape_of((PIECE, W))] * 2,
         compiler_params=params(8),
         cost_estimate=cost(2 * ROWS * D, 1024 * 1024),
-    )(mine, *parts)
+    )(mine, arrived)
 
 
 def final_kernel(own, other, value_grad, gate_grad, out_grad, taps_grad, gain_grad):
@@ -459,8 +477,8 @@
     mine = both[pl.ds(pl.multiple_of((chip * NC + core) * BLOCK, BLOCK), BLOCK), :]
     theirs = lent[pl.ds(pl.multiple_of(chip * BLOCK, BLOCK), BLOCK), :]
     contract = (((1,), (1,)), ((), ()))
-    total = lax.dot_general(slopes[:ROWS], mine, contract, preferred_element_type=F32)
-    return total + lax.dot_general(others[:ROWS], theirs, contract, preferred_element_type=F32)
+    total = lax.dot_general(slopes[...], mine, contract, preferred_element_type=F32)
+    return total + lax.dot_general(others[...], theirs, contract, preferred_element_type=F32)
 
 
 def far_kernel(slopes, others, both, lent, far, back):
@@ -516,13 +534,8 @@
     return [parts[0]] + [further(parts[by], axis, by) for by in order]
 
 
-def to_keeper(value, slot):
-    if slot == 0:
-        pairs = [(z * NC, (z + 4) % NZ * NC) for z in range(NZ)]
-    else:
-        pairs = [
-            (z * NC + c, (z + (slot if c == 0 else -slot)) % NZ * NC + c) for z in range(NZ) for c in range(NC)
-        ]
+def round_z(value, cores):
+    pairs = [(z * NC + c, (z + 1 - 2 * c) % NZ * NC + c) for z in range(NZ) for c in cores]
     return lax.ppermute(value, ("z", "c"), pairs)
 
 
@@ -542,12 +555,10 @@
     other_activated = to_slot(activated, 1)
     out_parts = out_grad_of(grad_output, activated, other_activated)
     out_parts = spread(out_parts, "y", Y_ORDER)
-    slopes = adjoint_of(
-        normed, norm_slope, inverse, back, mixed, prior, conv_taps, sgate, factor, gain_part
-    )
+    slopes, curve = adjoint_of(normed, norm_slope, inverse, back, conv_taps, sgate, factor)
     others = to_slot(slopes, 1)
     own_parts = own_weight_grad_of(block_input, slopes)
-    both_parts = weight_grad_of(block_input, slopes, others, own_parts)
+    both_parts = weight_grad_of(block_input, others, own_parts)
     both_parts = spread(both_parts, "y", Y_ORDER)
     lent = to_slot(lend, 1)
     sides = (slopes, others, both, lent)
@@ -556,9 +567,15 @@
     (near,) = share_call(near_kernel, 1, 1, *sides, arrived)
     near = along(near, 1)
     single = along(single, -1)
-    parts = middle_of(both_parts, out_parts)
-    sent = {slot: to_keeper(parts[slot], slot) for slot in Z_ORDER}
-    own, other = chip_of(parts[0], [sent[slot] for slot in range(SLOTS)])
+    taps_part = taps_of(curve, mixed, prior, gain_part)
+    other_taps = to_slot(taps_part, 1)
+    small = spread([jnp.concatenate([taps_part, other_taps], axis=1)] * NY, "y", Y_ORDER)
+    parts = middle_of(both_parts, out_parts, small)
+    arrived = round_z(parts[0], (0,))
+    for slot in (3, 2, 1):
+        passed = added(parts[slot], arrived)
+        arrived = round_z(passed, (0, 1))
+    own, other = chip_of(parts[0], arrived)
     other = to_slot(other, 1)
     (input_grad,) = share_call(own_kernel, 1, 1, *sides, near, single)
     value_grad, gate_grad, out_grad, taps_grad, gain_grad = final_of(own, other)
@@ -566,7 +583,6 @@
 
 
 Y_ORDER = (2, 1, 3)
-Z_ORDER = (0, 3, 2, 1)
 
 
 def solution(mesh):

time: 91.6 us -> 100 us (1.092)
  waiting for transfers between devices: 24.4 us -> 40 us
  starting transfers between devices: 46.3 us -> 40.1 us
    ppermute x4, waiting for transfers between devices: 3.76 us -> 19.4 us  [round_z(): return lax.ppermute(value, ('z', 'c'), pairs)]
    ppermute x4, starting transfers between devices: 15.6 us -> 5.68 us  [round_z(): return lax.ppermute(value, ('z', 'c'), pairs)]
    ppermute x6 -> x9, starting transfers between devices: 11.6 us -> 16.7 us  [further(): lax.ppermute(value, axis, [(i, (i + by) % count) for i in range(count)])]
    ppermute x12 -> x13, waiting for transfers between devices: 10.6 us -> 7.26 us  [to_slot(): return lax.ppermute(value, TP, pairs)]
    ppermute x6 -> x9, waiting for transfers between devices: 8.58 us -> 11.7 us  [further(): lax.ppermute(value, axis, [(i, (i + by) % count) for i in range(count)])]
    ppermute x12 -> x13, starting transfers between devices: 10.8 us -> 9.21 us  [to_slot(): return lax.ppermute(value, TP, pairs)]
    pallas_call x2 -> x6, Pallas kernels: 4.17 us -> 4.24 us  [the longest x1 1.89 us: adjoint_of(): pl.pallas_call(adjoint_kernel, out_shape=[shape_of((ROWS, 2 * W), BF16),...]
  transfers between devices with their start and end apart: 27 -> 31, of which waited for: 14 -> 14; matrix products, arithmetic and copies ran while one was open for 0% -> 0% of each run, Pallas kernels for 11% -> 14%
where the time goes in v3:
time: 100 us; the launch traced here: 99.1 us
  starting transfers between devices  40.1 us (40%)
  waiting for transfers between devices  40 us (40%)
  Pallas kernels  18 us (18%)
    ppermute x4, waiting for transfers between devices, round_z(): return lax.ppermute(value, ('z', 'c'), pairs)  19.4 us
    ppermute x9, starting transfers between devices, further(): lax.ppermute(value, axis, [(i, (i + by) % count) for i in range(count)])  16.7 us
    ppermute x9, waiting for transfers between devices, further(): lax.ppermute(value, axis, [(i, (i + by) % count) for i in range(count)])  11.7 us
    ppermute x13, starting transfers between devices, to_slot(): return lax.ppermute(value, TP, pairs)  9.21 us
    ppermute x13, waiting for transfers between devices, to_slot(): return lax.ppermute(value, TP, pairs)  7.26 us
    ppermute x4, starting transfers between devices, round_z(): return lax.ppermute(value, ('z', 'c'), pairs)  5.68 us
    ppermute x2, starting transfers between devices, from_behind(): lax.ppermute(value, SP, [(i, i + by) for i in range(count) if 0 <= i + by...  5.04 us
    ppermute x3, starting transfers between devices, along(): return lax.ppermute(value, TP, pairs)  3.48 us
  transfers between devices with their start and end apart: 31, of which 14 were waited for; matrix products, arithmetic and copies ran while one was open for 0% of the time, Pallas kernels for 14%

profile of v3, /device:TPU:2, one launch (start us, length us, event | category | flops | bytes accessed | tf_op | source)
XLA Modules:
  0.0 99.1 jit_solution(7601502682636396015)
XLA Ops:
  0.6 2.2 %shard_map.118 = (f32[32,128]{1,0:T(8,128)S(1)}, f32[64,128]{1,0:T(8,128)S(1)}, bf16[2048,256]{1,0:T(8,128)(2,1)S(1)}, bf16[2048,128]{1,0:T(8,128)(2,1)S(1)}) custom-call(bf16[1024,2048]{1,0:T(8,128)(2,1)} %rows.10, bf16[1024,2048]{1,0:T(8,128)(2,1)} %rows.11, bf16[2048,128]{1,0:T(8,128)(2,1)} %value_proj.1, bf16[2048,128]{1,0:T(8,128)(2,1)} %gate_proj.1, ...), custom_call_target="tpu_custom_call" | custom-call | flops 100663296 | bytes 2097152 | tf_op jit(solution)/shard_map/pallas_call | solution.py:79
  2.8 3.7 %collective-permute-start = (f32[32,128]{1,0:T(8,128)S(1)}, f32[32,128]{1,0:T(8,128)S(1)}, u32[]{:S(2)}, u32[]{:S(2)}) collective-permute-start(f32[32,128]{1,0:T(8,128)S(1)} %get-tuple-element.51), channel_id=1, source_target_pairs={{0,8},{8,16},{16,24},{24,32},{32,40},{40,48},{48,56},{56,64},{64,7... | collective-permute-start | bytes 49160 | tf_op jit(solution)/shard_map/ppermute | solution.py:510
  6.6 1.3 %collective-permute-start.1 = (f32[64,128]{1,0:T(8,128)S(1)}, f32[64,128]{1,0:T(8,128)S(1)}, u32[]{:S(2)}, u32[]{:S(2)}) collective-permute-start(f32[64,128]{1,0:T(8,128)S(1)} %get-tuple-element.52), channel_id=1, source_target_pairs={{8,0},{16,8},{24,16},{32,24},{40,32},{48,40},{56,48},{64,56},{72,6... | collective-permute-start | bytes 98312 | tf_op jit(solution)/shard_map/ppermute | solution.py:510
  7.9 1.3 %shard_map.119 = (f32[1024,128]{1,0:T(8,128)S(1)}, f32[1024,128]{1,0:T(8,128)S(1)}, f32[1024,128]{1,0:T(8,128)S(1)}) custom-call(bf16[1024,2048]{1,0:T(8,128)(2,1)S(1)} %copy-done, bf16[2048,256]{1,0:T(8,128)(2,1)S(1)} %get-tuple-element.48.both), custom_call_target="tpu_custom_call" | custom-call | flops 1073741824 | bytes 7340032 | tf_op jit(solution)/shard_map/pallas_call | solution.py:106
  9.2 1.6 %shard_map.120 = (f32[1024,128]{1,0:T(8,128)S(1)}, f32[2,1024]{1,0:T(2,128)S(1)}) custom-call(f32[1024,128]{1,0:T(8,128)S(1)} %get-tuple-element.49.mixed, f32[31,128]{1,0:T(8,128)S(1)} %copy-done.2), custom_call_target="tpu_custom_call" | custom-call | flops 536870912 | bytes 2097152 | tf_op jit(solution)/shard_map/pallas_call | solution.py:186
  10.8 1.6 %collective-permute-done.1.after = f32[64,128]{1,0:T(8,128)S(1)} collective-permute-done((f32[64,128]{1,0:T(8,128)S(1)}, f32[64,128]{1,0:T(8,128)S(1)}, u32[]{:S(2)}, u32[]{:S(2)}) %collective-permute-start.1) | collective-permute-done | bytes 32800 | tf_op jit(solution)/shard_map/ppermute | solution.py:510
  12.7 1.2 %collective-permute-done.2 = f32[2,1056]{1,0:T(2,128)S(1)} collective-permute-done((f32[2,1056]{1,0:T(2,128)S(1)}, f32[2,1056]{1,0:T(2,128)S(1)}, u32[]{:S(2)}, u32[]{:S(2)}) %collective-permute-start.2) | collective-permute-done | bytes 8480 | tf_op jit(solution)/shard_map/ppermute | solution.py:515
  13.8 2.1 %collective-permute-start.5 = (f32[2,1056]{1,0:T(2,128)S(1)}, f32[2,1056]{1,0:T(2,128)S(1)}, u32[]{:S(2)}, u32[]{:S(2)}) collective-permute-start(f32[2,1056]{1,0:T(2,128)S(1)} %add.6.s0), channel_id=1, source_target_pairs={{0,4},{1,5},{2,6},{3,7},{4,0},{5,1},{6,2},{7,3},{8,12},{9,13},{10,... | collective-permute-start | bytes 25352 | tf_op jit(solution)/shard_map/ppermute | solution.py:515
  16.0 1.4 %collective-permute-start.4 = (f32[2,1056]{1,0:T(2,128)S(1)}, f32[2,1056]{1,0:T(2,128)S(1)}, u32[]{:S(2)}, u32[]{:S(2)}) collective-permute-start(f32[2,1056]{1,0:T(2,128)S(1)} %add.6.s0), channel_id=1, source_target_pairs={{0,6},{1,7},{2,0},{3,1},{4,2},{5,3},{6,4},{7,5},{8,14},{9,15},{10,... | collective-permute-start | bytes 25352 | tf_op jit(solution)/shard_map/ppermute | solution.py:515
  18.0 1.9 %shard_map.122 = (f32[1024,128]{1,0:T(8,128)S(1)}, bf16[1024,256]{1,0:T(8,128)(2,1)S(1)}) custom-call(bf16[1024,2048]{1,0:T(8,128)(2,1)S(1)} %copy-done.1, bf16[2048,128]{1,0:T(8,128)(2,1)S(1)} %get-tuple-element.55.out_side, bf16[2048,256]{1,0:T(8,128)(2,1)S(1)} %get-tuple-element.48.both), custom_call_target="tpu_custom_call" | custom-call | flops 1073741824 | bytes 5242880 | tf_op jit(solution)/shard_map/pallas_call | solution.py:132
  23.3 1.5 %collective-permute-start.9 = (f32[2,1056]{1,0:T(2,128)S(1)}, f32[2,1056]{1,0:T(2,128)S(1)}, u32[]{:S(2)}, u32[]{:S(2)}) collective-permute-start(f32[2,1056]{1,0:T(2,128)S(1)} %add.7.s0), channel_id=1, source_target_pairs={{0,4},{1,5},{2,6},{3,7},{4,0},{5,1},{6,2},{7,3},{8,12},{9,13},{10,... | collective-permute-start | bytes 25352 | tf_op jit(solution)/shard_map/ppermute | solution.py:515
  27.1 1.3 %collective-permute-done.9.s3 = f32[2,1056]{1,0:T(2,128)S(1)} collective-permute-done((f32[2,1056]{1,0:T(2,128)S(1)}, f32[2,1056]{1,0:T(2,128)S(1)}, u32[]{:S(2)}, u32[]{:S(2)}) %collective-permute-start.9) | collective-permute-done | bytes 8480 | tf_op jit(solution)/shard_map/ppermute | solution.py:515
  29.6 1.9 %shard_map.124 = (bf16[1024,256]{1,0:T(8,128)(2,1)S(1)}, f32[1056,128]{1,0:T(8,128)S(1)}) custom-call(f32[1056,128]{1,0:T(8,128)S(1)} %get-tuple-element.58.normed, f32[1056,128]{1,0:T(8,128)S(1)} %get-tuple-element.59.norm_slope, f32[1056,128]{1,0:T(8,128)S(1)} %get-tuple-element.60.inverse, f32[2,1056]{1,0:T(2,128)S(1)} %add.7.s0, ...), custom_call_target="tpu_custom_call" | custom-call | flops 1073741824 | bytes 2097152 | tf_op jit(solution)/shard_map/pallas_call | solution.py:282
  32.1 1.3 %shard_map.131 = f32[32,128]{1,0:T(8,128)S(1)} custom-call(f32[1056,128]{1,0:T(8,128)S(1)} %get-tuple-element.77.curve, f32[1024,128]{1,0:T(8,128)S(1)} %get-tuple-element.49.mixed, f32[32,128]{1,0:T(8,128)S(1)} %collective-permute-done.prior, f32[1,128]{1,0:T(1,128)S(1)} %get-tuple-element.78.gain_part), custom_call_target="tpu_custom_call" | custom-call | flops 268435456 | bytes 1048576 | tf_op jit(solution)/shard_map/pallas_call | solution.py:316
  35.4 1.2 %collective-permute-start.12 = (bf16[1024,256]{1,0:T(8,128)(2,1)S(1)}, bf16[1024,256]{1,0:T(8,128)(2,1)S(1)}, u32[]{:S(2)}, u32[]{:S(2)}) collective-permute-start(bf16[1024,256]{1,0:T(8,128)(2,1)S(1)} %get-tuple-element.66), channel_id=1, source_target_pairs={{0,2},{1,7},{2,4},{3,1},{4,6},{5,3},{6,0},{7,5},{8,10},{9,15},{10,... | collective-permute-start | bytes 1572872 | tf_op jit(solution)/shard_map/ppermute | solution.py:525
  36.6 1.5 %shard_map.130 = (bf16[256,256]{1,0:T(8,128)(2,1)S(1)}, bf16[256,256]{1,0:T(8,128)(2,1)S(1)}, bf16[256,256]{1,0:T(8,128)(2,1)S(1)}, bf16[256,256]{1,0:T(8,128)(2,1)S(1)}) custom-call(bf16[1024,2048]{1,0:T(8,128)(2,1)S(1)} %copy-done.1, bf16[1024,128]{1,0:T(8,128)(2,1)S(1)} %get-tuple-element.72.activated, bf16[1024,128]{1,0:T(8,128)(2,1)S(1)} %collective-permute-done.18.other), custom_call_target="tpu_custom_call" | custom-call | flops 1073741824 | bytes 5242880 | tf_op jit(solution)/shard_map/pallas_call | solution.py:354
  38.1 3.0 %collective-permute-start.19 = (bf16[256,256]{1,0:T(8,128)(2,1)S(1)}, bf16[256,256]{1,0:T(8,128)(2,1)S(1)}, u32[]{:S(2)}, u32[]{:S(2)}) collective-permute-start(bf16[256,256]{1,0:T(8,128)(2,1)S(1)} %get-tuple-element.74), channel_id=1, source_target_pairs={{0,16},{8,24},{16,0},{24,8},{1,17},{9,25},{17,1},{25,9},{2,18},{10... | collective-permute-start | bytes 393224 | tf_op jit(solution)/shard_map/ppermute | solution.py:530
  41.1 2.3 %collective-permute-start.25 = (f32[32,256]{1,0:T(8,128)S(1)}, f32[32,256]{1,0:T(8,128)S(1)}, u32[]{:S(2)}, u32[]{:S(2)}) collective-permute-start(f32[32,256]{1,0:T(8,128)S(1)} %pad_maximum_fusion.refs_8_), channel_id=1, source_target_pairs={{0,24},{8,0},{16,8},{24,16},{1,25},{9,1},{17,9},{25,17},{2,26},{10... | collective-permute-start | bytes 98312 | tf_op jit(solution)/shard_map/ppermute | solution.py:530
  44.3 2.0 %collective-permute-start.23 = (f32[32,256]{1,0:T(8,128)S(1)}, f32[32,256]{1,0:T(8,128)S(1)}, u32[]{:S(2)}, u32[]{:S(2)}) collective-permute-start(f32[32,256]{1,0:T(8,128)S(1)} %pad_maximum_fusion.refs_8_), channel_id=1, source_target_pairs={{0,16},{8,24},{16,0},{24,8},{1,17},{9,25},{17,1},{25,9},{2,18},{10... | collective-permute-start | bytes 98312 | tf_op jit(solution)/shard_map/ppermute | solution.py:530
  48.1 1.4 %collective-permute-start.20 = (bf16[256,256]{1,0:T(8,128)(2,1)S(1)}, bf16[256,256]{1,0:T(8,128)(2,1)S(1)}, u32[]{:S(2)}, u32[]{:S(2)}) collective-permute-start(bf16[256,256]{1,0:T(8,128)(2,1)S(1)} %get-tuple-element.75), channel_id=1, source_target_pairs={{0,8},{8,16},{16,24},{24,0},{1,9},{9,17},{17,25},{25,1},{2,10},{10... | collective-permute-start | bytes 393224 | tf_op jit(solution)/shard_map/ppermute | solution.py:530
  49.5 2.4 %collective-permute-start.15 = (bf16[256,512]{1,0:T(8,128)(2,1)S(1)}, bf16[256,512]{1,0:T(8,128)(2,1)S(1)}, u32[]{:S(2)}, u32[]{:S(2)}) collective-permute-start(bf16[256,512]{1,0:T(8,128)(2,1)S(1)} %get-tuple-element.69), channel_id=1, source_target_pairs={{0,16},{8,24},{16,0},{24,8},{1,17},{9,25},{17,1},{25,9},{2,18},{10... | collective-permute-start | bytes 786440 | tf_op jit(solution)/shard_map/ppermute | solution.py:530
  52.2 3.0 %collective-permute-start.17 = (bf16[256,512]{1,0:T(8,128)(2,1)S(1)}, bf16[256,512]{1,0:T(8,128)(2,1)S(1)}, u32[]{:S(2)}, u32[]{:S(2)}) collective-permute-start(bf16[256,512]{1,0:T(8,128)(2,1)S(1)} %get-tuple-element.71), channel_id=1, source_target_pairs={{0,24},{8,0},{16,8},{24,16},{1,25},{9,1},{17,9},{25,17},{2,26},{10... | collective-permute-start | bytes 786440 | tf_op jit(solution)/shard_map/ppermute | solution.py:530
  55.1 1.5 %collective-permute-start.21 = (bf16[256,256]{1,0:T(8,128)(2,1)S(1)}, bf16[256,256]{1,0:T(8,128)(2,1)S(1)}, u32[]{:S(2)}, u32[]{:S(2)}) collective-permute-start(bf16[256,256]{1,0:T(8,128)(2,1)S(1)} %get-tuple-element.76), channel_id=1, source_target_pairs={{0,24},{8,0},{16,8},{24,16},{1,25},{9,1},{17,9},{25,17},{2,26},{10... | collective-permute-start | bytes 393224 | tf_op jit(solution)/shard_map/ppermute | solution.py:530
  56.7 10.8 %collective-permute-done.21.refs_7_ = bf16[256,256]{1,0:T(8,128)(2,1)S(1)} collective-permute-done((bf16[256,256]{1,0:T(8,128)(2,1)S(1)}, bf16[256,256]{1,0:T(8,128)(2,1)S(1)}, u32[]{:S(2)}, u32[]{:S(2)}) %collective-permute-start.21) | collective-permute-done | bytes 131104 | tf_op jit(solution)/shard_map/ppermute | solution.py:530
  67.5 1.8 %collective-permute-start.14 = (bf16[1024,256]{1,0:T(8,128)(2,1)S(1)}, bf16[1024,256]{1,0:T(8,128)(2,1)S(1)}, u32[]{:S(2)}, u32[]{:S(2)}) collective-permute-start(bf16[1024,256]{1,0:T(8,128)(2,1)S(1)} %get-tuple-element.67), channel_id=1, source_target_pairs={{0,6},{1,3},{2,0},{3,5},{4,2},{5,7},{6,4},{7,1},{8,14},{9,11},{10,... | collective-permute-start | bytes 1572872 | tf_op jit(solution)/shard_map/ppermute | solution.py:525
  69.5 3.8 %collective-permute-start.26 = (bf16[448,128]{1,0:T(8,128)(2,1)S(1)}, bf16[448,128]{1,0:T(8,128)(2,1)S(1)}, u32[]{:S(2)}, u32[]{:S(2)}) collective-permute-start(bf16[448,128]{1,0:T(8,128)(2,1)S(1)} %get-tuple-element.79.mine), channel_id=1, source_target_pairs={{0,32},{32,64},{64,96},{96,128},{128,160},{160,192},{192,224},{224... | collective-permute-start | bytes 344072 | tf_op jit(solution)/shard_map/ppermute | solution.py:539
  74.3 3.1 %collective-permute-done.26.arrived = bf16[448,128]{1,0:T(8,128)(2,1)S(1)} collective-permute-done((bf16[448,128]{1,0:T(8,128)(2,1)S(1)}, bf16[448,128]{1,0:T(8,128)(2,1)S(1)}, u32[]{:S(2)}, u32[]{:S(2)}) %collective-permute-start.26) | collective-permute-done | bytes 114720 | tf_op jit(solution)/shard_map/ppermute | solution.py:539
  78.2 5.3 %collective-permute-done.27.arrived = bf16[448,128]{1,0:T(8,128)(2,1)S(1)} collective-permute-done((bf16[448,128]{1,0:T(8,128)(2,1)S(1)}, bf16[448,128]{1,0:T(8,128)(2,1)S(1)}, u32[]{:S(2)}, u32[]{:S(2)}) %collective-permute-start.27) | collective-permute-done | bytes 114720 | tf_op jit(solution)/shard_map/ppermute | solution.py:539
  84.5 5.1 %collective-permute-done.28.arrived = bf16[448,128]{1,0:T(8,128)(2,1)S(1)} collective-permute-done((bf16[448,128]{1,0:T(8,128)(2,1)S(1)}, bf16[448,128]{1,0:T(8,128)(2,1)S(1)}, u32[]{:S(2)}, u32[]{:S(2)}) %collective-permute-start.28) | collective-permute-done | bytes 114720 | tf_op jit(solution)/shard_map/ppermute | solution.py:539
  89.7 6.0 %collective-permute-done.29.arrived = bf16[448,128]{1,0:T(8,128)(2,1)S(1)} collective-permute-done((bf16[448,128]{1,0:T(8,128)(2,1)S(1)}, bf16[448,128]{1,0:T(8,128)(2,1)S(1)}, u32[]{:S(2)}, u32[]{:S(2)}) %collective-permute-start.29) | collective-permute-done | bytes 114720 | tf_op jit(solution)/shard_map/ppermute | solution.py:539
  95.9 1.3 %collective-permute-done.30.other = f32[224,128]{1,0:T(8,128)S(1)} collective-permute-done((f32[224,128]{1,0:T(8,128)S(1)}, f32[224,128]{1,0:T(8,128)S(1)}, u32[]{:S(2)}, u32[]{:S(2)}) %collective-permute-start.30) | collective-permute-done | bytes 114720 | tf_op jit(solution)/shard_map/ppermute | solution.py:515
  97.8 1.3 %shard_map.127 = bf16[1024,256]{1,0:T(8,128)(2,1)} custom-call(bf16[1024,256]{1,0:T(8,128)(2,1)S(1)} %get-tuple-element.64.slopes, bf16[1024,256]{1,0:T(8,128)(2,1)S(1)} %collective-permute-done.10.others, bf16[2048,256]{1,0:T(8,128)(2,1)S(1)} %get-tuple-element.48.both, bf16[1024,256]{1,0:T(8,128)(2,1)S(1)} %collective-permute-done.11.lent, ...), custom_call_target="tpu_custom_call" | custom-call | flops 1073741824 | bytes 2097152 | tf_op jit(solution)/shard_map/pallas_call | solution.py:500
  (61 shorter events, 17.0 us)
Async XLA Ops:
  2.8 15.2 %copy-start.1 = (bf16[1024,2048]{1,0:T(8,128)(2,1)S(1)}, bf16[1024,2048]{1,0:T(8,128)(2,1)}, u32[]{:S(2)}) copy-start(bf16[1024,2048]{1,0:T(8,128)(2,1)} %rows.11) | copy-start | bytes 12582916
  2.8 8.0 %collective-permute-start = (f32[32,128]{1,0:T(8,128)S(1)}, f32[32,128]{1,0:T(8,128)S(1)}, u32[]{:S(2)}, u32[]{:S(2)}) collective-permute-start(f32[32,128]{1,0:T(8,128)S(1)} %get-tuple-element.51), channel_id=1, source_target_pairs={{0,8},{8,16},{16,24},{24,32},{32,40},{40,48},{48,56},{56,64},{64,7... | collective-permute-start | bytes 49160 | tf_op jit(solution)/shard_map/ppermute | solution.py:510
  6.6 5.8 %collective-permute-start.1 = (f32[64,128]{1,0:T(8,128)S(1)}, f32[64,128]{1,0:T(8,128)S(1)}, u32[]{:S(2)}, u32[]{:S(2)}) collective-permute-start(f32[64,128]{1,0:T(8,128)S(1)} %get-tuple-element.52), channel_id=1, source_target_pairs={{8,0},{16,8},{24,16},{32,24},{40,32},{48,40},{56,48},{64,56},{72,6... | collective-permute-start | bytes 98312 | tf_op jit(solution)/shard_map/ppermute | solution.py:510
  12.6 1.3 %collective-permute-start.2 = (f32[2,1056]{1,0:T(2,128)S(1)}, f32[2,1056]{1,0:T(2,128)S(1)}, u32[]{:S(2)}, u32[]{:S(2)}) collective-permute-start(f32[2,1056]{1,0:T(2,128)S(1)} %get-tuple-element.57), channel_id=1, source_target_pairs={{0,1},{1,0},{2,3},{3,2},{4,5},{5,4},{6,7},{7,6},{8,9},{9,8},{10,11... | collective-permute-start | bytes 25352 | tf_op jit(solution)/shard_map/ppermute | solution.py:515
  13.8 6.1 %collective-permute-start.5 = (f32[2,1056]{1,0:T(2,128)S(1)}, f32[2,1056]{1,0:T(2,128)S(1)}, u32[]{:S(2)}, u32[]{:S(2)}) collective-permute-start(f32[2,1056]{1,0:T(2,128)S(1)} %add.6.s0), channel_id=1, source_target_pairs={{0,4},{1,5},{2,6},{3,7},{4,0},{5,1},{6,2},{7,3},{8,12},{9,13},{10,... | collective-permute-start | bytes 25352 | tf_op jit(solution)/shard_map/ppermute | solution.py:515
  16.0 4.0 %collective-permute-start.4 = (f32[2,1056]{1,0:T(2,128)S(1)}, f32[2,1056]{1,0:T(2,128)S(1)}, u32[]{:S(2)}, u32[]{:S(2)}) collective-permute-start(f32[2,1056]{1,0:T(2,128)S(1)} %add.6.s0), channel_id=1, source_target_pairs={{0,6},{1,7},{2,0},{3,1},{4,2},{5,3},{6,4},{7,5},{8,14},{9,15},{10,... | collective-permute-start | bytes 25352 | tf_op jit(solution)/shard_map/ppermute | solution.py:515
  17.4 3.7 %collective-permute-start.3 = (f32[2,1056]{1,0:T(2,128)S(1)}, f32[2,1056]{1,0:T(2,128)S(1)}, u32[]{:S(2)}, u32[]{:S(2)}) collective-permute-start(f32[2,1056]{1,0:T(2,128)S(1)} %add.6.s0), channel_id=1, source_target_pairs={{0,2},{1,3},{2,4},{3,5},{4,6},{5,7},{6,0},{7,1},{8,10},{9,11},{10,... | collective-permute-start | bytes 25352 | tf_op jit(solution)/shard_map/ppermute | solution.py:515
  22.0 1.3 %collective-permute-start.6 = (f32[2,1056]{1,0:T(2,128)S(1)}, f32[2,1056]{1,0:T(2,128)S(1)}, u32[]{:S(2)}, u32[]{:S(2)}) collective-permute-start(f32[2,1056]{1,0:T(2,128)S(1)} %get-tuple-element.61), channel_id=1, source_target_pairs={{0,1},{1,0},{2,3},{3,2},{4,5},{5,4},{6,7},{7,6},{8,9},{9,8},{10,11... | collective-permute-start | bytes 25352 | tf_op jit(solution)/shard_map/ppermute | solution.py:515
  23.3 5.2 %collective-permute-start.9 = (f32[2,1056]{1,0:T(2,128)S(1)}, f32[2,1056]{1,0:T(2,128)S(1)}, u32[]{:S(2)}, u32[]{:S(2)}) collective-permute-start(f32[2,1056]{1,0:T(2,128)S(1)} %add.7.s0), channel_id=1, source_target_pairs={{0,4},{1,5},{2,6},{3,7},{4,0},{5,1},{6,2},{7,3},{8,12},{9,13},{10,... | collective-permute-start | bytes 25352 | tf_op jit(solution)/shard_map/ppermute | solution.py:515
  24.8 3.9 %collective-permute-start.8 = (f32[2,1056]{1,0:T(2,128)S(1)}, f32[2,1056]{1,0:T(2,128)S(1)}, u32[]{:S(2)}, u32[]{:S(2)}) collective-permute-start(f32[2,1056]{1,0:T(2,128)S(1)} %add.7.s0), channel_id=1, source_target_pairs={{0,6},{1,7},{2,0},{3,1},{4,2},{5,3},{6,4},{7,5},{8,14},{9,15},{10,... | collective-permute-start | bytes 25352 | tf_op jit(solution)/shard_map/ppermute | solution.py:515
  25.9 3.7 %collective-permute-start.7 = (f32[2,1056]{1,0:T(2,128)S(1)}, f32[2,1056]{1,0:T(2,128)S(1)}, u32[]{:S(2)}, u32[]{:S(2)}) collective-permute-start(f32[2,1056]{1,0:T(2,128)S(1)} %add.7.s0), channel_id=1, source_target_pairs={{0,2},{1,3},{2,4},{3,5},{4,6},{5,7},{6,0},{7,1},{8,10},{9,11},{10,... | collective-permute-start | bytes 25352 | tf_op jit(solution)/shard_map/ppermute | solution.py:515
  27.1 7.5 %collective-permute-start.11 = (bf16[1024,256]{1,0:T(8,128)(2,1)S(1)}, bf16[1024,256]{1,0:T(8,128)(2,1)S(1)}, u32[]{:S(2)}, u32[]{:S(2)}) collective-permute-start(bf16[1024,256]{1,0:T(8,128)(2,1)S(1)} %get-tuple-element.65), channel_id=1, source_target_pairs={{0,1},{1,0},{2,3},{3,2},{4,5},{5,4},{6,7},{7,6},{8,9},{9,8},{10,11... | collective-permute-start | bytes 1572872 | tf_op jit(solution)/shard_map/ppermute | solution.py:515
  31.5 3.1 %collective-permute-start.10 = (bf16[1024,256]{1,0:T(8,128)(2,1)S(1)}, bf16[1024,256]{1,0:T(8,128)(2,1)S(1)}, u32[]{:S(2)}, u32[]{:S(2)}) collective-permute-start(bf16[1024,256]{1,0:T(8,128)(2,1)S(1)} %get-tuple-element.64.slopes), channel_id=1, source_target_pairs={{0,1},{1,0},{2,3},{3,2},{4,5},{5,4},{6,7},{7,6},{8,9},{9,8},{10,11... | collective-permute-start | bytes 1572872 | tf_op jit(solution)/shard_map/ppermute | solution.py:515
  31.6 5.0 %collective-permute-start.18 = (bf16[1024,128]{1,0:T(8,128)(2,1)S(1)}, bf16[1024,128]{1,0:T(8,128)(2,1)S(1)}, u32[]{:S(2)}, u32[]{:S(2)}) collective-permute-start(bf16[1024,128]{1,0:T(8,128)(2,1)S(1)} %get-tuple-element.72.activated), channel_id=1, source_target_pairs={{0,1},{1,0},{2,3},{3,2},{4,5},{5,4},{6,7},{7,6},{8,9},{9,8},{10,11... | collective-permute-start | bytes 786440 | tf_op jit(solution)/shard_map/ppermute | solution.py:515
  33.4 7.7 %collective-permute-start.22 = (f32[32,128]{1,0:T(8,128)S(1)}, f32[32,128]{1,0:T(8,128)S(1)}, u32[]{:S(2)}, u32[]{:S(2)}) collective-permute-start(f32[32,128]{1,0:T(8,128)S(1)} %shard_map.131), channel_id=1, source_target_pairs={{0,1},{1,0},{2,3},{3,2},{4,5},{5,4},{6,7},{7,6},{8,9},{9,8},{10,11... | collective-permute-start | bytes 49160 | tf_op jit(solution)/shard_map/ppermute | solution.py:515
  35.4 38.0 %collective-permute-start.12 = (bf16[1024,256]{1,0:T(8,128)(2,1)S(1)}, bf16[1024,256]{1,0:T(8,128)(2,1)S(1)}, u32[]{:S(2)}, u32[]{:S(2)}) collective-permute-start(bf16[1024,256]{1,0:T(8,128)(2,1)S(1)} %get-tuple-element.66), channel_id=1, source_target_pairs={{0,2},{1,7},{2,4},{3,1},{4,6},{5,3},{6,0},{7,5},{8,10},{9,15},{10,... | collective-permute-start | bytes 1572872 | tf_op jit(solution)/shard_map/ppermute | solution.py:525
  38.1 14.1 %collective-permute-start.19 = (bf16[256,256]{1,0:T(8,128)(2,1)S(1)}, bf16[256,256]{1,0:T(8,128)(2,1)S(1)}, u32[]{:S(2)}, u32[]{:S(2)}) collective-permute-start(bf16[256,256]{1,0:T(8,128)(2,1)S(1)} %get-tuple-element.74), channel_id=1, source_target_pairs={{0,16},{8,24},{16,0},{24,8},{1,17},{9,25},{17,1},{25,9},{2,18},{10... | collective-permute-start | bytes 393224 | tf_op jit(solution)/shard_map/ppermute | solution.py:530
  41.1 7.0 %collective-permute-start.25 = (f32[32,256]{1,0:T(8,128)S(1)}, f32[32,256]{1,0:T(8,128)S(1)}, u32[]{:S(2)}, u32[]{:S(2)}) collective-permute-start(f32[32,256]{1,0:T(8,128)S(1)} %pad_maximum_fusion.refs_8_), channel_id=1, source_target_pairs={{0,24},{8,0},{16,8},{24,16},{1,25},{9,1},{17,9},{25,17},{2,26},{10... | collective-permute-start | bytes 98312 | tf_op jit(solution)/shard_map/ppermute | solution.py:530
  43.4 6.1 %collective-permute-start.24 = (f32[32,256]{1,0:T(8,128)S(1)}, f32[32,256]{1,0:T(8,128)S(1)}, u32[]{:S(2)}, u32[]{:S(2)}) collective-permute-start(f32[32,256]{1,0:T(8,128)S(1)} %pad_maximum_fusion.refs_8_), channel_id=1, source_target_pairs={{0,8},{8,16},{16,24},{24,0},{1,9},{9,17},{17,25},{25,1},{2,10},{10... | collective-permute-start | bytes 98312 | tf_op jit(solution)/shard_map/ppermute | solution.py:530
  44.3 7.6 %collective-permute-start.23 = (f32[32,256]{1,0:T(8,128)S(1)}, f32[32,256]{1,0:T(8,128)S(1)}, u32[]{:S(2)}, u32[]{:S(2)}) collective-permute-start(f32[32,256]{1,0:T(8,128)S(1)} %pad_maximum_fusion.refs_8_), channel_id=1, source_target_pairs={{0,16},{8,24},{16,0},{24,8},{1,17},{9,25},{17,1},{25,9},{2,18},{10... | collective-permute-start | bytes 98312 | tf_op jit(solution)/shard_map/ppermute | solution.py:530
  48.1 7.1 %collective-permute-start.20 = (bf16[256,256]{1,0:T(8,128)(2,1)S(1)}, bf16[256,256]{1,0:T(8,128)(2,1)S(1)}, u32[]{:S(2)}, u32[]{:S(2)}) collective-permute-start(bf16[256,256]{1,0:T(8,128)(2,1)S(1)} %get-tuple-element.75), channel_id=1, source_target_pairs={{0,8},{8,16},{16,24},{24,0},{1,9},{9,17},{17,25},{25,1},{2,10},{10... | collective-permute-start | bytes 393224 | tf_op jit(solution)/shard_map/ppermute | solution.py:530
  49.5 19.8 %collective-permute-start.15 = (bf16[256,512]{1,0:T(8,128)(2,1)S(1)}, bf16[256,512]{1,0:T(8,128)(2,1)S(1)}, u32[]{:S(2)}, u32[]{:S(2)}) collective-permute-start(bf16[256,512]{1,0:T(8,128)(2,1)S(1)} %get-tuple-element.69), channel_id=1, source_target_pairs={{0,16},{8,24},{16,0},{24,8},{1,17},{9,25},{17,1},{25,9},{2,18},{10... | collective-permute-start | bytes 786440 | tf_op jit(solution)/shard_map/ppermute | solution.py:530
  51.9 17.4 %collective-permute-start.16 = (bf16[256,512]{1,0:T(8,128)(2,1)S(1)}, bf16[256,512]{1,0:T(8,128)(2,1)S(1)}, u32[]{:S(2)}, u32[]{:S(2)}) collective-permute-start(bf16[256,512]{1,0:T(8,128)(2,1)S(1)} %get-tuple-element.70), channel_id=1, source_target_pairs={{0,8},{8,16},{16,24},{24,0},{1,9},{9,17},{17,25},{25,1},{2,10},{10... | collective-permute-start | bytes 786440 | tf_op jit(solution)/shard_map/ppermute | solution.py:530
  52.2 17.1 %collective-permute-start.17 = (bf16[256,512]{1,0:T(8,128)(2,1)S(1)}, bf16[256,512]{1,0:T(8,128)(2,1)S(1)}, u32[]{:S(2)}, u32[]{:S(2)}) collective-permute-start(bf16[256,512]{1,0:T(8,128)(2,1)S(1)} %get-tuple-element.71), channel_id=1, source_target_pairs={{0,24},{8,0},{16,8},{24,16},{1,25},{9,1},{17,9},{25,17},{2,26},{10... | collective-permute-start | bytes 786440 | tf_op jit(solution)/shard_map/ppermute | solution.py:530
  55.1 12.4 %collective-permute-start.21 = (bf16[256,256]{1,0:T(8,128)(2,1)S(1)}, bf16[256,256]{1,0:T(8,128)(2,1)S(1)}, u32[]{:S(2)}, u32[]{:S(2)}) collective-permute-start(bf16[256,256]{1,0:T(8,128)(2,1)S(1)} %get-tuple-element.76), channel_id=1, source_target_pairs={{0,24},{8,0},{16,8},{24,16},{1,25},{9,1},{17,9},{25,17},{2,26},{10... | collective-permute-start | bytes 393224 | tf_op jit(solution)/shard_map/ppermute | solution.py:530
  67.5 30.3 %collective-permute-start.14 = (bf16[1024,256]{1,0:T(8,128)(2,1)S(1)}, bf16[1024,256]{1,0:T(8,128)(2,1)S(1)}, u32[]{:S(2)}, u32[]{:S(2)}) collective-permute-start(bf16[1024,256]{1,0:T(8,128)(2,1)S(1)} %get-tuple-element.67), channel_id=1, source_target_pairs={{0,6},{1,3},{2,0},{3,5},{4,2},{5,7},{6,4},{7,1},{8,14},{9,11},{10,... | collective-permute-start | bytes 1572872 | tf_op jit(solution)/shard_map/ppermute | solution.py:525
  69.5 7.9 %collective-permute-start.26 = (bf16[448,128]{1,0:T(8,128)(2,1)S(1)}, bf16[448,128]{1,0:T(8,128)(2,1)S(1)}, u32[]{:S(2)}, u32[]{:S(2)}) collective-permute-start(bf16[448,128]{1,0:T(8,128)(2,1)S(1)} %get-tuple-element.79.mine), channel_id=1, source_target_pairs={{0,32},{32,64},{64,96},{96,128},{128,160},{160,192},{192,224},{224... | collective-permute-start | bytes 344072 | tf_op jit(solution)/shard_map/ppermute | solution.py:539
  73.8 24.0 %collective-permute-start.13 = (bf16[1024,256]{1,0:T(8,128)(2,1)S(1)}, bf16[1024,256]{1,0:T(8,128)(2,1)S(1)}, u32[]{:S(2)}, u32[]{:S(2)}) collective-permute-start(bf16[1024,256]{1,0:T(8,128)(2,1)S(1)} %shard_map.126), channel_id=1, source_target_pairs={{0,2},{1,7},{2,4},{3,1},{4,6},{5,3},{6,0},{7,5},{8,10},{9,15},{10,... | collective-permute-start | bytes 1572872 | tf_op jit(solution)/shard_map/ppermute | solution.py:525
  77.4 6.1 %collective-permute-start.27 = (bf16[448,128]{1,0:T(8,128)(2,1)S(1)}, bf16[448,128]{1,0:T(8,128)(2,1)S(1)}, u32[]{:S(2)}, u32[]{:S(2)}) collective-permute-start(bf16[448,128]{1,0:T(8,128)(2,1)S(1)} %shard_map.133), channel_id=1, source_target_pairs={{0,32},{1,225},{32,64},{33,1},{64,96},{65,33},{96,128},{97,65},{12... | collective-permute-start | bytes 344072 | tf_op jit(solution)/shard_map/ppermute | solution.py:539
  83.5 6.1 %collective-permute-start.28 = (bf16[448,128]{1,0:T(8,128)(2,1)S(1)}, bf16[448,128]{1,0:T(8,128)(2,1)S(1)}, u32[]{:S(2)}, u32[]{:S(2)}) collective-permute-start(bf16[448,128]{1,0:T(8,128)(2,1)S(1)} %shard_map.134), channel_id=1, source_target_pairs={{0,32},{1,225},{32,64},{33,1},{64,96},{65,33},{96,128},{97,65},{12... | collective-permute-start | bytes 344072 | tf_op jit(solution)/shard_map/ppermute | solution.py:539
  89.6 6.1 %collective-permute-start.29 = (bf16[448,128]{1,0:T(8,128)(2,1)S(1)}, bf16[448,128]{1,0:T(8,128)(2,1)S(1)}, u32[]{:S(2)}, u32[]{:S(2)}) collective-permute-start(bf16[448,128]{1,0:T(8,128)(2,1)S(1)} %shard_map.135), channel_id=1, source_target_pairs={{0,32},{1,225},{32,64},{33,1},{64,96},{65,33},{96,128},{97,65},{12... | collective-permute-start | bytes 344072 | tf_op jit(solution)/shard_map/ppermute | solution.py:539
  95.8 1.4 %collective-permute-start.30 = (f32[224,128]{1,0:T(8,128)S(1)}, f32[224,128]{1,0:T(8,128)S(1)}, u32[]{:S(2)}, u32[]{:S(2)}) collective-permute-start(f32[224,128]{1,0:T(8,128)S(1)} %get-tuple-element.84), channel_id=1, source_target_pairs={{0,1},{1,0},{2,3},{3,2},{4,5},{5,4},{6,7},{7,6},{8,9},{9,8},{10,11... | collective-permute-start | bytes 344072 | tf_op jit(solution)/shard_map/ppermute | solution.py:515
  (3 other events, 25.5 us)

commit v4 on v3

--- a/solution.py
+++ b/solution.py
@@ -422,33 +422,20 @@
     )(*both, *side, *small)
 
 
-def add_kernel(mine, arrived, out):
-    out[...] = (mine[...].astype(F32) + arrived[...].astype(F32)).astype(BF16)
-
-
-def added(mine, arrived):
-    return pl.pallas_call(
-        add_kernel,
-        out_shape=shape_of(mine.shape, BF16),
-        compiler_params=params(8),
-        cost_estimate=cost(2 * ROWS * D, 1024 * 1024),
-    )(mine, arrived)
-
-
-def chip_kernel(mine, arrived, own, other):
-    total = arrived[...].astype(F32)
-    total = total + jnp.where(lax.axis_index("c") == 0, jnp.zeros_like(total), mine[...].astype(F32))
+def chip_kernel(mine, opposite, one, two, three, own, other):
+    first = jnp.where(lax.axis_index("c") == 0, opposite[...].astype(F32), mine[...].astype(F32))
+    total = first + summed((one, two, three))
     own[...] = total[:PIECE]
     other[...] = total[PIECE:]
 
 
-def chip_of(mine, arrived):
+def chip_of(mine, parts):
     return pl.pallas_call(
         chip_kernel,
         out_shape=[shape_of((PIECE, W))] * 2,
         compiler_params=params(8),
         cost_estimate=cost(2 * ROWS * D, 1024 * 1024),
-    )(mine, arrived)
+    )(mine, *parts)
 
 
 def final_kernel(own, other, value_grad, gate_grad, out_grad, taps_grad, gain_grad):
@@ -534,8 +521,13 @@
     return [parts[0]] + [further(parts[by], axis, by) for by in order]
 
 
-def round_z(value, cores):
-    pairs = [(z * NC + c, (z + 1 - 2 * c) % NZ * NC + c) for z in range(NZ) for c in cores]
+def to_keeper(value, slot):
+    if slot == 0:
+        pairs = [(z * NC, (z + 4) % NZ * NC) for z in range(NZ)]
+    else:
+        pairs = [
+            (z * NC + c, (z + (slot if c == 0 else -slot)) % NZ * NC + c) for z in range(NZ) for c in range(NC)
+        ]
     return lax.ppermute(value, ("z", "c"), pairs)
 
 
@@ -571,11 +563,8 @@
     other_taps = to_slot(taps_part, 1)
     small = spread([jnp.concatenate([taps_part, other_taps], axis=1)] * NY, "y", Y_ORDER)
     parts = middle_of(both_parts, out_parts, small)
-    arrived = round_z(parts[0], (0,))
-    for slot in (3, 2, 1):
-        passed = added(parts[slot], arrived)
-        arrived = round_z(passed, (0, 1))
-    own, other = chip_of(parts[0], arrived)
+    sent = {slot: to_keeper(parts[slot], slot) for slot in Z_ORDER}
+    own, other = chip_of(parts[0], [sent[slot] for slot in range(SLOTS)])
     other = to_slot(other, 1)
     (input_grad,) = share_call(own_kernel, 1, 1, *sides, near, single)
     value_grad, gate_grad, out_grad, taps_grad, gain_grad = final_of(own, other)
@@ -583,6 +572,7 @@
 
 
 Y_ORDER = (2, 1, 3)
+Z_ORDER = (0, 3, 2, 1)
 
 
 def solution(mesh):

time: 100 us -> 94.9 us (0.949)
  the two profiles are of different devices: /device:TPU:2 before, /device:TPU:103 now
where the time goes in v4:
time: 94.9 us; the launch traced here: 94.8 us
  starting transfers between devices  52.5 us (55%)
  waiting for transfers between devices  23.4 us (25%)
  Pallas kernels  17.9 us (19%)
    ppermute x13, starting transfers between devices, to_slot(): return lax.ppermute(value, TP, pairs)  25.7 us
    ppermute x9, starting transfers between devices, further(): lax.ppermute(value, axis, [(i, (i + by) % count) for i in range(count)])  14.2 us
    ppermute x9, waiting for transfers between devices, further(): lax.ppermute(value, axis, [(i, (i + by) % count) for i in range(count)])  11.7 us
    ppermute x2, starting transfers between devices, from_behind(): lax.ppermute(value, SP, [(i, i + by) for i in range(count) if 0 <= i + by...  7.66 us
    ppermute x4, waiting for transfers between devices, to_keeper(): return lax.ppermute(value, ('z', 'c'), pairs)  7.51 us
    ppermute x13, waiting for transfers between devices, to_slot(): return lax.ppermute(value, TP, pairs)  4.18 us
    ppermute x4, starting transfers between devices, to_keeper(): return lax.ppermute(value, ('z', 'c'), pairs)  3.09 us
    pallas_call x3, Pallas kernels, share_call(): pl.pallas_call(kernel, out_shape=[piece] * count, compiler_params=params(...  2.49 us
  transfers between devices with their start and end apart: 31, of which 11 were waited for; matrix products, arithmetic and copies ran while one was open for 0% of the time, Pallas kernels for 14%

profile of v4, /device:TPU:103, one launch (start us, length us, event | category | flops | bytes accessed | tf_op | source)
XLA Modules:
  0.0 94.8 jit_solution(8146092217223293690)
XLA Ops:
  0.6 2.2 %shard_map.118 = (f32[32,128]{1,0:T(8,128)S(1)}, f32[64,128]{1,0:T(8,128)S(1)}, bf16[2048,256]{1,0:T(8,128)(2,1)S(1)}, bf16[2048,128]{1,0:T(8,128)(2,1)S(1)}) custom-call(bf16[1024,2048]{1,0:T(8,128)(2,1)} %rows.10, bf16[1024,2048]{1,0:T(8,128)(2,1)} %rows.11, bf16[2048,128]{1,0:T(8,128)(2,1)} %value_proj.1, bf16[2048,128]{1,0:T(8,128)(2,1)} %gate_proj.1, ...), custom_call_target="tpu_custom_call" | custom-call | flops 100663296 | bytes 2097152 | tf_op jit(solution)/shard_map/pallas_call | solution.py:79
  2.8 3.5 %collective-permute-start = (f32[32,128]{1,0:T(8,128)S(1)}, f32[32,128]{1,0:T(8,128)S(1)}, u32[]{:S(2)}, u32[]{:S(2)}) collective-permute-start(f32[32,128]{1,0:T(8,128)S(1)} %get-tuple-element.51), channel_id=1, source_target_pairs={{0,8},{8,16},{16,24},{24,32},{32,40},{40,48},{48,56},{56,64},{64,7... | collective-permute-start | bytes 49160 | tf_op jit(solution)/shard_map/ppermute | solution.py:497
  6.3 4.2 %collective-permute-start.1 = (f32[64,128]{1,0:T(8,128)S(1)}, f32[64,128]{1,0:T(8,128)S(1)}, u32[]{:S(2)}, u32[]{:S(2)}) collective-permute-start(f32[64,128]{1,0:T(8,128)S(1)} %get-tuple-element.52), channel_id=1, source_target_pairs={{8,0},{16,8},{24,16},{32,24},{40,32},{48,40},{56,48},{64,56},{72,6... | collective-permute-start | bytes 98312 | tf_op jit(solution)/shard_map/ppermute | solution.py:497
  10.5 1.3 %shard_map.119 = (f32[1024,128]{1,0:T(8,128)S(1)}, f32[1024,128]{1,0:T(8,128)S(1)}, f32[1024,128]{1,0:T(8,128)S(1)}) custom-call(bf16[1024,2048]{1,0:T(8,128)(2,1)S(1)} %copy-done, bf16[2048,256]{1,0:T(8,128)(2,1)S(1)} %get-tuple-element.48.both), custom_call_target="tpu_custom_call" | custom-call | flops 1073741824 | bytes 7340032 | tf_op jit(solution)/shard_map/pallas_call | solution.py:106
  11.8 1.6 %shard_map.120 = (f32[1024,128]{1,0:T(8,128)S(1)}, f32[2,1024]{1,0:T(2,128)S(1)}) custom-call(f32[1024,128]{1,0:T(8,128)S(1)} %get-tuple-element.49.mixed, f32[31,128]{1,0:T(8,128)S(1)} %copy-done.2), custom_call_target="tpu_custom_call" | custom-call | flops 536870912 | bytes 2097152 | tf_op jit(solution)/shard_map/pallas_call | solution.py:186
  13.6 1.3 %collective-permute-start.2 = (f32[2,1056]{1,0:T(2,128)S(1)}, f32[2,1056]{1,0:T(2,128)S(1)}, u32[]{:S(2)}, u32[]{:S(2)}) collective-permute-start(f32[2,1056]{1,0:T(2,128)S(1)} %get-tuple-element.57), channel_id=1, source_target_pairs={{0,1},{1,0},{2,3},{3,2},{4,5},{5,4},{6,7},{7,6},{8,9},{9,8},{10,11... | collective-permute-start | bytes 25352 | tf_op jit(solution)/shard_map/ppermute | solution.py:502
  16.9 2.7 %collective-permute-start.3 = (f32[2,1056]{1,0:T(2,128)S(1)}, f32[2,1056]{1,0:T(2,128)S(1)}, u32[]{:S(2)}, u32[]{:S(2)}) collective-permute-start(f32[2,1056]{1,0:T(2,128)S(1)} %add.6.s0), channel_id=1, source_target_pairs={{0,2},{1,3},{2,4},{3,5},{4,6},{5,7},{6,0},{7,1},{8,10},{9,11},{10,... | collective-permute-start | bytes 25352 | tf_op jit(solution)/shard_map/ppermute | solution.py:502
  19.6 1.9 %shard_map.122 = (f32[1024,128]{1,0:T(8,128)S(1)}, bf16[1024,256]{1,0:T(8,128)(2,1)S(1)}) custom-call(bf16[1024,2048]{1,0:T(8,128)(2,1)S(1)} %copy-done.1, bf16[2048,128]{1,0:T(8,128)(2,1)S(1)} %get-tuple-element.55.out_side, bf16[2048,256]{1,0:T(8,128)(2,1)S(1)} %get-tuple-element.48.both), custom_call_target="tpu_custom_call" | custom-call | flops 1073741824 | bytes 5242880 | tf_op jit(solution)/shard_map/pallas_call | solution.py:132
  22.5 1.3 %collective-permute-start.6 = (f32[2,1056]{1,0:T(2,128)S(1)}, f32[2,1056]{1,0:T(2,128)S(1)}, u32[]{:S(2)}, u32[]{:S(2)}) collective-permute-start(f32[2,1056]{1,0:T(2,128)S(1)} %get-tuple-element.61), channel_id=1, source_target_pairs={{0,1},{1,0},{2,3},{3,2},{4,5},{5,4},{6,7},{7,6},{8,9},{9,8},{10,11... | collective-permute-start | bytes 25352 | tf_op jit(solution)/shard_map/ppermute | solution.py:502
  24.6 1.7 %collective-permute-start.9 = (f32[2,1056]{1,0:T(2,128)S(1)}, f32[2,1056]{1,0:T(2,128)S(1)}, u32[]{:S(2)}, u32[]{:S(2)}) collective-permute-start(f32[2,1056]{1,0:T(2,128)S(1)} %add.7.s0), channel_id=1, source_target_pairs={{0,4},{1,5},{2,6},{3,7},{4,0},{5,1},{6,2},{7,3},{8,12},{9,13},{10,... | collective-permute-start | bytes 25352 | tf_op jit(solution)/shard_map/ppermute | solution.py:502
  26.4 1.5 %collective-permute-start.8 = (f32[2,1056]{1,0:T(2,128)S(1)}, f32[2,1056]{1,0:T(2,128)S(1)}, u32[]{:S(2)}, u32[]{:S(2)}) collective-permute-start(f32[2,1056]{1,0:T(2,128)S(1)} %add.7.s0), channel_id=1, source_target_pairs={{0,6},{1,7},{2,0},{3,1},{4,2},{5,3},{6,4},{7,5},{8,14},{9,15},{10,... | collective-permute-start | bytes 25352 | tf_op jit(solution)/shard_map/ppermute | solution.py:502
  30.3 1.9 %shard_map.124 = (bf16[1024,256]{1,0:T(8,128)(2,1)S(1)}, f32[1056,128]{1,0:T(8,128)S(1)}) custom-call(f32[1056,128]{1,0:T(8,128)S(1)} %get-tuple-element.58.normed, f32[1056,128]{1,0:T(8,128)S(1)} %get-tuple-element.59.norm_slope, f32[1056,128]{1,0:T(8,128)S(1)} %get-tuple-element.60.inverse, f32[2,1056]{1,0:T(2,128)S(1)} %add.7.s0, ...), custom_call_target="tpu_custom_call" | custom-call | flops 1073741824 | bytes 2097152 | tf_op jit(solution)/shard_map/pallas_call | solution.py:282
  32.2 2.1 %collective-permute-start.10 = (bf16[1024,256]{1,0:T(8,128)(2,1)S(1)}, bf16[1024,256]{1,0:T(8,128)(2,1)S(1)}, u32[]{:S(2)}, u32[]{:S(2)}) collective-permute-start(bf16[1024,256]{1,0:T(8,128)(2,1)S(1)} %get-tuple-element.64.slopes), channel_id=1, source_target_pairs={{0,1},{1,0},{2,3},{3,2},{4,5},{5,4},{6,7},{7,6},{8,9},{9,8},{10,11... | collective-permute-start | bytes 1572872 | tf_op jit(solution)/shard_map/ppermute | solution.py:502
  34.5 1.4 %collective-permute-done.10.others = bf16[1024,256]{1,0:T(8,128)(2,1)S(1)} collective-permute-done((bf16[1024,256]{1,0:T(8,128)(2,1)S(1)}, bf16[1024,256]{1,0:T(8,128)(2,1)S(1)}, u32[]{:S(2)}, u32[]{:S(2)}) %collective-permute-start.10) | collective-permute-done | bytes 524320 | tf_op jit(solution)/shard_map/ppermute | solution.py:502
  36.9 1.3 %shard_map.131 = f32[32,128]{1,0:T(8,128)S(1)} custom-call(f32[1056,128]{1,0:T(8,128)S(1)} %get-tuple-element.77.curve, f32[1024,128]{1,0:T(8,128)S(1)} %get-tuple-element.49.mixed, f32[32,128]{1,0:T(8,128)S(1)} %collective-permute-done.prior, f32[1,128]{1,0:T(1,128)S(1)} %get-tuple-element.78.gain_part), custom_call_target="tpu_custom_call" | custom-call | flops 268435456 | bytes 1048576 | tf_op jit(solution)/shard_map/pallas_call | solution.py:316
  38.2 3.1 %collective-permute-start.22 = (f32[32,128]{1,0:T(8,128)S(1)}, f32[32,128]{1,0:T(8,128)S(1)}, u32[]{:S(2)}, u32[]{:S(2)}) collective-permute-start(f32[32,128]{1,0:T(8,128)S(1)} %shard_map.131), channel_id=1, source_target_pairs={{0,1},{1,0},{2,3},{3,2},{4,5},{5,4},{6,7},{7,6},{8,9},{9,8},{10,11... | collective-permute-start | bytes 49160 | tf_op jit(solution)/shard_map/ppermute | solution.py:502
  41.4 1.5 %shard_map.130 = (bf16[256,256]{1,0:T(8,128)(2,1)S(1)}, bf16[256,256]{1,0:T(8,128)(2,1)S(1)}, bf16[256,256]{1,0:T(8,128)(2,1)S(1)}, bf16[256,256]{1,0:T(8,128)(2,1)S(1)}) custom-call(bf16[1024,2048]{1,0:T(8,128)(2,1)S(1)} %copy-done.1, bf16[1024,128]{1,0:T(8,128)(2,1)S(1)} %get-tuple-element.72.activated, bf16[1024,128]{1,0:T(8,128)(2,1)S(1)} %collective-permute-done.18.other), custom_call_target="tpu_custom_call" | custom-call | flops 1073741824 | bytes 5242880 | tf_op jit(solution)/shard_map/pallas_call | solution.py:354
  42.9 1.9 %collective-permute-start.19 = (bf16[256,256]{1,0:T(8,128)(2,1)S(1)}, bf16[256,256]{1,0:T(8,128)(2,1)S(1)}, u32[]{:S(2)}, u32[]{:S(2)}) collective-permute-start(bf16[256,256]{1,0:T(8,128)(2,1)S(1)} %get-tuple-element.74), channel_id=1, source_target_pairs={{0,16},{8,24},{16,0},{24,8},{1,17},{9,25},{17,1},{25,9},{2,18},{10... | collective-permute-start | bytes 393224 | tf_op jit(solution)/shard_map/ppermute | solution.py:517
  44.7 4.0 %collective-permute-start.25 = (f32[32,256]{1,0:T(8,128)S(1)}, f32[32,256]{1,0:T(8,128)S(1)}, u32[]{:S(2)}, u32[]{:S(2)}) collective-permute-start(f32[32,256]{1,0:T(8,128)S(1)} %pad_maximum_fusion.refs_8_), channel_id=1, source_target_pairs={{0,24},{8,0},{16,8},{24,16},{1,25},{9,1},{17,9},{25,17},{2,26},{10... | collective-permute-start | bytes 98312 | tf_op jit(solution)/shard_map/ppermute | solution.py:517
  50.1 1.8 %collective-permute-start.23 = (f32[32,256]{1,0:T(8,128)S(1)}, f32[32,256]{1,0:T(8,128)S(1)}, u32[]{:S(2)}, u32[]{:S(2)}) collective-permute-start(f32[32,256]{1,0:T(8,128)S(1)} %pad_maximum_fusion.refs_8_), channel_id=1, source_target_pairs={{0,16},{8,24},{16,0},{24,8},{1,17},{9,25},{17,1},{25,9},{2,18},{10... | collective-permute-start | bytes 98312 | tf_op jit(solution)/shard_map/ppermute | solution.py:517
  51.9 1.6 %collective-permute-done.25.refs_11_ = f32[32,256]{1,0:T(8,128)S(1)} collective-permute-done((f32[32,256]{1,0:T(8,128)S(1)}, f32[32,256]{1,0:T(8,128)S(1)}, u32[]{:S(2)}, u32[]{:S(2)}) %collective-permute-start.25) | collective-permute-done | bytes 32800 | tf_op jit(solution)/shard_map/ppermute | solution.py:517
  53.9 2.3 %collective-permute-start.21 = (bf16[256,256]{1,0:T(8,128)(2,1)S(1)}, bf16[256,256]{1,0:T(8,128)(2,1)S(1)}, u32[]{:S(2)}, u32[]{:S(2)}) collective-permute-start(bf16[256,256]{1,0:T(8,128)(2,1)S(1)} %get-tuple-element.76), channel_id=1, source_target_pairs={{0,24},{8,0},{16,8},{24,16},{1,25},{9,1},{17,9},{25,17},{2,26},{10... | collective-permute-start | bytes 393224 | tf_op jit(solution)/shard_map/ppermute | solution.py:517
  58.7 1.8 %collective-permute-start.17 = (bf16[256,512]{1,0:T(8,128)(2,1)S(1)}, bf16[256,512]{1,0:T(8,128)(2,1)S(1)}, u32[]{:S(2)}, u32[]{:S(2)}) collective-permute-start(bf16[256,512]{1,0:T(8,128)(2,1)S(1)} %get-tuple-element.71), channel_id=1, source_target_pairs={{0,24},{8,0},{16,8},{24,16},{1,25},{9,1},{17,9},{25,17},{2,26},{10... | collective-permute-start | bytes 786440 | tf_op jit(solution)/shard_map/ppermute | solution.py:517
  61.1 1.4 %collective-permute-start.13 = (bf16[1024,256]{1,0:T(8,128)(2,1)S(1)}, bf16[1024,256]{1,0:T(8,128)(2,1)S(1)}, u32[]{:S(2)}, u32[]{:S(2)}) collective-permute-start(bf16[1024,256]{1,0:T(8,128)(2,1)S(1)} %shard_map.126), channel_id=1, source_target_pairs={{0,2},{1,7},{2,4},{3,1},{4,6},{5,3},{6,0},{7,5},{8,10},{9,15},{10,... | collective-permute-start | bytes 1572872 | tf_op jit(solution)/shard_map/ppermute | solution.py:512
  62.5 2.7 %collective-permute-done.15.refs_1_ = bf16[256,512]{1,0:T(8,128)(2,1)S(1)} collective-permute-done((bf16[256,512]{1,0:T(8,128)(2,1)S(1)}, bf16[256,512]{1,0:T(8,128)(2,1)S(1)}, u32[]{:S(2)}, u32[]{:S(2)}) %collective-permute-start.15) | collective-permute-done | bytes 262176 | tf_op jit(solution)/shard_map/ppermute | solution.py:517
  65.2 7.4 %collective-permute-done.16.refs_2_ = bf16[256,512]{1,0:T(8,128)(2,1)S(1)} collective-permute-done((bf16[256,512]{1,0:T(8,128)(2,1)S(1)}, bf16[256,512]{1,0:T(8,128)(2,1)S(1)}, u32[]{:S(2)}, u32[]{:S(2)}) %collective-permute-start.16) | collective-permute-done | bytes 262176 | tf_op jit(solution)/shard_map/ppermute | solution.py:517
  72.9 2.3 %collective-permute-start.29 = (bf16[448,128]{1,0:T(8,128)(2,1)S(1)}, bf16[448,128]{1,0:T(8,128)(2,1)S(1)}, u32[]{:S(2)}, u32[]{:S(2)}) collective-permute-start(bf16[448,128]{1,0:T(8,128)(2,1)S(1)} %get-tuple-element.82), channel_id=1, source_target_pairs={{0,96},{1,161},{32,128},{33,193},{64,160},{65,225},{96,192},{97,1}... | collective-permute-start | bytes 344072 | tf_op jit(solution)/shard_map/ppermute | solution.py:531
  75.2 3.6 %collective-permute-done.27.one = bf16[448,128]{1,0:T(8,128)(2,1)S(1)} collective-permute-done((bf16[448,128]{1,0:T(8,128)(2,1)S(1)}, bf16[448,128]{1,0:T(8,128)(2,1)S(1)}, u32[]{:S(2)}, u32[]{:S(2)}) %collective-permute-start.27) | collective-permute-done | bytes 114720 | tf_op jit(solution)/shard_map/ppermute | solution.py:531
  79.5 2.4 %collective-permute-done.28.two = bf16[448,128]{1,0:T(8,128)(2,1)S(1)} collective-permute-done((bf16[448,128]{1,0:T(8,128)(2,1)S(1)}, bf16[448,128]{1,0:T(8,128)(2,1)S(1)}, u32[]{:S(2)}, u32[]{:S(2)}) %collective-permute-start.28) | collective-permute-done | bytes 114720 | tf_op jit(solution)/shard_map/ppermute | solution.py:531
  81.9 1.5 %collective-permute-done.29.three = bf16[448,128]{1,0:T(8,128)(2,1)S(1)} collective-permute-done((bf16[448,128]{1,0:T(8,128)(2,1)S(1)}, bf16[448,128]{1,0:T(8,128)(2,1)S(1)}, u32[]{:S(2)}, u32[]{:S(2)}) %collective-permute-start.29) | collective-permute-done | bytes 114720 | tf_op jit(solution)/shard_map/ppermute | solution.py:531
  83.5 8.4 %collective-permute-start.30 = (f32[224,128]{1,0:T(8,128)S(1)}, f32[224,128]{1,0:T(8,128)S(1)}, u32[]{:S(2)}, u32[]{:S(2)}) collective-permute-start(f32[224,128]{1,0:T(8,128)S(1)} %get-tuple-element.84), channel_id=1, source_target_pairs={{0,1},{1,0},{2,3},{3,2},{4,5},{5,4},{6,7},{7,6},{8,9},{9,8},{10,11... | collective-permute-start | bytes 344072 | tf_op jit(solution)/shard_map/ppermute | solution.py:502
  93.5 1.3 %shard_map.127 = bf16[1024,256]{1,0:T(8,128)(2,1)} custom-call(bf16[1024,256]{1,0:T(8,128)(2,1)S(1)} %get-tuple-element.64.slopes, bf16[1024,256]{1,0:T(8,128)(2,1)S(1)} %collective-permute-done.10.others, bf16[2048,256]{1,0:T(8,128)(2,1)S(1)} %get-tuple-element.48.both, bf16[1024,256]{1,0:T(8,128)(2,1)S(1)} %collective-permute-done.11.lent, ...), custom_call_target="tpu_custom_call" | custom-call | flops 1073741824 | bytes 2097152 | tf_op jit(solution)/shard_map/pallas_call | solution.py:487
  (58 shorter events, 15.1 us)
Async XLA Ops:
  2.8 16.8 %copy-start.1 = (bf16[1024,2048]{1,0:T(8,128)(2,1)S(1)}, bf16[1024,2048]{1,0:T(8,128)(2,1)}, u32[]{:S(2)}) copy-start(bf16[1024,2048]{1,0:T(8,128)(2,1)} %rows.11) | copy-start | bytes 12582916
  2.8 10.6 %collective-permute-start = (f32[32,128]{1,0:T(8,128)S(1)}, f32[32,128]{1,0:T(8,128)S(1)}, u32[]{:S(2)}, u32[]{:S(2)}) collective-permute-start(f32[32,128]{1,0:T(8,128)S(1)} %get-tuple-element.51), channel_id=1, source_target_pairs={{0,8},{8,16},{16,24},{24,32},{32,40},{40,48},{48,56},{56,64},{64,7... | collective-permute-start | bytes 49160 | tf_op jit(solution)/shard_map/ppermute | solution.py:497
  6.3 7.1 %collective-permute-start.1 = (f32[64,128]{1,0:T(8,128)S(1)}, f32[64,128]{1,0:T(8,128)S(1)}, u32[]{:S(2)}, u32[]{:S(2)}) collective-permute-start(f32[64,128]{1,0:T(8,128)S(1)} %get-tuple-element.52), channel_id=1, source_target_pairs={{8,0},{16,8},{24,16},{32,24},{40,32},{48,40},{56,48},{64,56},{72,6... | collective-permute-start | bytes 98312 | tf_op jit(solution)/shard_map/ppermute | solution.py:497
  13.6 2.2 %collective-permute-start.2 = (f32[2,1056]{1,0:T(2,128)S(1)}, f32[2,1056]{1,0:T(2,128)S(1)}, u32[]{:S(2)}, u32[]{:S(2)}) collective-permute-start(f32[2,1056]{1,0:T(2,128)S(1)} %get-tuple-element.57), channel_id=1, source_target_pairs={{0,1},{1,0},{2,3},{3,2},{4,5},{5,4},{6,7},{7,6},{8,9},{9,8},{10,11... | collective-permute-start | bytes 25352 | tf_op jit(solution)/shard_map/ppermute | solution.py:502
  15.8 5.8 %collective-permute-start.5 = (f32[2,1056]{1,0:T(2,128)S(1)}, f32[2,1056]{1,0:T(2,128)S(1)}, u32[]{:S(2)}, u32[]{:S(2)}) collective-permute-start(f32[2,1056]{1,0:T(2,128)S(1)} %add.6.s0), channel_id=1, source_target_pairs={{0,4},{1,5},{2,6},{3,7},{4,0},{5,1},{6,2},{7,3},{8,12},{9,13},{10,... | collective-permute-start | bytes 25352 | tf_op jit(solution)/shard_map/ppermute | solution.py:502
  16.9 4.6 %collective-permute-start.4 = (f32[2,1056]{1,0:T(2,128)S(1)}, f32[2,1056]{1,0:T(2,128)S(1)}, u32[]{:S(2)}, u32[]{:S(2)}) collective-permute-start(f32[2,1056]{1,0:T(2,128)S(1)} %add.6.s0), channel_id=1, source_target_pairs={{0,6},{1,7},{2,0},{3,1},{4,2},{5,3},{6,4},{7,5},{8,14},{9,15},{10,... | collective-permute-start | bytes 25352 | tf_op jit(solution)/shard_map/ppermute | solution.py:502
  16.9 4.7 %collective-permute-start.3 = (f32[2,1056]{1,0:T(2,128)S(1)}, f32[2,1056]{1,0:T(2,128)S(1)}, u32[]{:S(2)}, u32[]{:S(2)}) collective-permute-start(f32[2,1056]{1,0:T(2,128)S(1)} %add.6.s0), channel_id=1, source_target_pairs={{0,2},{1,3},{2,4},{3,5},{4,6},{5,7},{6,0},{7,1},{8,10},{9,11},{10,... | collective-permute-start | bytes 25352 | tf_op jit(solution)/shard_map/ppermute | solution.py:502
  22.5 2.1 %collective-permute-start.6 = (f32[2,1056]{1,0:T(2,128)S(1)}, f32[2,1056]{1,0:T(2,128)S(1)}, u32[]{:S(2)}, u32[]{:S(2)}) collective-permute-start(f32[2,1056]{1,0:T(2,128)S(1)} %get-tuple-element.61), channel_id=1, source_target_pairs={{0,1},{1,0},{2,3},{3,2},{4,5},{5,4},{6,7},{7,6},{8,9},{9,8},{10,11... | collective-permute-start | bytes 25352 | tf_op jit(solution)/shard_map/ppermute | solution.py:502
  24.6 5.6 %collective-permute-start.9 = (f32[2,1056]{1,0:T(2,128)S(1)}, f32[2,1056]{1,0:T(2,128)S(1)}, u32[]{:S(2)}, u32[]{:S(2)}) collective-permute-start(f32[2,1056]{1,0:T(2,128)S(1)} %add.7.s0), channel_id=1, source_target_pairs={{0,4},{1,5},{2,6},{3,7},{4,0},{5,1},{6,2},{7,3},{8,12},{9,13},{10,... | collective-permute-start | bytes 25352 | tf_op jit(solution)/shard_map/ppermute | solution.py:502
  26.4 3.9 %collective-permute-start.8 = (f32[2,1056]{1,0:T(2,128)S(1)}, f32[2,1056]{1,0:T(2,128)S(1)}, u32[]{:S(2)}, u32[]{:S(2)}) collective-permute-start(f32[2,1056]{1,0:T(2,128)S(1)} %add.7.s0), channel_id=1, source_target_pairs={{0,6},{1,7},{2,0},{3,1},{4,2},{5,3},{6,4},{7,5},{8,14},{9,15},{10,... | collective-permute-start | bytes 25352 | tf_op jit(solution)/shard_map/ppermute | solution.py:502
  27.8 2.5 %collective-permute-start.7 = (f32[2,1056]{1,0:T(2,128)S(1)}, f32[2,1056]{1,0:T(2,128)S(1)}, u32[]{:S(2)}, u32[]{:S(2)}) collective-permute-start(f32[2,1056]{1,0:T(2,128)S(1)} %add.7.s0), channel_id=1, source_target_pairs={{0,2},{1,3},{2,4},{3,5},{4,6},{5,7},{6,0},{7,1},{8,10},{9,11},{10,... | collective-permute-start | bytes 25352 | tf_op jit(solution)/shard_map/ppermute | solution.py:502
  29.0 5.4 %collective-permute-start.11 = (bf16[1024,256]{1,0:T(8,128)(2,1)S(1)}, bf16[1024,256]{1,0:T(8,128)(2,1)S(1)}, u32[]{:S(2)}, u32[]{:S(2)}) collective-permute-start(bf16[1024,256]{1,0:T(8,128)(2,1)S(1)} %get-tuple-element.65), channel_id=1, source_target_pairs={{0,1},{1,0},{2,3},{3,2},{4,5},{5,4},{6,7},{7,6},{8,9},{9,8},{10,11... | collective-permute-start | bytes 1572872 | tf_op jit(solution)/shard_map/ppermute | solution.py:502
  32.2 3.7 %collective-permute-start.10 = (bf16[1024,256]{1,0:T(8,128)(2,1)S(1)}, bf16[1024,256]{1,0:T(8,128)(2,1)S(1)}, u32[]{:S(2)}, u32[]{:S(2)}) collective-permute-start(bf16[1024,256]{1,0:T(8,128)(2,1)S(1)} %get-tuple-element.64.slopes), channel_id=1, source_target_pairs={{0,1},{1,0},{2,3},{3,2},{4,5},{5,4},{6,7},{7,6},{8,9},{9,8},{10,11... | collective-permute-start | bytes 1572872 | tf_op jit(solution)/shard_map/ppermute | solution.py:502
  34.4 7.0 %collective-permute-start.18 = (bf16[1024,128]{1,0:T(8,128)(2,1)S(1)}, bf16[1024,128]{1,0:T(8,128)(2,1)S(1)}, u32[]{:S(2)}, u32[]{:S(2)}) collective-permute-start(bf16[1024,128]{1,0:T(8,128)(2,1)S(1)} %get-tuple-element.72.activated), channel_id=1, source_target_pairs={{0,1},{1,0},{2,3},{3,2},{4,5},{5,4},{6,7},{7,6},{8,9},{9,8},{10,11... | collective-permute-start | bytes 786440 | tf_op jit(solution)/shard_map/ppermute | solution.py:502
  36.6 22.0 %collective-permute-start.12 = (bf16[1024,256]{1,0:T(8,128)(2,1)S(1)}, bf16[1024,256]{1,0:T(8,128)(2,1)S(1)}, u32[]{:S(2)}, u32[]{:S(2)}) collective-permute-start(bf16[1024,256]{1,0:T(8,128)(2,1)S(1)} %get-tuple-element.66), channel_id=1, source_target_pairs={{0,2},{1,7},{2,4},{3,1},{4,6},{5,3},{6,0},{7,5},{8,10},{9,15},{10,... | collective-permute-start | bytes 1572872 | tf_op jit(solution)/shard_map/ppermute | solution.py:512
  38.2 6.5 %collective-permute-start.22 = (f32[32,128]{1,0:T(8,128)S(1)}, f32[32,128]{1,0:T(8,128)S(1)}, u32[]{:S(2)}, u32[]{:S(2)}) collective-permute-start(f32[32,128]{1,0:T(8,128)S(1)} %shard_map.131), channel_id=1, source_target_pairs={{0,1},{1,0},{2,3},{3,2},{4,5},{5,4},{6,7},{7,6},{8,9},{9,8},{10,11... | collective-permute-start | bytes 49160 | tf_op jit(solution)/shard_map/ppermute | solution.py:502
  42.9 14.9 %collective-permute-start.19 = (bf16[256,256]{1,0:T(8,128)(2,1)S(1)}, bf16[256,256]{1,0:T(8,128)(2,1)S(1)}, u32[]{:S(2)}, u32[]{:S(2)}) collective-permute-start(bf16[256,256]{1,0:T(8,128)(2,1)S(1)} %get-tuple-element.74), channel_id=1, source_target_pairs={{0,16},{8,24},{16,0},{24,8},{1,17},{9,25},{17,1},{25,9},{2,18},{10... | collective-permute-start | bytes 393224 | tf_op jit(solution)/shard_map/ppermute | solution.py:517
  44.7 8.7 %collective-permute-start.25 = (f32[32,256]{1,0:T(8,128)S(1)}, f32[32,256]{1,0:T(8,128)S(1)}, u32[]{:S(2)}, u32[]{:S(2)}) collective-permute-start(f32[32,256]{1,0:T(8,128)S(1)} %pad_maximum_fusion.refs_8_), channel_id=1, source_target_pairs={{0,24},{8,0},{16,8},{24,16},{1,25},{9,1},{17,9},{25,17},{2,26},{10... | collective-permute-start | bytes 98312 | tf_op jit(solution)/shard_map/ppermute | solution.py:517
  48.7 5.2 %collective-permute-start.24 = (f32[32,256]{1,0:T(8,128)S(1)}, f32[32,256]{1,0:T(8,128)S(1)}, u32[]{:S(2)}, u32[]{:S(2)}) collective-permute-start(f32[32,256]{1,0:T(8,128)S(1)} %pad_maximum_fusion.refs_8_), channel_id=1, source_target_pairs={{0,8},{8,16},{16,24},{24,0},{1,9},{9,17},{17,25},{25,1},{2,10},{10... | collective-permute-start | bytes 98312 | tf_op jit(solution)/shard_map/ppermute | solution.py:517
  50.1 7.0 %collective-permute-start.23 = (f32[32,256]{1,0:T(8,128)S(1)}, f32[32,256]{1,0:T(8,128)S(1)}, u32[]{:S(2)}, u32[]{:S(2)}) collective-permute-start(f32[32,256]{1,0:T(8,128)S(1)} %pad_maximum_fusion.refs_8_), channel_id=1, source_target_pairs={{0,16},{8,24},{16,0},{24,8},{1,17},{9,25},{17,1},{25,9},{2,18},{10... | collective-permute-start | bytes 98312 | tf_op jit(solution)/shard_map/ppermute | solution.py:517
  53.5 7.5 %collective-permute-start.20 = (bf16[256,256]{1,0:T(8,128)(2,1)S(1)}, bf16[256,256]{1,0:T(8,128)(2,1)S(1)}, u32[]{:S(2)}, u32[]{:S(2)}) collective-permute-start(bf16[256,256]{1,0:T(8,128)(2,1)S(1)} %get-tuple-element.75), channel_id=1, source_target_pairs={{0,8},{8,16},{16,24},{24,0},{1,9},{9,17},{17,25},{25,1},{2,10},{10... | collective-permute-start | bytes 393224 | tf_op jit(solution)/shard_map/ppermute | solution.py:517
  53.9 7.2 %collective-permute-start.21 = (bf16[256,256]{1,0:T(8,128)(2,1)S(1)}, bf16[256,256]{1,0:T(8,128)(2,1)S(1)}, u32[]{:S(2)}, u32[]{:S(2)}) collective-permute-start(bf16[256,256]{1,0:T(8,128)(2,1)S(1)} %get-tuple-element.76), channel_id=1, source_target_pairs={{0,24},{8,0},{16,8},{24,16},{1,25},{9,1},{17,9},{25,17},{2,26},{10... | collective-permute-start | bytes 393224 | tf_op jit(solution)/shard_map/ppermute | solution.py:517
  57.1 8.1 %collective-permute-start.15 = (bf16[256,512]{1,0:T(8,128)(2,1)S(1)}, bf16[256,512]{1,0:T(8,128)(2,1)S(1)}, u32[]{:S(2)}, u32[]{:S(2)}) collective-permute-start(bf16[256,512]{1,0:T(8,128)(2,1)S(1)} %get-tuple-element.69), channel_id=1, source_target_pairs={{0,16},{8,24},{16,0},{24,8},{1,17},{9,25},{17,1},{25,9},{2,18},{10... | collective-permute-start | bytes 786440 | tf_op jit(solution)/shard_map/ppermute | solution.py:517
  57.8 14.8 %collective-permute-start.16 = (bf16[256,512]{1,0:T(8,128)(2,1)S(1)}, bf16[256,512]{1,0:T(8,128)(2,1)S(1)}, u32[]{:S(2)}, u32[]{:S(2)}) collective-permute-start(bf16[256,512]{1,0:T(8,128)(2,1)S(1)} %get-tuple-element.70), channel_id=1, source_target_pairs={{0,8},{8,16},{16,24},{24,0},{1,9},{9,17},{17,25},{25,1},{2,10},{10... | collective-permute-start | bytes 786440 | tf_op jit(solution)/shard_map/ppermute | solution.py:517
  58.7 13.9 %collective-permute-start.17 = (bf16[256,512]{1,0:T(8,128)(2,1)S(1)}, bf16[256,512]{1,0:T(8,128)(2,1)S(1)}, u32[]{:S(2)}, u32[]{:S(2)}) collective-permute-start(bf16[256,512]{1,0:T(8,128)(2,1)S(1)} %get-tuple-element.71), channel_id=1, source_target_pairs={{0,24},{8,0},{16,8},{24,16},{1,25},{9,1},{17,9},{25,17},{2,26},{10... | collective-permute-start | bytes 786440 | tf_op jit(solution)/shard_map/ppermute | solution.py:517
  61.0 32.5 %collective-permute-start.14 = (bf16[1024,256]{1,0:T(8,128)(2,1)S(1)}, bf16[1024,256]{1,0:T(8,128)(2,1)S(1)}, u32[]{:S(2)}, u32[]{:S(2)}) collective-permute-start(bf16[1024,256]{1,0:T(8,128)(2,1)S(1)} %get-tuple-element.67), channel_id=1, source_target_pairs={{0,6},{1,3},{2,0},{3,5},{4,2},{5,7},{6,4},{7,1},{8,14},{9,11},{10,... | collective-permute-start | bytes 1572872 | tf_op jit(solution)/shard_map/ppermute | solution.py:512
  61.1 32.4 %collective-permute-start.13 = (bf16[1024,256]{1,0:T(8,128)(2,1)S(1)}, bf16[1024,256]{1,0:T(8,128)(2,1)S(1)}, u32[]{:S(2)}, u32[]{:S(2)}) collective-permute-start(bf16[1024,256]{1,0:T(8,128)(2,1)S(1)} %shard_map.126), channel_id=1, source_target_pairs={{0,2},{1,7},{2,4},{3,1},{4,6},{5,3},{6,0},{7,5},{8,10},{9,15},{10,... | collective-permute-start | bytes 1572872 | tf_op jit(solution)/shard_map/ppermute | solution.py:512
  72.8 6.1 %collective-permute-start.27 = (bf16[448,128]{1,0:T(8,128)(2,1)S(1)}, bf16[448,128]{1,0:T(8,128)(2,1)S(1)}, u32[]{:S(2)}, u32[]{:S(2)}) collective-permute-start(bf16[448,128]{1,0:T(8,128)(2,1)S(1)} %get-tuple-element.80), channel_id=1, source_target_pairs={{0,32},{1,225},{32,64},{33,1},{64,96},{65,33},{96,128},{97,65},{12... | collective-permute-start | bytes 344072 | tf_op jit(solution)/shard_map/ppermute | solution.py:531
  72.9 9.1 %collective-permute-start.28 = (bf16[448,128]{1,0:T(8,128)(2,1)S(1)}, bf16[448,128]{1,0:T(8,128)(2,1)S(1)}, u32[]{:S(2)}, u32[]{:S(2)}) collective-permute-start(bf16[448,128]{1,0:T(8,128)(2,1)S(1)} %get-tuple-element.81), channel_id=1, source_target_pairs={{0,64},{1,193},{32,96},{33,225},{64,128},{65,1},{96,160},{97,33},{... | collective-permute-start | bytes 344072 | tf_op jit(solution)/shard_map/ppermute | solution.py:531
  72.9 10.4 %collective-permute-start.29 = (bf16[448,128]{1,0:T(8,128)(2,1)S(1)}, bf16[448,128]{1,0:T(8,128)(2,1)S(1)}, u32[]{:S(2)}, u32[]{:S(2)}) collective-permute-start(bf16[448,128]{1,0:T(8,128)(2,1)S(1)} %get-tuple-element.82), channel_id=1, source_target_pairs={{0,96},{1,161},{32,128},{33,193},{64,160},{65,225},{96,192},{97,1}... | collective-permute-start | bytes 344072 | tf_op jit(solution)/shard_map/ppermute | solution.py:531
  78.8 4.6 %collective-permute-start.26 = (bf16[448,128]{1,0:T(8,128)(2,1)S(1)}, bf16[448,128]{1,0:T(8,128)(2,1)S(1)}, u32[]{:S(2)}, u32[]{:S(2)}) collective-permute-start(bf16[448,128]{1,0:T(8,128)(2,1)S(1)} %get-tuple-element.79.mine), channel_id=1, source_target_pairs={{0,128},{32,160},{64,192},{96,224},{128,0},{160,32},{192,64},{224,... | collective-permute-start | bytes 344072 | tf_op jit(solution)/shard_map/ppermute | solution.py:531
  83.5 9.4 %collective-permute-start.30 = (f32[224,128]{1,0:T(8,128)S(1)}, f32[224,128]{1,0:T(8,128)S(1)}, u32[]{:S(2)}, u32[]{:S(2)}) collective-permute-start(f32[224,128]{1,0:T(8,128)S(1)} %get-tuple-element.84), channel_id=1, source_target_pairs={{0,1},{1,0},{2,3},{3,2},{4,5},{5,4},{6,7},{7,6},{8,9},{9,8},{10,11... | collective-permute-start | bytes 344072 | tf_op jit(solution)/shard_map/ppermute | solution.py:502
  (3 other events, 28.6 us)

commit v5 on v4

--- a/solution.py
+++ b/solution.py
@@ -1,3 +1,5 @@
+import functools
+
 import jax
 import jax.numpy as jnp
 from jax import lax
@@ -21,6 +23,9 @@
 SLOTS = NZ // NC
 PART = D // (NY * NC)
 CUT = D // (NY * NZ)
+HALF = PART // 2
+Y_ORDER = (2, 1, 3)
+Z_ORDER = (0, 3, 2, 1)
 PIECE = 3 * CUT + K + 1
 FLOOR = 0.1
 F32 = jnp.float32
@@ -330,12 +335,12 @@
 
 def across(rows, side, parts, lanes):
     step = D // NZ
-    for slot in range(SLOTS):
+    for i, slot in enumerate(Z_ORDER):
         at = pl.multiple_of(kept_by(slot) * step, step)
         part = lax.dot_general(
             rows[:, pl.ds(at, step)], side, (((0,), (0,)), ((), ())), preferred_element_type=F32
         )
-        parts[:, slot * CUT : (slot + 1) * CUT, lanes] = part.astype(BF16).reshape(NY, CUT, side.shape[1])
+        parts[:, i * CUT : (i + 1) * CUT, lanes] = part.astype(BF16).reshape(NY, CUT, side.shape[1])
 
 
 def along_y(by):
@@ -373,22 +378,30 @@
     )(block_input, slopes)
 
 
-def weight_grad_kernel(rows, others, own, *rest):
-    outs, parts = rest[:NY], rest[NY]
+def weight_grad_kernel(rows, others, own, taps_part, other_taps, *rest):
+    firsts, seconds, parts = rest[:NY], rest[NY : 2 * NY], rest[2 * NY]
     across(rows, others[...], parts, slice(0, 2 * W))
-    for by, out in enumerate(outs):
-        out[:, : 2 * W] = own[along_y(by)]
-        out[:, 2 * W :] = parts[along_y(by)]
-
-
-def weight_grad_of(block_input, others, own):
+    half = (K + 1) // 2
+    small = (taps_part[:half], taps_part[half:], other_taps[:half], other_taps[half:])
+    small = jnp.concatenate([part.astype(BF16) for part in small], axis=1)
+    for by in range(NY):
+        mine, theirs = own[along_y(by)], parts[along_y(by)]
+        firsts[by][:HALF, : 2 * W] = mine[:HALF]
+        firsts[by][:HALF, 2 * W :] = theirs[:HALF]
+        firsts[by][HALF:] = small
+        seconds[by][:, : 2 * W] = mine[HALF:]
+        seconds[by][:, 2 * W :] = theirs[HALF:]
+
+
+def weight_grad_of(block_input, others, own, taps_part, other_taps):
+    first = shape_of((HALF + (K + 1) // 2, 4 * W), BF16)
     return pl.pallas_call(
         weight_grad_kernel,
-        out_shape=[shape_of((PART, 4 * W), BF16)] * NY,
+        out_shape=[first] * NY + [shape_of((HALF, 4 * W), BF16)] * NY,
         scratch_shapes=[pltpu.VMEM((NY, PART, 2 * W), BF16)],
         compiler_params=params(12),
         cost_estimate=cost(2 * ROWS * D * 128, 5 * 1024 * 1024),
-    )(block_input, others, own)
+    )(block_input, others, own, taps_part, other_taps)
 
 
 def summed(parts):
@@ -398,25 +411,27 @@
     return total
 
 
-def middle_kernel(*refs):
+def middle_kernel(low, *refs):
     both, side, small, outs = refs[:NY], refs[NY : 2 * NY], refs[2 * NY : 3 * NY], refs[3 * NY :]
-    total = summed(both).astype(BF16)
-    outer = summed(side).astype(BF16)
-    tail = summed(small).astype(BF16)
-    for slot, out in enumerate(outs):
-        rows = slice(slot * CUT, (slot + 1) * CUT)
+    total = summed([part.at[:HALF] for part in both]).astype(BF16)
+    outer = summed([part.at[low : low + HALF] for part in side]).astype(BF16)
+    tail = summed([part.at[HALF:] for part in small]).astype(BF16)
+    half = (K + 1) // 2
+    for i, out in enumerate(outs):
+        rows = slice(i * CUT, (i + 1) * CUT)
         for core in range(NC):
             at, lane = core * PIECE, core * 2 * W
             out[at : at + CUT] = total[rows, lane : lane + W]
             out[at + CUT : at + 2 * CUT] = total[rows, lane + W : lane + 2 * W]
             out[at + 2 * CUT : at + 3 * CUT] = outer[rows, core * W : (core + 1) * W]
-            out[at + 3 * CUT : at + PIECE] = tail[:, core * W : (core + 1) * W]
-
-
-def middle_of(both, side, small):
-    return pl.pallas_call(
-        middle_kernel,
-        out_shape=[shape_of((NC * PIECE, W), BF16)] * SLOTS,
+            out[at + 3 * CUT : at + 3 * CUT + half] = tail[:, lane : lane + W]
+            out[at + 3 * CUT + half : at + PIECE] = tail[:, lane + W : lane + 2 * W]
+
+
+def middle_of(low, both, side, small):
+    return pl.pallas_call(
+        functools.partial(middle_kernel, low),
+        out_shape=[shape_of((NC * PIECE, W), BF16)] * 2,
         compiler_params=params(12),
         cost_estimate=cost(2 * ROWS * D, 2 * 1024 * 1024),
     )(*both, *side, *small)
@@ -549,9 +564,12 @@
     out_parts = spread(out_parts, "y", Y_ORDER)
     slopes, curve = adjoint_of(normed, norm_slope, inverse, back, conv_taps, sgate, factor)
     others = to_slot(slopes, 1)
+    taps_part = taps_of(curve, mixed, prior, gain_part)
+    other_taps = to_slot(taps_part, 1)
     own_parts = own_weight_grad_of(block_input, slopes)
-    both_parts = weight_grad_of(block_input, others, own_parts)
-    both_parts = spread(both_parts, "y", Y_ORDER)
+    halves = weight_grad_of(block_input, others, own_parts, taps_part, other_taps)
+    firsts = spread(halves[:NY], "y", Y_ORDER)
+    seconds = spread(halves[NY:], "y", Y_ORDER)
     lent = to_slot(lend, 1)
     sides = (slopes, others, both, lent)
     far, single = share_call(far_kernel, 2, 2, *sides)
@@ -559,20 +577,14 @@
     (near,) = share_call(near_kernel, 1, 1, *sides, arrived)
     near = along(near, 1)
     single = along(single, -1)
-    taps_part = taps_of(curve, mixed, prior, gain_part)
-    other_taps = to_slot(taps_part, 1)
-    small = spread([jnp.concatenate([taps_part, other_taps], axis=1)] * NY, "y", Y_ORDER)
-    parts = middle_of(both_parts, out_parts, small)
-    sent = {slot: to_keeper(parts[slot], slot) for slot in Z_ORDER}
+    parts = middle_of(0, firsts, out_parts, firsts)
+    parts += middle_of(HALF, seconds, out_parts, firsts)
+    sent = {slot: to_keeper(part, slot) for slot, part in zip(Z_ORDER, parts)}
     own, other = chip_of(parts[0], [sent[slot] for slot in range(SLOTS)])
     other = to_slot(other, 1)
     (input_grad,) = share_call(own_kernel, 1, 1, *sides, near, single)
     value_grad, gate_grad, out_grad, taps_grad, gain_grad = final_of(own, other)
     return (input_grad, value_grad, gate_grad, out_grad, taps_grad, gain_grad.reshape(W))
-
-
-Y_ORDER = (2, 1, 3)
-Z_ORDER = (0, 3, 2, 1)
 
 
 def solution(mesh):

time: 94.9 us -> 94.4 us (level)
  the two profiles are of different devices: /device:TPU:103 before, /device:TPU:7 now
where the time goes in v5:
time: 94.4 us; the launch traced here: 94.3 us
  starting transfers between devices  57.3 us (61%)
  waiting for transfers between devices  18.1 us (19%)
  Pallas kernels  18 us (19%)
    ppermute x13, starting transfers between devices, to_slot(): return lax.ppermute(value, TP, pairs)  26.2 us
    ppermute x9, starting transfers between devices, further(): lax.ppermute(value, axis, [(i, (i + by) % count) for i in range(count)])  14.5 us
    ppermute x4, starting transfers between devices, to_keeper(): return lax.ppermute(value, ('z', 'c'), pairs)  10.3 us
    ppermute x9, waiting for transfers between devices, further(): lax.ppermute(value, axis, [(i, (i + by) % count) for i in range(count)])  6.6 us
    ppermute x4, waiting for transfers between devices, to_keeper(): return lax.ppermute(value, ('z', 'c'), pairs)  5.59 us
    ppermute x13, waiting for transfers between devices, to_slot(): return lax.ppermute(value, TP, pairs)  5.45 us
    ppermute x2, starting transfers between devices, from_behind(): lax.ppermute(value, SP, [(i, i + by) for i in range(count) if 0 <= i + by...  4.76 us
    pallas_call x3, Pallas kernels, share_call(): pl.pallas_call(kernel, out_shape=[piece] * count, compiler_params=params(...  2.48 us
  transfers between devices with their start and end apart: 31, of which 11 were waited for; matrix products, arithmetic and copies ran while one was open for 0% of the time, Pallas kernels for 13%

profile of v5, /device:TPU:7, one launch (start us, length us, event | category | flops | bytes accessed | tf_op | source)
XLA Modules:
  0.0 94.3 jit_solution(12181650419801235916)
XLA Ops:
  0.6 2.2 %shard_map.118 = (f32[32,128]{1,0:T(8,128)S(1)}, f32[64,128]{1,0:T(8,128)S(1)}, bf16[2048,256]{1,0:T(8,128)(2,1)S(1)}, bf16[2048,128]{1,0:T(8,128)(2,1)S(1)}) custom-call(bf16[1024,2048]{1,0:T(8,128)(2,1)} %rows.10, bf16[1024,2048]{1,0:T(8,128)(2,1)} %rows.11, bf16[2048,128]{1,0:T(8,128)(2,1)} %value_proj.1, bf16[2048,128]{1,0:T(8,128)(2,1)} %gate_proj.1, ...), custom_call_target="tpu_custom_call" | custom-call | flops 100663296 | bytes 2097152 | tf_op jit(solution)/shard_map/pallas_call | solution.py:84
  2.8 3.5 %collective-permute-start = (f32[32,128]{1,0:T(8,128)S(1)}, f32[32,128]{1,0:T(8,128)S(1)}, u32[]{:S(2)}, u32[]{:S(2)}) collective-permute-start(f32[32,128]{1,0:T(8,128)S(1)} %get-tuple-element.55), channel_id=1, source_target_pairs={{0,8},{8,16},{16,24},{24,32},{32,40},{40,48},{48,56},{56,64},{64,7... | collective-permute-start | bytes 49160 | tf_op jit(solution)/shard_map/ppermute | solution.py:512
  6.3 1.3 %collective-permute-start.1 = (f32[64,128]{1,0:T(8,128)S(1)}, f32[64,128]{1,0:T(8,128)S(1)}, u32[]{:S(2)}, u32[]{:S(2)}) collective-permute-start(f32[64,128]{1,0:T(8,128)S(1)} %get-tuple-element.56), channel_id=1, source_target_pairs={{8,0},{16,8},{24,16},{32,24},{40,32},{48,40},{56,48},{64,56},{72,6... | collective-permute-start | bytes 98312 | tf_op jit(solution)/shard_map/ppermute | solution.py:512
  7.6 1.3 %shard_map.119 = (f32[1024,128]{1,0:T(8,128)S(1)}, f32[1024,128]{1,0:T(8,128)S(1)}, f32[1024,128]{1,0:T(8,128)S(1)}) custom-call(bf16[1024,2048]{1,0:T(8,128)(2,1)S(1)} %copy-done, bf16[2048,256]{1,0:T(8,128)(2,1)S(1)} %get-tuple-element.52.both), custom_call_target="tpu_custom_call" | custom-call | flops 1073741824 | bytes 7340032 | tf_op jit(solution)/shard_map/pallas_call | solution.py:111
  8.9 1.6 %shard_map.120 = (f32[1024,128]{1,0:T(8,128)S(1)}, f32[2,1024]{1,0:T(2,128)S(1)}) custom-call(f32[1024,128]{1,0:T(8,128)S(1)} %get-tuple-element.53.mixed, f32[31,128]{1,0:T(8,128)S(1)} %copy-done.2), custom_call_target="tpu_custom_call" | custom-call | flops 536870912 | bytes 2097152 | tf_op jit(solution)/shard_map/pallas_call | solution.py:191
  11.2 2.2 %collective-permute-start.2 = (f32[2,1056]{1,0:T(2,128)S(1)}, f32[2,1056]{1,0:T(2,128)S(1)}, u32[]{:S(2)}, u32[]{:S(2)}) collective-permute-start(f32[2,1056]{1,0:T(2,128)S(1)} %get-tuple-element.61), channel_id=1, source_target_pairs={{0,1},{1,0},{2,3},{3,2},{4,5},{5,4},{6,7},{7,6},{8,9},{9,8},{10,11... | collective-permute-start | bytes 25352 | tf_op jit(solution)/shard_map/ppermute | solution.py:517
  15.3 2.7 %collective-permute-start.3 = (f32[2,1056]{1,0:T(2,128)S(1)}, f32[2,1056]{1,0:T(2,128)S(1)}, u32[]{:S(2)}, u32[]{:S(2)}) collective-permute-start(f32[2,1056]{1,0:T(2,128)S(1)} %add.6.s0), channel_id=1, source_target_pairs={{0,2},{1,3},{2,4},{3,5},{4,6},{5,7},{6,0},{7,1},{8,10},{9,11},{10,... | collective-permute-start | bytes 25352 | tf_op jit(solution)/shard_map/ppermute | solution.py:517
  18.0 1.9 %shard_map.122 = (f32[1024,128]{1,0:T(8,128)S(1)}, bf16[1024,256]{1,0:T(8,128)(2,1)S(1)}) custom-call(bf16[1024,2048]{1,0:T(8,128)(2,1)S(1)} %copy-done.1, bf16[2048,128]{1,0:T(8,128)(2,1)S(1)} %get-tuple-element.59.out_side, bf16[2048,256]{1,0:T(8,128)(2,1)S(1)} %get-tuple-element.52.both), custom_call_target="tpu_custom_call" | custom-call | flops 1073741824 | bytes 5242880 | tf_op jit(solution)/shard_map/pallas_call | solution.py:137
  20.9 1.3 %collective-permute-start.6 = (f32[2,1056]{1,0:T(2,128)S(1)}, f32[2,1056]{1,0:T(2,128)S(1)}, u32[]{:S(2)}, u32[]{:S(2)}) collective-permute-start(f32[2,1056]{1,0:T(2,128)S(1)} %get-tuple-element.65), channel_id=1, source_target_pairs={{0,1},{1,0},{2,3},{3,2},{4,5},{5,4},{6,7},{7,6},{8,9},{9,8},{10,11... | collective-permute-start | bytes 25352 | tf_op jit(solution)/shard_map/ppermute | solution.py:517
  23.0 1.7 %collective-permute-start.9 = (f32[2,1056]{1,0:T(2,128)S(1)}, f32[2,1056]{1,0:T(2,128)S(1)}, u32[]{:S(2)}, u32[]{:S(2)}) collective-permute-start(f32[2,1056]{1,0:T(2,128)S(1)} %add.7.s0), channel_id=1, source_target_pairs={{0,4},{1,5},{2,6},{3,7},{4,0},{5,1},{6,2},{7,3},{8,12},{9,13},{10,... | collective-permute-start | bytes 25352 | tf_op jit(solution)/shard_map/ppermute | solution.py:517
  24.7 1.5 %collective-permute-start.8 = (f32[2,1056]{1,0:T(2,128)S(1)}, f32[2,1056]{1,0:T(2,128)S(1)}, u32[]{:S(2)}, u32[]{:S(2)}) collective-permute-start(f32[2,1056]{1,0:T(2,128)S(1)} %add.7.s0), channel_id=1, source_target_pairs={{0,6},{1,7},{2,0},{3,1},{4,2},{5,3},{6,4},{7,5},{8,14},{9,15},{10,... | collective-permute-start | bytes 25352 | tf_op jit(solution)/shard_map/ppermute | solution.py:517
  28.7 1.9 %shard_map.124 = (bf16[1024,256]{1,0:T(8,128)(2,1)S(1)}, f32[1056,128]{1,0:T(8,128)S(1)}) custom-call(f32[1056,128]{1,0:T(8,128)S(1)} %get-tuple-element.62.normed, f32[1056,128]{1,0:T(8,128)S(1)} %get-tuple-element.63.norm_slope, f32[1056,128]{1,0:T(8,128)S(1)} %get-tuple-element.64.inverse, f32[2,1056]{1,0:T(2,128)S(1)} %add.7.s0, ...), custom_call_target="tpu_custom_call" | custom-call | flops 1073741824 | bytes 2097152 | tf_op jit(solution)/shard_map/pallas_call | solution.py:287
  30.6 2.1 %collective-permute-start.10 = (bf16[1024,256]{1,0:T(8,128)(2,1)S(1)}, bf16[1024,256]{1,0:T(8,128)(2,1)S(1)}, u32[]{:S(2)}, u32[]{:S(2)}) collective-permute-start(bf16[1024,256]{1,0:T(8,128)(2,1)S(1)} %get-tuple-element.68.slopes), channel_id=1, source_target_pairs={{0,1},{1,0},{2,3},{3,2},{4,5},{5,4},{6,7},{7,6},{8,9},{9,8},{10,11... | collective-permute-start | bytes 1572872 | tf_op jit(solution)/shard_map/ppermute | solution.py:517
  32.7 1.5 %collective-permute-done.10.others = bf16[1024,256]{1,0:T(8,128)(2,1)S(1)} collective-permute-done((bf16[1024,256]{1,0:T(8,128)(2,1)S(1)}, bf16[1024,256]{1,0:T(8,128)(2,1)S(1)}, u32[]{:S(2)}, u32[]{:S(2)}) %collective-permute-start.10) | collective-permute-done | bytes 524320 | tf_op jit(solution)/shard_map/ppermute | solution.py:517
  35.1 3.1 %collective-permute-start.19 = (bf16[1024,128]{1,0:T(8,128)(2,1)S(1)}, bf16[1024,128]{1,0:T(8,128)(2,1)S(1)}, u32[]{:S(2)}, u32[]{:S(2)}) collective-permute-start(bf16[1024,128]{1,0:T(8,128)(2,1)S(1)} %get-tuple-element.78.activated), channel_id=1, source_target_pairs={{0,1},{1,0},{2,3},{3,2},{4,5},{5,4},{6,7},{7,6},{8,9},{9,8},{10,11... | collective-permute-start | bytes 786440 | tf_op jit(solution)/shard_map/ppermute | solution.py:517
  39.3 1.5 %shard_map.131 = (bf16[256,256]{1,0:T(8,128)(2,1)S(1)}, bf16[256,256]{1,0:T(8,128)(2,1)S(1)}, bf16[256,256]{1,0:T(8,128)(2,1)S(1)}, bf16[256,256]{1,0:T(8,128)(2,1)S(1)}) custom-call(bf16[1024,2048]{1,0:T(8,128)(2,1)S(1)} %copy-done.1, bf16[1024,128]{1,0:T(8,128)(2,1)S(1)} %get-tuple-element.78.activated, bf16[1024,128]{1,0:T(8,128)(2,1)S(1)} %collective-permute-done.19.other), custom_call_target="tpu_custom_call" | custom-call | flops 1073741824 | bytes 5242880 | tf_op jit(solution)/shard_map/pallas_call | solution.py:359
  40.8 2.7 %collective-permute-start.20 = (bf16[256,256]{1,0:T(8,128)(2,1)S(1)}, bf16[256,256]{1,0:T(8,128)(2,1)S(1)}, u32[]{:S(2)}, u32[]{:S(2)}) collective-permute-start(bf16[256,256]{1,0:T(8,128)(2,1)S(1)} %get-tuple-element.80), channel_id=1, source_target_pairs={{0,16},{8,24},{16,0},{24,8},{1,17},{9,25},{17,1},{25,9},{2,18},{10... | collective-permute-start | bytes 393224 | tf_op jit(solution)/shard_map/ppermute | solution.py:532
  43.5 1.3 %shard_map.129.taps_part = f32[32,128]{1,0:T(8,128)S(1)} custom-call(f32[1056,128]{1,0:T(8,128)S(1)} %get-tuple-element.72.curve, f32[1024,128]{1,0:T(8,128)S(1)} %get-tuple-element.53.mixed, f32[32,128]{1,0:T(8,128)S(1)} %collective-permute-done.prior, f32[1,128]{1,0:T(1,128)S(1)} %get-tuple-element.73.gain_part), custom_call_target="tpu_custom_call" | custom-call | flops 268435456 | bytes 1048576 | tf_op jit(solution)/shard_map/pallas_call | solution.py:321
  46.4 2.9 %collective-permute-start.21 = (bf16[256,256]{1,0:T(8,128)(2,1)S(1)}, bf16[256,256]{1,0:T(8,128)(2,1)S(1)}, u32[]{:S(2)}, u32[]{:S(2)}) collective-permute-start(bf16[256,256]{1,0:T(8,128)(2,1)S(1)} %get-tuple-element.81), channel_id=1, source_target_pairs={{0,8},{8,16},{16,24},{24,0},{1,9},{9,17},{17,25},{25,1},{2,10},{10... | collective-permute-start | bytes 393224 | tf_op jit(solution)/shard_map/ppermute | solution.py:532
  50.3 1.9 %collective-permute-start.24 = (bf16[128,512]{1,0:T(8,128)(2,1)S(1)}, bf16[128,512]{1,0:T(8,128)(2,1)S(1)}, u32[]{:S(2)}, u32[]{:S(2)}) collective-permute-start(bf16[128,512]{1,0:T(8,128)(2,1)S(1)} %get-tuple-element.85), channel_id=1, source_target_pairs={{0,16},{8,24},{16,0},{24,8},{1,17},{9,25},{17,1},{25,9},{2,18},{10... | collective-permute-start | bytes 393224 | tf_op jit(solution)/shard_map/ppermute | solution.py:532
  52.2 2.7 %collective-permute-start.26 = (bf16[128,512]{1,0:T(8,128)(2,1)S(1)}, bf16[128,512]{1,0:T(8,128)(2,1)S(1)}, u32[]{:S(2)}, u32[]{:S(2)}) collective-permute-start(bf16[128,512]{1,0:T(8,128)(2,1)S(1)} %get-tuple-element.87), channel_id=1, source_target_pairs={{0,24},{8,0},{16,8},{24,16},{1,25},{9,1},{17,9},{25,17},{2,26},{10... | collective-permute-start | bytes 393224 | tf_op jit(solution)/shard_map/ppermute | solution.py:532
  55.5 1.4 %collective-permute-start.13 = (bf16[1024,256]{1,0:T(8,128)(2,1)S(1)}, bf16[1024,256]{1,0:T(8,128)(2,1)S(1)}, u32[]{:S(2)}, u32[]{:S(2)}) collective-permute-start(bf16[1024,256]{1,0:T(8,128)(2,1)S(1)} %shard_map.126), channel_id=1, source_target_pairs={{0,2},{1,7},{2,4},{3,1},{4,6},{5,3},{6,0},{7,5},{8,10},{9,15},{10,... | collective-permute-start | bytes 1572872 | tf_op jit(solution)/shard_map/ppermute | solution.py:527
  56.9 1.6 %collective-permute-start.16 = (bf16[144,512]{1,0:T(8,128)(2,1)S(1)}, bf16[144,512]{1,0:T(8,128)(2,1)S(1)}, u32[]{:S(2)}, u32[]{:S(2)}) collective-permute-start(bf16[144,512]{1,0:T(8,128)(2,1)S(1)} %get-tuple-element.75), channel_id=1, source_target_pairs={{0,16},{8,24},{16,0},{24,8},{1,17},{9,25},{17,1},{25,9},{2,18},{10... | collective-permute-start | bytes 442376 | tf_op jit(solution)/shard_map/ppermute | solution.py:532
  58.5 1.4 %collective-permute-done.25.refs_2_ = bf16[128,512]{1,0:T(8,128)(2,1)S(1)} collective-permute-done((bf16[128,512]{1,0:T(8,128)(2,1)S(1)}, bf16[128,512]{1,0:T(8,128)(2,1)S(1)}, u32[]{:S(2)}, u32[]{:S(2)}) %collective-permute-start.25) | collective-permute-done | bytes 131104 | tf_op jit(solution)/shard_map/ppermute | solution.py:532
  59.9 2.7 %collective-permute-start.18 = (bf16[144,512]{1,0:T(8,128)(2,1)S(1)}, bf16[144,512]{1,0:T(8,128)(2,1)S(1)}, u32[]{:S(2)}, u32[]{:S(2)}) collective-permute-start(bf16[144,512]{1,0:T(8,128)(2,1)S(1)} %get-tuple-element.77), channel_id=1, source_target_pairs={{0,24},{8,0},{16,8},{24,16},{1,25},{9,1},{17,9},{25,17},{2,26},{10... | collective-permute-start | bytes 442376 | tf_op jit(solution)/shard_map/ppermute | solution.py:532
  62.6 5.2 %collective-permute-done.17.refs_2_.refs_10_ = bf16[144,512]{1,0:T(8,128)(2,1)S(1)} collective-permute-done((bf16[144,512]{1,0:T(8,128)(2,1)S(1)}, bf16[144,512]{1,0:T(8,128)(2,1)S(1)}, u32[]{:S(2)}, u32[]{:S(2)}) %collective-permute-start.17) | collective-permute-done | bytes 147488 | tf_op jit(solution)/shard_map/ppermute | solution.py:532
  67.9 6.3 %collective-permute-start.27 = (bf16[448,128]{1,0:T(8,128)(2,1)S(1)}, bf16[448,128]{1,0:T(8,128)(2,1)S(1)}, u32[]{:S(2)}, u32[]{:S(2)}) collective-permute-start(bf16[448,128]{1,0:T(8,128)(2,1)S(1)} %get-tuple-element.88), channel_id=1, source_target_pairs={{0,32},{1,225},{32,64},{33,1},{64,96},{65,33},{96,128},{97,65},{12... | collective-permute-start | bytes 344072 | tf_op jit(solution)/shard_map/ppermute | solution.py:546
  75.5 2.1 %collective-permute-start.29 = (bf16[448,128]{1,0:T(8,128)(2,1)S(1)}, bf16[448,128]{1,0:T(8,128)(2,1)S(1)}, u32[]{:S(2)}, u32[]{:S(2)}) collective-permute-start(bf16[448,128]{1,0:T(8,128)(2,1)S(1)} %get-tuple-element.90), channel_id=1, source_target_pairs={{0,96},{1,161},{32,128},{33,193},{64,160},{65,225},{96,192},{97,1}... | collective-permute-start | bytes 344072 | tf_op jit(solution)/shard_map/ppermute | solution.py:546
  78.3 1.6 %collective-permute-done.28.two = bf16[448,128]{1,0:T(8,128)(2,1)S(1)} collective-permute-done((bf16[448,128]{1,0:T(8,128)(2,1)S(1)}, bf16[448,128]{1,0:T(8,128)(2,1)S(1)}, u32[]{:S(2)}, u32[]{:S(2)}) %collective-permute-start.28) | collective-permute-done | bytes 114720 | tf_op jit(solution)/shard_map/ppermute | solution.py:546
  79.9 4.0 %collective-permute-done.29.three = bf16[448,128]{1,0:T(8,128)(2,1)S(1)} collective-permute-done((bf16[448,128]{1,0:T(8,128)(2,1)S(1)}, bf16[448,128]{1,0:T(8,128)(2,1)S(1)}, u32[]{:S(2)}, u32[]{:S(2)}) %collective-permute-start.29) | collective-permute-done | bytes 114720 | tf_op jit(solution)/shard_map/ppermute | solution.py:546
  84.0 7.4 %collective-permute-start.30 = (f32[224,128]{1,0:T(8,128)S(1)}, f32[224,128]{1,0:T(8,128)S(1)}, u32[]{:S(2)}, u32[]{:S(2)}) collective-permute-start(f32[224,128]{1,0:T(8,128)S(1)} %get-tuple-element.92), channel_id=1, source_target_pairs={{0,1},{1,0},{2,3},{3,2},{4,5},{5,4},{6,7},{7,6},{8,9},{9,8},{10,11... | collective-permute-start | bytes 344072 | tf_op jit(solution)/shard_map/ppermute | solution.py:517
  93.0 1.3 %shard_map.127 = bf16[1024,256]{1,0:T(8,128)(2,1)} custom-call(bf16[1024,256]{1,0:T(8,128)(2,1)S(1)} %get-tuple-element.68.slopes, bf16[1024,256]{1,0:T(8,128)(2,1)S(1)} %collective-permute-done.10.others, bf16[2048,256]{1,0:T(8,128)(2,1)S(1)} %get-tuple-element.52.both, bf16[1024,256]{1,0:T(8,128)(2,1)S(1)} %collective-permute-done.11.lent, ...), custom_call_target="tpu_custom_call" | custom-call | flops 1073741824 | bytes 2097152 | tf_op jit(solution)/shard_map/pallas_call | solution.py:502
  (58 shorter events, 15.7 us)
Async XLA Ops:
  2.8 15.2 %copy-start.1 = (bf16[1024,2048]{1,0:T(8,128)(2,1)S(1)}, bf16[1024,2048]{1,0:T(8,128)(2,1)}, u32[]{:S(2)}) copy-start(bf16[1024,2048]{1,0:T(8,128)(2,1)} %rows.11) | copy-start | bytes 12582916
  2.8 7.7 %collective-permute-start = (f32[32,128]{1,0:T(8,128)S(1)}, f32[32,128]{1,0:T(8,128)S(1)}, u32[]{:S(2)}, u32[]{:S(2)}) collective-permute-start(f32[32,128]{1,0:T(8,128)S(1)} %get-tuple-element.55), channel_id=1, source_target_pairs={{0,8},{8,16},{16,24},{24,32},{32,40},{40,48},{48,56},{56,64},{64,7... | collective-permute-start | bytes 49160 | tf_op jit(solution)/shard_map/ppermute | solution.py:512
  6.3 4.7 %collective-permute-start.1 = (f32[64,128]{1,0:T(8,128)S(1)}, f32[64,128]{1,0:T(8,128)S(1)}, u32[]{:S(2)}, u32[]{:S(2)}) collective-permute-start(f32[64,128]{1,0:T(8,128)S(1)} %get-tuple-element.56), channel_id=1, source_target_pairs={{8,0},{16,8},{24,16},{32,24},{40,32},{48,40},{56,48},{64,56},{72,6... | collective-permute-start | bytes 98312 | tf_op jit(solution)/shard_map/ppermute | solution.py:512
  11.2 3.0 %collective-permute-start.2 = (f32[2,1056]{1,0:T(2,128)S(1)}, f32[2,1056]{1,0:T(2,128)S(1)}, u32[]{:S(2)}, u32[]{:S(2)}) collective-permute-start(f32[2,1056]{1,0:T(2,128)S(1)} %get-tuple-element.61), channel_id=1, source_target_pairs={{0,1},{1,0},{2,3},{3,2},{4,5},{5,4},{6,7},{7,6},{8,9},{9,8},{10,11... | collective-permute-start | bytes 25352 | tf_op jit(solution)/shard_map/ppermute | solution.py:517
  14.2 5.8 %collective-permute-start.5 = (f32[2,1056]{1,0:T(2,128)S(1)}, f32[2,1056]{1,0:T(2,128)S(1)}, u32[]{:S(2)}, u32[]{:S(2)}) collective-permute-start(f32[2,1056]{1,0:T(2,128)S(1)} %add.6.s0), channel_id=1, source_target_pairs={{0,4},{1,5},{2,6},{3,7},{4,0},{5,1},{6,2},{7,3},{8,12},{9,13},{10,... | collective-permute-start | bytes 25352 | tf_op jit(solution)/shard_map/ppermute | solution.py:517
  15.3 4.6 %collective-permute-start.4 = (f32[2,1056]{1,0:T(2,128)S(1)}, f32[2,1056]{1,0:T(2,128)S(1)}, u32[]{:S(2)}, u32[]{:S(2)}) collective-permute-start(f32[2,1056]{1,0:T(2,128)S(1)} %add.6.s0), channel_id=1, source_target_pairs={{0,6},{1,7},{2,0},{3,1},{4,2},{5,3},{6,4},{7,5},{8,14},{9,15},{10,... | collective-permute-start | bytes 25352 | tf_op jit(solution)/shard_map/ppermute | solution.py:517
  15.3 4.6 %collective-permute-start.3 = (f32[2,1056]{1,0:T(2,128)S(1)}, f32[2,1056]{1,0:T(2,128)S(1)}, u32[]{:S(2)}, u32[]{:S(2)}) collective-permute-start(f32[2,1056]{1,0:T(2,128)S(1)} %add.6.s0), channel_id=1, source_target_pairs={{0,2},{1,3},{2,4},{3,5},{4,6},{5,7},{6,0},{7,1},{8,10},{9,11},{10,... | collective-permute-start | bytes 25352 | tf_op jit(solution)/shard_map/ppermute | solution.py:517
  20.9 2.1 %collective-permute-start.6 = (f32[2,1056]{1,0:T(2,128)S(1)}, f32[2,1056]{1,0:T(2,128)S(1)}, u32[]{:S(2)}, u32[]{:S(2)}) collective-permute-start(f32[2,1056]{1,0:T(2,128)S(1)} %get-tuple-element.65), channel_id=1, source_target_pairs={{0,1},{1,0},{2,3},{3,2},{4,5},{5,4},{6,7},{7,6},{8,9},{9,8},{10,11... | collective-permute-start | bytes 25352 | tf_op jit(solution)/shard_map/ppermute | solution.py:517
  23.0 5.6 %collective-permute-start.9 = (f32[2,1056]{1,0:T(2,128)S(1)}, f32[2,1056]{1,0:T(2,128)S(1)}, u32[]{:S(2)}, u32[]{:S(2)}) collective-permute-start(f32[2,1056]{1,0:T(2,128)S(1)} %add.7.s0), channel_id=1, source_target_pairs={{0,4},{1,5},{2,6},{3,7},{4,0},{5,1},{6,2},{7,3},{8,12},{9,13},{10,... | collective-permute-start | bytes 25352 | tf_op jit(solution)/shard_map/ppermute | solution.py:517
  24.7 3.9 %collective-permute-start.8 = (f32[2,1056]{1,0:T(2,128)S(1)}, f32[2,1056]{1,0:T(2,128)S(1)}, u32[]{:S(2)}, u32[]{:S(2)}) collective-permute-start(f32[2,1056]{1,0:T(2,128)S(1)} %add.7.s0), channel_id=1, source_target_pairs={{0,6},{1,7},{2,0},{3,1},{4,2},{5,3},{6,4},{7,5},{8,14},{9,15},{10,... | collective-permute-start | bytes 25352 | tf_op jit(solution)/shard_map/ppermute | solution.py:517
  26.2 2.5 %collective-permute-start.7 = (f32[2,1056]{1,0:T(2,128)S(1)}, f32[2,1056]{1,0:T(2,128)S(1)}, u32[]{:S(2)}, u32[]{:S(2)}) collective-permute-start(f32[2,1056]{1,0:T(2,128)S(1)} %add.7.s0), channel_id=1, source_target_pairs={{0,2},{1,3},{2,4},{3,5},{4,6},{5,7},{6,0},{7,1},{8,10},{9,11},{10,... | collective-permute-start | bytes 25352 | tf_op jit(solution)/shard_map/ppermute | solution.py:517
  27.4 5.3 %collective-permute-start.11 = (bf16[1024,256]{1,0:T(8,128)(2,1)S(1)}, bf16[1024,256]{1,0:T(8,128)(2,1)S(1)}, u32[]{:S(2)}, u32[]{:S(2)}) collective-permute-start(bf16[1024,256]{1,0:T(8,128)(2,1)S(1)} %get-tuple-element.69), channel_id=1, source_target_pairs={{0,1},{1,0},{2,3},{3,2},{4,5},{5,4},{6,7},{7,6},{8,9},{9,8},{10,11... | collective-permute-start | bytes 1572872 | tf_op jit(solution)/shard_map/ppermute | solution.py:517
  30.6 3.7 %collective-permute-start.10 = (bf16[1024,256]{1,0:T(8,128)(2,1)S(1)}, bf16[1024,256]{1,0:T(8,128)(2,1)S(1)}, u32[]{:S(2)}, u32[]{:S(2)}) collective-permute-start(bf16[1024,256]{1,0:T(8,128)(2,1)S(1)} %get-tuple-element.68.slopes), channel_id=1, source_target_pairs={{0,1},{1,0},{2,3},{3,2},{4,5},{5,4},{6,7},{7,6},{8,9},{9,8},{10,11... | collective-permute-start | bytes 1572872 | tf_op jit(solution)/shard_map/ppermute | solution.py:517
  35.0 17.2 %collective-permute-start.12 = (bf16[1024,256]{1,0:T(8,128)(2,1)S(1)}, bf16[1024,256]{1,0:T(8,128)(2,1)S(1)}, u32[]{:S(2)}, u32[]{:S(2)}) collective-permute-start(bf16[1024,256]{1,0:T(8,128)(2,1)S(1)} %get-tuple-element.70), channel_id=1, source_target_pairs={{0,2},{1,7},{2,4},{3,1},{4,6},{5,3},{6,0},{7,5},{8,10},{9,15},{10,... | collective-permute-start | bytes 1572872 | tf_op jit(solution)/shard_map/ppermute | solution.py:527
  35.1 4.2 %collective-permute-start.19 = (bf16[1024,128]{1,0:T(8,128)(2,1)S(1)}, bf16[1024,128]{1,0:T(8,128)(2,1)S(1)}, u32[]{:S(2)}, u32[]{:S(2)}) collective-permute-start(bf16[1024,128]{1,0:T(8,128)(2,1)S(1)} %get-tuple-element.78.activated), channel_id=1, source_target_pairs={{0,1},{1,0},{2,3},{3,2},{4,5},{5,4},{6,7},{7,6},{8,9},{9,8},{10,11... | collective-permute-start | bytes 786440 | tf_op jit(solution)/shard_map/ppermute | solution.py:517
  40.8 11.4 %collective-permute-start.20 = (bf16[256,256]{1,0:T(8,128)(2,1)S(1)}, bf16[256,256]{1,0:T(8,128)(2,1)S(1)}, u32[]{:S(2)}, u32[]{:S(2)}) collective-permute-start(bf16[256,256]{1,0:T(8,128)(2,1)S(1)} %get-tuple-element.80), channel_id=1, source_target_pairs={{0,16},{8,24},{16,0},{24,8},{1,17},{9,25},{17,1},{25,9},{2,18},{10... | collective-permute-start | bytes 393224 | tf_op jit(solution)/shard_map/ppermute | solution.py:532
  44.8 4.5 %collective-permute-start.15 = (f32[32,128]{1,0:T(8,128)S(1)}, f32[32,128]{1,0:T(8,128)S(1)}, u32[]{:S(2)}, u32[]{:S(2)}) collective-permute-start(f32[32,128]{1,0:T(8,128)S(1)} %shard_map.129.taps_part), channel_id=1, source_target_pairs={{0,1},{1,0},{2,3},{3,2},{4,5},{5,4},{6,7},{7,6},{8,9},{9,8},{10,11... | collective-permute-start | bytes 49160 | tf_op jit(solution)/shard_map/ppermute | solution.py:517
  46.4 9.0 %collective-permute-start.21 = (bf16[256,256]{1,0:T(8,128)(2,1)S(1)}, bf16[256,256]{1,0:T(8,128)(2,1)S(1)}, u32[]{:S(2)}, u32[]{:S(2)}) collective-permute-start(bf16[256,256]{1,0:T(8,128)(2,1)S(1)} %get-tuple-element.81), channel_id=1, source_target_pairs={{0,8},{8,16},{16,24},{24,0},{1,9},{9,17},{17,25},{25,1},{2,10},{10... | collective-permute-start | bytes 393224 | tf_op jit(solution)/shard_map/ppermute | solution.py:532
  49.3 6.2 %collective-permute-start.22 = (bf16[256,256]{1,0:T(8,128)(2,1)S(1)}, bf16[256,256]{1,0:T(8,128)(2,1)S(1)}, u32[]{:S(2)}, u32[]{:S(2)}) collective-permute-start(bf16[256,256]{1,0:T(8,128)(2,1)S(1)} %get-tuple-element.82), channel_id=1, source_target_pairs={{0,24},{8,0},{16,8},{24,16},{1,25},{9,1},{17,9},{25,17},{2,26},{10... | collective-permute-start | bytes 393224 | tf_op jit(solution)/shard_map/ppermute | solution.py:532
  50.3 6.7 %collective-permute-start.24 = (bf16[128,512]{1,0:T(8,128)(2,1)S(1)}, bf16[128,512]{1,0:T(8,128)(2,1)S(1)}, u32[]{:S(2)}, u32[]{:S(2)}) collective-permute-start(bf16[128,512]{1,0:T(8,128)(2,1)S(1)} %get-tuple-element.85), channel_id=1, source_target_pairs={{0,16},{8,24},{16,0},{24,8},{1,17},{9,25},{17,1},{25,9},{2,18},{10... | collective-permute-start | bytes 393224 | tf_op jit(solution)/shard_map/ppermute | solution.py:532
  52.2 7.7 %collective-permute-start.25 = (bf16[128,512]{1,0:T(8,128)(2,1)S(1)}, bf16[128,512]{1,0:T(8,128)(2,1)S(1)}, u32[]{:S(2)}, u32[]{:S(2)}) collective-permute-start(bf16[128,512]{1,0:T(8,128)(2,1)S(1)} %get-tuple-element.86), channel_id=1, source_target_pairs={{0,8},{8,16},{16,24},{24,0},{1,9},{9,17},{17,25},{25,1},{2,10},{10... | collective-permute-start | bytes 393224 | tf_op jit(solution)/shard_map/ppermute | solution.py:532
  52.2 7.7 %collective-permute-start.26 = (bf16[128,512]{1,0:T(8,128)(2,1)S(1)}, bf16[128,512]{1,0:T(8,128)(2,1)S(1)}, u32[]{:S(2)}, u32[]{:S(2)}) collective-permute-start(bf16[128,512]{1,0:T(8,128)(2,1)S(1)} %get-tuple-element.87), channel_id=1, source_target_pairs={{0,24},{8,0},{16,8},{24,16},{1,25},{9,1},{17,9},{25,17},{2,26},{10... | collective-permute-start | bytes 393224 | tf_op jit(solution)/shard_map/ppermute | solution.py:532
  55.4 37.6 %collective-permute-start.14 = (bf16[1024,256]{1,0:T(8,128)(2,1)S(1)}, bf16[1024,256]{1,0:T(8,128)(2,1)S(1)}, u32[]{:S(2)}, u32[]{:S(2)}) collective-permute-start(bf16[1024,256]{1,0:T(8,128)(2,1)S(1)} %get-tuple-element.71), channel_id=1, source_target_pairs={{0,6},{1,3},{2,0},{3,5},{4,2},{5,7},{6,4},{7,1},{8,14},{9,11},{10,... | collective-permute-start | bytes 1572872 | tf_op jit(solution)/shard_map/ppermute | solution.py:527
  55.5 37.5 %collective-permute-start.13 = (bf16[1024,256]{1,0:T(8,128)(2,1)S(1)}, bf16[1024,256]{1,0:T(8,128)(2,1)S(1)}, u32[]{:S(2)}, u32[]{:S(2)}) collective-permute-start(bf16[1024,256]{1,0:T(8,128)(2,1)S(1)} %shard_map.126), channel_id=1, source_target_pairs={{0,2},{1,7},{2,4},{3,1},{4,6},{5,3},{6,0},{7,5},{8,10},{9,15},{10,... | collective-permute-start | bytes 1572872 | tf_op jit(solution)/shard_map/ppermute | solution.py:527
  56.9 5.7 %collective-permute-start.16 = (bf16[144,512]{1,0:T(8,128)(2,1)S(1)}, bf16[144,512]{1,0:T(8,128)(2,1)S(1)}, u32[]{:S(2)}, u32[]{:S(2)}) collective-permute-start(bf16[144,512]{1,0:T(8,128)(2,1)S(1)} %get-tuple-element.75), channel_id=1, source_target_pairs={{0,16},{8,24},{16,0},{24,8},{1,17},{9,25},{17,1},{25,9},{2,18},{10... | collective-permute-start | bytes 442376 | tf_op jit(solution)/shard_map/ppermute | solution.py:532
  59.9 7.9 %collective-permute-start.17 = (bf16[144,512]{1,0:T(8,128)(2,1)S(1)}, bf16[144,512]{1,0:T(8,128)(2,1)S(1)}, u32[]{:S(2)}, u32[]{:S(2)}) collective-permute-start(bf16[144,512]{1,0:T(8,128)(2,1)S(1)} %get-tuple-element.76), channel_id=1, source_target_pairs={{0,8},{8,16},{16,24},{24,0},{1,9},{9,17},{17,25},{25,1},{2,10},{10... | collective-permute-start | bytes 442376 | tf_op jit(solution)/shard_map/ppermute | solution.py:532
  59.9 7.9 %collective-permute-start.18 = (bf16[144,512]{1,0:T(8,128)(2,1)S(1)}, bf16[144,512]{1,0:T(8,128)(2,1)S(1)}, u32[]{:S(2)}, u32[]{:S(2)}) collective-permute-start(bf16[144,512]{1,0:T(8,128)(2,1)S(1)} %get-tuple-element.77), channel_id=1, source_target_pairs={{0,24},{8,0},{16,8},{24,16},{1,25},{9,1},{17,9},{25,17},{2,26},{10... | collective-permute-start | bytes 442376 | tf_op jit(solution)/shard_map/ppermute | solution.py:532
  67.9 9.7 %collective-permute-start.27 = (bf16[448,128]{1,0:T(8,128)(2,1)S(1)}, bf16[448,128]{1,0:T(8,128)(2,1)S(1)}, u32[]{:S(2)}, u32[]{:S(2)}) collective-permute-start(bf16[448,128]{1,0:T(8,128)(2,1)S(1)} %get-tuple-element.88), channel_id=1, source_target_pairs={{0,32},{1,225},{32,64},{33,1},{64,96},{65,33},{96,128},{97,65},{12... | collective-permute-start | bytes 344072 | tf_op jit(solution)/shard_map/ppermute | solution.py:546
  74.2 5.7 %collective-permute-start.28 = (bf16[448,128]{1,0:T(8,128)(2,1)S(1)}, bf16[448,128]{1,0:T(8,128)(2,1)S(1)}, u32[]{:S(2)}, u32[]{:S(2)}) collective-permute-start(bf16[448,128]{1,0:T(8,128)(2,1)S(1)} %get-tuple-element.89), channel_id=1, source_target_pairs={{0,64},{1,193},{32,96},{33,225},{64,128},{65,1},{96,160},{97,33},{... | collective-permute-start | bytes 344072 | tf_op jit(solution)/shard_map/ppermute | solution.py:546
  75.5 8.4 %collective-permute-start.29 = (bf16[448,128]{1,0:T(8,128)(2,1)S(1)}, bf16[448,128]{1,0:T(8,128)(2,1)S(1)}, u32[]{:S(2)}, u32[]{:S(2)}) collective-permute-start(bf16[448,128]{1,0:T(8,128)(2,1)S(1)} %get-tuple-element.90), channel_id=1, source_target_pairs={{0,96},{1,161},{32,128},{33,193},{64,160},{65,225},{96,192},{97,1}... | collective-permute-start | bytes 344072 | tf_op jit(solution)/shard_map/ppermute | solution.py:546
  77.6 6.2 %collective-permute-start.23 = (bf16[448,128]{1,0:T(8,128)(2,1)S(1)}, bf16[448,128]{1,0:T(8,128)(2,1)S(1)}, u32[]{:S(2)}, u32[]{:S(2)}) collective-permute-start(bf16[448,128]{1,0:T(8,128)(2,1)S(1)} %get-tuple-element.83.mine), channel_id=1, source_target_pairs={{0,128},{32,160},{64,192},{96,224},{128,0},{160,32},{192,64},{224,... | collective-permute-start | bytes 344072 | tf_op jit(solution)/shard_map/ppermute | solution.py:546
  84.0 8.4 %collective-permute-start.30 = (f32[224,128]{1,0:T(8,128)S(1)}, f32[224,128]{1,0:T(8,128)S(1)}, u32[]{:S(2)}, u32[]{:S(2)}) collective-permute-start(f32[224,128]{1,0:T(8,128)S(1)} %get-tuple-element.92), channel_id=1, source_target_pairs={{0,1},{1,0},{2,3},{3,2},{4,5},{5,4},{6,7},{7,6},{8,9},{9,8},{10,11... | collective-permute-start | bytes 344072 | tf_op jit(solution)/shard_map/ppermute | solution.py:517
  (3 other events, 24.1 us)
